TPU v7x, 512 devices: a whole 4x8x8 slice. The times are simulated.
512 devices in a mesh: sp: 32 (over z, x), tp: 16 (over y, core).
Axes of the slice: x: 4, y: 8, z: 8, core: 2. Of those that a mesh axis runs over, the one named last changes fastest.
Arguments:
- queries: bfloat16 [12288, 1024], P('sp', 'tp'), may hold values from -6 to 6
- keys: bfloat16 [12288, 1024], P('sp', 'tp'), may hold values from -6 to 6
- values: bfloat16 [12288, 1024], P('sp', 'tp'), may hold values from -6 to 6
- log_cum: float32 [16, 12288], P('tp'), as said below
- residual: bfloat16 [12288, 2048], P('sp', 'tp'), may hold values from -6 to 6
- out_gain: float32 [1024], replicated, may hold values from 0.1 to 1.9
- w_out: bfloat16 [1024, 2048], P(None, 'tp'), may hold values from -0.1875 to 0.1875
- ffn_gain: float32 [2048], replicated, may hold values from 0.1 to 1.9
- routes: int32 [12288, 2], P('sp'), may hold values from 0 to 63, all different within a row; in each aligned block of 384 rows (0 to 383, 384 to 767, ...) at most 24 rows name the same one
- route_weight: float32 [12288, 2], P('sp'), may hold values from 0.25 to 2
- sh_gate: bfloat16 [2048, 512], P(None, 'tp'), may hold values from -0.125 to 0.125
- sh_up: bfloat16 [2048, 512], P(None, 'tp'), may hold values from -0.125 to 0.125
- sh_down: bfloat16 [512, 2048], P(None, 'tp'), may hold values from -0.25 to 0.25
- exp_gate: bfloat16 [64, 2048, 512], P('sp', None, 'tp'), may hold values from -0.125 to 0.125
- exp_up: bfloat16 [64, 2048, 512], P('sp', None, 'tp'), may hold values from -0.125 to 0.125
- exp_down: bfloat16 [64, 512, 2048], P('sp', None, 'tp'), may hold values from -0.25 to 0.25
Outputs:
- result: bfloat16 [12288, 2048], P('sp', 'tp')
Inputs may be any that keep to these rules, and one draw needn't show every extreme that they name: `routes`: in each aligned block of 384 rows no expert is named by more than 24 rows, a bound that some block reaches. `log_cum`: never rises along positions.
All inputs are finite; a program needn't handle non-finite values.
Results may differ from a plain program's by a relative error of at most 0.0095.
Values may be sent and summed in bfloat16 or wider, within the bound.
No kernel may reach another device: no remote copies, remote signals or barrier semaphores. Data moves between devices by JAX's collectives and lax.ppermute only.
A program may use at most 64 MiB of HBM per device.

v0:
```python
import jax
import jax.numpy as jnp
from jax import lax
from jax.sharding import PartitionSpec as P

EPS = 1e-06


def side_by_side(arrays, axis, dim, along):
    ends, at = ([], 0)
    for a in arrays[:-1]:
        at += a.shape[along]
        ends.append(at)
    both = jnp.concatenate(arrays, axis=along)
    return tuple(jnp.split(lax.all_gather(both, axis, axis=dim, tiled=True), ends, axis=along))


def copy_for_each(value, axis):
    copies = jnp.broadcast_to(value, (lax.axis_size(axis), *value.shape))
    return lax.all_to_all(copies, axis, split_axis=0, concat_axis=0, tiled=True)


def joined_along(pieces, dim):
    shape = list(pieces.shape[1:])
    shape[dim] *= pieces.shape[0]
    return jnp.moveaxis(pieces, 0, dim).reshape(shape)


def collect(value, axis, dim):
    pieces = copy_for_each(value, axis)
    return joined_along(pieces, dim)


def rms_scaled(matrix, gain):
    floats = matrix.astype(jnp.float32)
    inverse = lax.rsqrt(jnp.mean(floats * floats, axis=-1, keepdims=True) + EPS)
    return (floats * inverse * gain).astype(jnp.bfloat16)


def gated_hidden(gate, upward):
    return (jax.nn.silu(gate) * upward).astype(jnp.bfloat16)


def per_device(
    queries,
    keys,
    values,
    log_cum,
    residual,
    out_gain,
    w_out,
    ffn_gain,
    routes,
    route_weight,
    sh_gate,
    sh_up,
    sh_down,
    exp_gate,
    exp_up,
    exp_down,
):
    row_count = queries.shape[0]
    heads_here = log_cum.shape[0]
    head_size = queries.shape[1] // heads_here
    scale = head_size ** (-0.5)
    offset = lax.axis_index("sp") * row_count
    query_heads = queries.reshape(row_count, heads_here, head_size)
    query_pos = offset + lax.iota(jnp.int32, row_count)
    cum_query = lax.dynamic_slice_in_dim(log_cum, offset, row_count, 1)
    best = jnp.full((heads_here, row_count), -1e30, jnp.float32)
    key_piece, value_piece = side_by_side((keys, values), "sp", 0, 1)
    count = key_piece.shape[0]
    key_heads = key_piece.reshape(count, heads_here, head_size)
    value_heads = value_piece.reshape(count, heads_here, head_size)
    causal = lax.iota(jnp.int32, count)[None, :] <= query_pos[:, None]
    score = (
        jnp.einsum("qhd,khd->hqk", query_heads, key_heads, preferred_element_type=jnp.float32)
        * scale
    )
    score = jnp.where(causal[None], score + cum_query[:, :, None] - log_cum[:, None, :], -1e30)
    new_best = jnp.maximum(best, jnp.max(score, axis=2))
    weight = jnp.where(causal[None], jnp.exp(score - new_best[:, :, None]), 0.0)
    running_sum = jnp.sum(weight, axis=2)
    weighted = jnp.einsum(
        "hqk,khd->hqd", weight.astype(jnp.bfloat16), value_heads, preferred_element_type=jnp.float32
    )
    best, running_sum, weighted = (new_best, running_sum, weighted)
    head_out = (
        jnp.transpose(weighted / running_sum[:, :, None], (1, 0, 2))
        .reshape(row_count, heads_here * head_size)
        .astype(jnp.bfloat16)
    )
    all_heads = lax.all_gather(head_out, "tp", axis=1, tiled=True)
    mixed = rms_scaled(all_heads, out_gain)
    attended = jnp.dot(mixed, w_out, preferred_element_type=jnp.float32)
    updated = (residual.astype(jnp.float32) + attended).astype(jnp.bfloat16)
    full_rows = collect(updated, "tp", 1)
    normed = rms_scaled(full_rows, ffn_gain)
    width = normed.shape[1]
    shared_part = gated_hidden(
        jnp.dot(normed, sh_gate, preferred_element_type=jnp.float32),
        jnp.dot(normed, sh_up, preferred_element_type=jnp.float32),
    )
    shared_all = lax.all_gather(shared_part, "tp", axis=1, tiled=True)
    shared_out = jnp.dot(shared_all, sh_down, preferred_element_type=jnp.float32)
    top_count = routes.shape[1]
    expert_local = exp_gate.shape[0]
    sp_count = lax.axis_size("sp")
    tp_count = lax.axis_size("tp")
    expert_count = expert_local * sp_count
    capacity = 2 * row_count * top_count // expert_count
    assigned = routes.reshape(-1)
    onehot = (assigned[:, None] == lax.iota(jnp.int32, expert_count)[None, :]).astype(jnp.int32)
    slot_rank = jnp.sum((jnp.cumsum(onehot, axis=0) - 1) * onehot, axis=1)
    slot = assigned * capacity + slot_rank
    owner_row = lax.iota(jnp.int32, assigned.shape[0]) // top_count
    table = jnp.full((expert_count * capacity,), row_count, jnp.int32).at[slot].set(owner_row)
    padded = jnp.concatenate([normed, jnp.zeros((1, width), jnp.bfloat16)], axis=0)
    outgoing = padded[table].reshape(sp_count, expert_local * capacity, width)
    share = expert_local * capacity // tp_count
    portion = lax.dynamic_slice_in_dim(outgoing, lax.axis_index("tp") * share, share, 1)
    landed = lax.all_to_all(portion, "sp", split_axis=0, concat_axis=0, tiled=True)
    arrived = lax.all_gather(landed, "tp", axis=1, tiled=True)
    arrived = arrived.reshape(sp_count, expert_local, capacity, width)
    gate_part = jnp.einsum("secd,edf->secf", arrived, exp_gate, preferred_element_type=jnp.float32)
    up_part = jnp.einsum("secd,edf->secf", arrived, exp_up, preferred_element_type=jnp.float32)
    hidden = gated_hidden(gate_part, up_part)
    hidden_all = lax.all_gather(hidden, "tp", axis=3, tiled=True)
    expert_out = jnp.einsum(
        "secf,efd->secd", hidden_all, exp_down, preferred_element_type=jnp.float32
    ).astype(jnp.bfloat16)
    returned = lax.all_to_all(expert_out, "sp", split_axis=0, concat_axis=0, tiled=True)
    returned = returned.reshape(expert_count * capacity, returned.shape[3])
    picked = returned[slot].astype(jnp.float32) * route_weight.reshape(-1)[:, None]
    routed = jnp.sum(picked.reshape(row_count, top_count, picked.shape[1]), axis=1)
    return (updated.astype(jnp.float32) + shared_out + routed).astype(jnp.bfloat16)


def solution(mesh):
    in_specs = (
        P("sp", "tp"),
        P("sp", "tp"),
        P("sp", "tp"),
        P("tp", None),
        P("sp", "tp"),
        P(),
        P(None, "tp"),
        P(),
        P("sp", None),
        P("sp", None),
        P(None, "tp"),
        P(None, "tp"),
        P(None, "tp"),
        P("sp", None, "tp"),
        P("sp", None, "tp"),
        P("sp", None, "tp"),
    )
    out_specs = P("sp", "tp")
    return jax.shard_map(
        per_device, mesh=mesh, in_specs=in_specs, out_specs=out_specs, check_vma=False
    )
```

profile of v0, /device:TPU:1, one launch (start us, length us, event | category | flops | bytes accessed | tf_op | source)
XLA Modules:
  0.0 371.9 jit_solution(12435414797633586448)
XLA Ops:
  6.5 0.0 copy-start
  6.5 0.0 all-gather.4.cloned.1.call-start
  6.5 1.5 pad_maximum_fusion
  8.1 0.0 all-gather.4.cloned.1.call-update
  8.1 0.7 dynamic-slice_reduce_fusion
  8.8 88.6 %all-gather.4.cloned.1.call-done = bf16[12288,128]{0,1:T(8,128)(2,1)} async-done(((bf16[384,128]{0,1:T(8,128)(2,1)}), bf16[12288,128]{0,1:T(8,128)(2,1)}) %all-gather.4.cloned.1.call-update) | async-done | bytes 3145744 | tf_op jit(solution)/shard_map/all_gather | solution.py:15
  97.4 8.4 %fusion.60 = (f32[384]{0:T(512)S(1)}, f32[384,12288]{0,1:T(8,128)S(1)}) fusion(f32[12288]{0:T(1024)} %bitcast.74, f32[384]{0:T(512)S(1)} %dynamic-slice_reduce_fusion, bf16[384,64]{0,1:T(8,128)(2,1)} %param.16, bf16[12288,128]{0,1:T(8,128)(2,1)} %all-gather.4.cloned.1.call-done, s32[384]{0:T(512)S(1)} %iota_add_fusion), kind=kOutput, calls=%fused_computation.79 | convolution fusion | flops 632290944 | bytes 20550144 | tf_op jit(solution)/shard_map/qhd,khd->hqk/dot_general | solution.py:77
  105.8 0.0 copy-start.6
  105.9 4.8 %fusion = f32[384]{0:T(512)S(1)} fusion(f32[384,12288]{0,1:T(8,128)S(1)} %get-tuple-element.6, f32[384]{0:T(512)S(1)} %broadcast_maximum_fusion, s32[384]{0:T(512)S(1)} %iota_add_fusion), kind=kLoop, calls=%fused_computation.6 | loop fusion | flops 18873984 | bytes 18878976 | tf_op jit(solution)/shard_map/reduce_sum | solution.py:83
  110.6 0.0 copy-done.6
  110.6 0.0 copy-start.7
  110.6 0.0 copy-start.9
  110.6 0.0 copy-start.10
  110.6 3.7 %fusion.38 = bf16[384,64]{0,1:T(8,128)(2,1)S(1)} fusion(f32[384,12288]{0,1:T(8,128)S(1)} %get-tuple-element.6, f32[384]{0:T(512)S(1)} %broadcast_maximum_fusion, s32[384]{0:T(512)S(1)} %iota_add_fusion, bf16[12288,128]{0,1:T(8,128)(2,1)S(1)} %copy-done.6, f32[384]{0:T(512)S(1)} %fusion), kind=kOutput, calls=%fused_computation.40 | convolution fusion | flops 622903296 | bytes 20502528 | tf_op jit(solution)/shard_map/hqk,khd->hqd/dot_general | solution.py:84
  114.4 0.0 copy-start.2
  114.4 23.0 %all_gather.16 = bf16[384,1024]{0,1:T(8,128)(2,1)S(1)} all-gather(bf16[384,64]{0,1:T(8,128)(2,1)S(1)} %fusion.38), channel_id=1, replica_groups=mesh['sp'=32,'tp'=16] {'tp'}, dimensions={1}, use_global_device_ids=true | all-gather | bytes 835584 | tf_op jit(solution)/shard_map/all_gather | solution.py:93
  137.4 0.2 fusion.11
  137.7 0.0 copy-done.7
  137.7 0.0 copy-start.3
  137.7 0.6 fusion.30
  138.3 1.5 broadcast_in_dim.18
  139.8 4.7 %all-to-all-start = ((bf16[16,384,128]{2,1,0:T(8,128)(2,1)}), bf16[16,384,128]{2,1,0:T(8,128)(2,1)S(1)}, u32[]{:S(2)}, u32[]{:S(2)}) async-start(bf16[16,384,128]{2,1,0:T(8,128)(2,1)} %broadcast_in_dim.18), calls=%async_computation | async-start | bytes 3145728 | tf_op jit(solution)/shard_map/all_to_all | solution.py:20
  144.5 0.0 all-gather.6.cloned.1.call-start
  144.5 0.1 copy.40
  144.7 0.1 eq.29
  144.8 0.1 eq.25
  145.0 1.8 reduce-window.6
  146.8 0.3 slice_reduce_fusion
  147.1 0.1 copy.39
  147.2 0.2 mul.113
  147.4 0.1 fusion.51
  147.6 3.4 scatter_custom_fusion
  151.0 32.0 %all-to-all-done = bf16[16,384,128]{2,1,0:T(8,128)(2,1)S(1)} async-done(((bf16[16,384,128]{2,1,0:T(8,128)(2,1)}), bf16[16,384,128]{2,1,0:T(8,128)(2,1)S(1)}, u32[]{:S(2)}, u32[]{:S(2)}) %all-to-all-start) | async-done | bytes 1572896 | tf_op jit(solution)/shard_map/all_to_all | solution.py:20
  183.0 0.4 fusion.8
  183.4 0.0 copy-done.3
  183.4 0.4 fusion.10
  183.8 0.2 concatenate.7
  184.0 7.1 %gather_fusion = bf16[1536,2048]{1,0:T(8,128)(2,1)} fusion(bf16[385,2048]{1,0:T(8,128)(2,1)S(1)} %concatenate.7, s32[2048]{0:T(1024)S(1)} %pad_clamp_fusion), kind=kCustom, calls=%fused_computation | custom fusion | bytes 12589056 | tf_op jit(solution)/shard_map/gather | solution.py:119
  191.1 2.0 constant_dynamic-slice_fusion
  193.1 24.7 %all_to_all.15 = bf16[32,3,2048]{2,1,0:T(4,128)(2,1)S(1)} all-to-all(bf16[32,3,2048]{2,1,0:T(4,128)(2,1)S(1)} %constant_dynamic-slice_fusion), channel_id=1, replica_groups=mesh['sp'=32,'tp'=16] {'sp'}, dimensions={0} | all-to-all | bytes 786432 | tf_op jit(solution)/shard_map/all_to_all | solution.py:122
  217.8 1.1 copy.43
  218.8 0.0 all-gather.6.cloned.1.call-update
  218.8 0.0 all-gather.8.cloned.1.call-start
  218.9 42.5 %all-gather.6.cloned.1.call-done = bf16[32,48,2048]{2,0,1:T(8,128)(2,1)} async-done(((bf16[32,3,2048]{2,0,1:T(8,128)(2,1)}), bf16[32,48,2048]{2,0,1:T(8,128)(2,1)}) %all-gather.6.cloned.1.call-update) | async-done | bytes 6291472 | tf_op jit(solution)/shard_map/all_gather | solution.py:123
  261.4 7.5 %fusion.16 = f32[32,2,24,32]{3,2,0,1:T(8,128)S(1)} fusion(bf16[32,2,24,2048]{3,0,2,1:T(8,128)(2,1)} %bitcast.75, bf16[2,2048,32]{1,2,0:T(8,128)(2,1)} %param.29), kind=kOutput, calls=%fused_computation.26 | convolution fusion | flops 201326592 | bytes 6750208 | tf_op jit(solution)/shard_map/secd,edf->secf/dot_general | solution.py:125
  268.9 0.0 copy-done.5
  269.0 4.7 %fusion.25 = bf16[32,2,24,32]{3,2,0,1:T(8,128)(2,1)S(1)} fusion(bf16[32,2,24,2048]{3,0,2,1:T(8,128)(2,1)S(1)} %bitcast.76, f32[32,2,24,32]{3,2,0,1:T(8,128)S(1)} %fusion.16, bf16[2,2048,32]{1,2,0:T(8,128)(2,1)S(1)} %copy-done.8), kind=kOutput, calls=%fused_computation.30 | convolution fusion | flops 201621504 | bytes 6848512 | tf_op jit(solution)/shard_map/secd,edf->secf/dot_general | solution.py:126
  273.6 1.2 copy.47
  274.8 0.0 all-gather.8.cloned.1.call-update
  274.9 0.0 copy-start.4
  274.9 47.6 %all-gather.8.cloned.1.call-done = bf16[32,2,24,512]{0,2,1,3:T(8,128)(2,1)} async-done(((bf16[32,2,24,32]{0,2,1,3:T(8,128)(2,1)}), bf16[32,2,24,512]{0,2,1,3:T(8,128)(2,1)}) %all-gather.8.cloned.1.call-update) | async-done | bytes 1572880 | tf_op jit(solution)/shard_map/all_gather | solution.py:128
  322.5 7.4 %copy.48 = bf16[32,2,24,512]{3,2,0,1:T(8,128)(2,1)S(1)} copy(bf16[32,2,24,512]{0,2,1,3:T(8,128)(2,1)} %all-gather.8.cloned.1.call-done) | data formatting | bytes 3145728 | tf_op jit(solution)/shard_map/all_gather | solution.py:128
  329.9 0.6 fusion.28
  330.5 0.0 copy-start.1
  330.5 0.8 copy.49
  331.3 9.9 %all-to-all-start.2 = ((bf16[32,2,24,128]{3,2,1,0:T(8,128)(2,1)}), bf16[32,2,24,128]{3,2,1,0:T(8,128)(2,1)S(1)}, u32[]{:S(2)}, u32[]{:S(2)}) async-start(bf16[32,2,24,128]{3,2,1,0:T(8,128)(2,1)} %copy.49), calls=%async_computation.2 | async-start | bytes 786432 | tf_op jit(solution)/shard_map/all_to_all | solution.py:132
  341.2 0.1 copy.50
  341.4 1.5 fusion.61
  342.9 1.5 fusion.32
  344.4 17.5 %all_gather.17 = bf16[384,512]{0,1:T(8,128)(2,1)S(1)} all-gather(bf16[384,32]{0,1:T(8,128)(2,1)S(1)} %fusion.32), channel_id=1, replica_groups=mesh['sp'=32,'tp'=16] {'tp'}, dimensions={1}, use_global_device_ids=true | all-gather | bytes 417792 | tf_op jit(solution)/shard_map/all_gather | solution.py:104
  361.9 0.0 all-to-all-done.2
  361.9 1.9 gather_fusion.1
  363.8 0.6 fusion.46
  364.4 1.0 fusion.31
  (21 shorter events, 0.1 us)
Async XLA Ops:
  6.5 323.4 %copy-start = (bf16[2,512,128]{2,1,0:T(8,128)(2,1)S(1)}, bf16[2,512,128]{2,1,0:T(8,128)(2,1)}, u32[]{:S(2)}) copy-start(bf16[2,512,128]{2,1,0:T(8,128)(2,1)} %param.31) | copy-start | bytes 786436
  6.5 90.9 %all-gather.4.cloned.1.call-start = ((), (), s32[]{:S(2)}) async-start(), calls=%async_computation.3 | async-start | bytes 3244032 | tf_op jit(solution)/shard_map/all_gather | solution.py:15
  105.8 4.8 %copy-start.6 = (bf16[12288,128]{0,1:T(8,128)(2,1)S(1)}, bf16[12288,128]{0,1:T(8,128)(2,1)}, u32[]{:S(2)}) copy-start(bf16[12288,128]{0,1:T(8,128)(2,1)} %all-gather.4.cloned.1.call-done) | copy-start | bytes 9437188
  110.6 27.1 %copy-start.7 = (bf16[1024,128]{1,0:T(8,128)(2,1)S(1)}, bf16[1024,128]{1,0:T(8,128)(2,1)}, u32[]{:S(2)}) copy-start(bf16[1024,128]{1,0:T(8,128)(2,1)} %param.22) | copy-start | bytes 786436
  110.6 27.0 %copy-start.9 = (bf16[384,128]{1,0:T(8,128)(2,1)S(1)}, bf16[384,128]{1,0:T(8,128)(2,1)}, u32[]{:S(2)}) copy-start(bf16[384,128]{1,0:T(8,128)(2,1)} %param.20) | copy-start | bytes 294916
  110.6 27.0 %copy-start.10 = (f32[1024]{0:T(1024)S(1)}, f32[1024]{0:T(1024)}, u32[]{:S(2)}) copy-start(f32[1024]{0:T(1024)} %param.21) | copy-start | bytes 12292
  114.4 30.1 %copy-start.2 = (s32[384,2]{0,1:T(2,128)S(1)}, s32[384,2]{0,1:T(2,128)}, u32[]{:S(2)}) copy-start(s32[384,2]{0,1:T(2,128)} %param.24) | copy-start | bytes 9220
  137.7 45.7 %copy-start.3 = (f32[2048]{0:T(1024)S(1)}, f32[2048]{0:T(1024)}, u32[]{:S(2)}) copy-start(f32[2048]{0:T(1024)} %param.23) | copy-start | bytes 24580
  139.8 43.2 %all-to-all-start = ((bf16[16,384,128]{2,1,0:T(8,128)(2,1)}), bf16[16,384,128]{2,1,0:T(8,128)(2,1)S(1)}, u32[]{:S(2)}, u32[]{:S(2)}) async-start(bf16[16,384,128]{2,1,0:T(8,128)(2,1)} %broadcast_in_dim.18), calls=%async_computation | async-start | bytes 3145728 | tf_op jit(solution)/shard_map/all_to_all | solution.py:20
  144.5 116.9 %all-gather.6.cloned.1.call-start = ((), (), s32[]{:S(2)}) async-start(), calls=%async_computation.4 | async-start | bytes 6684672 | tf_op jit(solution)/shard_map/all_gather | solution.py:123
  218.8 103.6 %all-gather.8.cloned.1.call-start = ((), (), s32[]{:S(2)}) async-start(), calls=%async_computation.5 | async-start | bytes 6684672 | tf_op jit(solution)/shard_map/all_gather | solution.py:128
  261.4 7.5 %copy-start.5 = (bf16[32,48,2048]{2,0,1:T(8,128)(2,1)S(1)}, bf16[32,48,2048]{2,0,1:T(8,128)(2,1)}, u32[]{:S(2)}) copy-start(bf16[32,48,2048]{2,0,1:T(8,128)(2,1)} %all-gather.6.cloned.1.call-done) | copy-start | bytes 18874372
  261.4 7.5 %copy-start.8 = (bf16[2,2048,32]{1,2,0:T(8,128)(2,1)S(1)}, bf16[2,2048,32]{1,2,0:T(8,128)(2,1)}, u32[]{:S(2)}) copy-start(bf16[2,2048,32]{1,2,0:T(8,128)(2,1)} %param.30) | copy-start | bytes 786436
  274.9 66.4 %copy-start.4 = (f32[384,2]{0,1:T(2,128)S(1)}, f32[384,2]{0,1:T(2,128)}, u32[]{:S(2)}) copy-start(f32[384,2]{0,1:T(2,128)} %param.25) | copy-start | bytes 9220
  330.5 33.8 %copy-start.1 = (bf16[512,128]{1,0:T(8,128)(2,1)S(1)}, bf16[512,128]{1,0:T(8,128)(2,1)}, u32[]{:S(2)}) copy-start(bf16[512,128]{1,0:T(8,128)(2,1)} %param.28) | copy-start | bytes 393220
  331.3 30.6 %all-to-all-start.2 = ((bf16[32,2,24,128]{3,2,1,0:T(8,128)(2,1)}), bf16[32,2,24,128]{3,2,1,0:T(8,128)(2,1)S(1)}, u32[]{:S(2)}, u32[]{:S(2)}) async-start(bf16[32,2,24,128]{3,2,1,0:T(8,128)(2,1)} %copy.49), calls=%async_computation.2 | async-start | bytes 786432 | tf_op jit(solution)/shard_map/all_to_all | solution.py:132
Sparse Core Ops, SparseCore 0:
  10.4 86.9 all-gather.3
  219.0 42.3 all-gather.5
  275.0 47.4 all-gather.7
where the time goes:
time: 372 us
  waiting for transfers between devices  211 us (57%)
  blocking collectives  65.2 us (18%)
  matrix products  29.4 us (8%)
  local copies, waits for them, and re-layouts  28.4 us (8%)
  starting transfers between devices  14.6 us (4%)
  between operations  13.5 us (4%)
  other arithmetic  9.93 us (3%)
    all_gather x1, waiting for transfers between devices, side_by_side(): lax.all_gather(both, axis, axis=dim, tiled=True)  88.6 us
    all_gather x1, waiting for transfers between devices, per_device(): hidden_all = lax.all_gather(hidden, 'tp', axis=3, tiled=True)  47.6 us
    all_gather x1, waiting for transfers between devices, per_device(): arrived = lax.all_gather(landed, 'tp', axis=1, tiled=True)  42.5 us
    all_to_all x1, waiting for transfers between devices, copy_for_each(): return lax.all_to_all(copies, axis, split_axis=0, concat_axis=0, tiled=True)  32 us
    all_to_all x1, blocking collectives, per_device(): lax.all_to_all(portion, 'sp', split_axis=0, concat_axis=0, tiled=True)  24.7 us
    all_gather x1, blocking collectives, per_device(): all_heads = lax.all_gather(head_out, 'tp', axis=1, tiled=True)  23 us
    all_gather x1, blocking collectives, per_device(): shared_all = lax.all_gather(shared_part, 'tp', axis=1, tiled=True)  17.5 us
    all_to_all x1, starting transfers between devices, per_device(): lax.all_to_all(expert_out, 'sp', split_axis=0, concat_axis=0, tiled=True)  9.9 us
  transfers between devices with their start and end apart: 5, of which 4 were waited for; matrix products, arithmetic and copies ran while one was open for 3% of the time, Pallas kernels for 0%

commit v1 on v0

v1 whole, which is shorter than its diff:
```python
import jax
import jax.numpy as jnp
from jax import lax
from jax.experimental import pallas as pl
from jax.experimental.pallas import tpu as pltpu
from jax.sharding import Mesh, PartitionSpec as P

EPS = 1e-06
LANES = 128
LOW = -1e30
PAD = 16
BF16 = jnp.bfloat16
F32 = jnp.float32
GRIDS = {32: (8, 4), 4: (2, 2), 8: (4, 2)}


def exchange(value, axis):
    return lax.all_to_all(value, axis, split_axis=0, concat_axis=0, tiled=True)


def copy_to_each(value, axis):
    return exchange(jnp.broadcast_to(value, (lax.axis_size(axis), *value.shape)), axis)


def three_parts(value):
    high = value.astype(BF16)
    rest = value - high.astype(F32)
    middle = rest.astype(BF16)
    low = (rest - middle.astype(F32)).astype(BF16)
    return [high, middle, low]


def attention_kernel(place, kv, query, cum, out, *, width, query_tile):
    zone, column = place[0], place[1]
    head = query.shape[1]
    count = query.shape[0]
    keys_each = kv.shape[2]
    total = count * width
    queries = jnp.concatenate([query[j] for j in range(count)], axis=1)
    ones = jnp.ones((PAD, total), BF16)
    queries = jnp.concatenate([queries, ones], axis=0)
    tiles = total // query_tile

    def step(block, state, masked):
        key_t = kv[block, :head, :]
        value_t = kv[block, head:, :]
        parts = three_parts(-cum[pl.ds(block, 1), :])
        filler = jnp.zeros((PAD - 3, keys_each), BF16)
        key_t = jnp.concatenate([key_t, *parts, filler], axis=0)
        result = []
        for i in range(tiles):
            best, total_weight, acc = state[i]
            part = queries[:, i * query_tile : (i + 1) * query_tile]
            score = lax.dot_general(
                key_t, part, (((0,), (0,)), ((), ())), preferred_element_type=F32
            )
            if masked:
                key_pos = column * width + lax.broadcasted_iota(jnp.int32, score.shape, 0)
                query_pos = i * query_tile + lax.broadcasted_iota(jnp.int32, score.shape, 1)
                score = jnp.where(key_pos <= query_pos, score, LOW)
            new_best = jnp.maximum(best, jnp.max(score, axis=0, keepdims=True))
            weight = jnp.exp(score - new_best)
            keep = jnp.exp(best - new_best)
            total_weight = total_weight * keep + jnp.sum(weight, axis=0, keepdims=True)
            acc = acc * keep + jnp.dot(
                value_t, weight.astype(BF16), preferred_element_type=F32
            )
            result.append((new_best, total_weight, acc))
        return tuple(result)

    start = tuple(
        (
            jnp.full((1, query_tile), LOW, F32),
            jnp.zeros((1, query_tile), F32),
            jnp.zeros((head, query_tile), F32),
        )
        for _ in range(tiles)
    )
    state = lax.fori_loop(0, zone, lambda block, s: step(block, s, False), start)
    state = step(zone, state, True)
    best = jnp.concatenate([s[0] for s in state], axis=1)
    weight = jnp.concatenate([s[1] for s in state], axis=1)
    acc = jnp.concatenate([s[2] for s in state], axis=1)
    normal = (acc / weight).astype(BF16)
    parts = three_parts(best + jnp.log(weight))
    full = jnp.concatenate([normal, *parts, jnp.zeros((PAD - 3, total), BF16)], axis=0)
    for j in range(count):
        out[j] = full[:, j * width : (j + 1) * width]


def partial_attention(place, kv, query, cum):
    count, head, width = query.shape
    total = count * width
    tile = 512 if total % 512 == 0 else width
    return pl.pallas_call(
        lambda *refs: attention_kernel(*refs, width=width, query_tile=tile),
        out_shape=jax.ShapeDtypeStruct((count, head + PAD, width), BF16),
        in_specs=[
            pl.BlockSpec(memory_space=pltpu.SMEM),
            pl.BlockSpec(memory_space=pltpu.VMEM),
            pl.BlockSpec(memory_space=pltpu.VMEM),
            pl.BlockSpec(memory_space=pltpu.VMEM),
        ],
        out_specs=pl.BlockSpec(memory_space=pltpu.VMEM),
        compiler_params=pltpu.CompilerParams(vmem_limit_bytes=40 * 1024 * 1024),
        name="partial_attention",
    )(place, kv, query, cum)


def rms_inverse(squares, count):
    return lax.rsqrt(squares / count + EPS)


def gated_hidden(gate, upward):
    return (jax.nn.silu(gate) * upward).astype(BF16)


def wide_shard(matrix):
    columns, rows = matrix.shape[-2], matrix.shape[-1]
    turned = jnp.swapaxes(matrix, -1, -2)
    split = turned.reshape(-1, rows, columns // LANES, LANES)
    return jnp.swapaxes(split, 1, 2).reshape(-1, LANES)


def joined_wide(pieces, hidden):
    shards = pieces.shape[0]
    blocks = pieces.reshape(shards, -1, hidden, LANES)
    return jnp.transpose(blocks, (0, 2, 1, 3)).reshape(shards * hidden, -1)


def joined_tall(pieces):
    shards, inner = pieces.shape[0], pieces.shape[1]
    return jnp.transpose(pieces, (1, 0, 2)).reshape(inner, shards * LANES)


def feed_forward(rows, gate, upward, down):
    across = (((1,), (1,)), ((), ()))
    hidden = gated_hidden(
        lax.dot_general(rows, gate, across, preferred_element_type=F32),
        lax.dot_general(rows, upward, across, preferred_element_type=F32),
    )
    return jnp.dot(hidden, down, preferred_element_type=F32).astype(BF16)


def per_device(
    queries,
    keys,
    values,
    log_cum,
    residual,
    out_gain,
    w_out,
    ffn_gain,
    routes,
    route_weight,
    sh_gate,
    sh_up,
    sh_down,
    exp_gate,
    exp_up,
    exp_down,
):
    width, head = queries.shape
    zones, columns = lax.axis_size("z"), lax.axis_size("x")
    shards = lax.axis_size("tp")
    blocks = zones * columns
    zone, column, shard = lax.axis_index("z"), lax.axis_index("x"), lax.axis_index("tp")
    features = shards * LANES
    hidden = sh_gate.shape[1]
    inner = hidden * shards
    local_experts = exp_gate.shape[0]
    teams = shards // local_experts

    scale = head ** (-0.5)
    key_value = jnp.concatenate([keys.T, values.T], axis=0)
    query = (queries.T.astype(F32) * scale).astype(BF16)
    key_value = copy_to_each(key_value, "z")
    query = copy_to_each(query, "x")
    cum = lax.dynamic_index_in_dim(
        log_cum.reshape(zones, columns, width), column, 1, keepdims=False
    )

    packed = jnp.concatenate(
        [
            wide_shard(exp_gate),
            wide_shard(exp_up),
            exp_down.reshape(-1, LANES),
            wide_shard(sh_gate),
            wide_shard(sh_up),
            sh_down,
        ],
        axis=0,
    )
    packed = lax.all_gather(packed, "tp", axis=0, tiled=False)

    place = jnp.stack([zone, column]).astype(jnp.int32)
    partial = partial_attention(place, key_value, query, cum)
    partial = exchange(partial, "x").astype(F32)
    level = partial[:, head] + partial[:, head + 1] + partial[:, head + 2]
    share = jnp.exp(level - jnp.max(level, axis=0, keepdims=True))
    share = share / jnp.sum(share, axis=0, keepdims=True)
    head_out = jnp.sum(partial[:, :head] * share[:, None], axis=0).astype(BF16)

    all_heads = lax.all_gather(head_out, "tp", axis=0, tiled=True).astype(F32)
    inverse = rms_inverse(jnp.sum(all_heads * all_heads, axis=0, keepdims=True), all_heads.shape[0])
    mixed = (all_heads * inverse * out_gain[:, None]).astype(BF16)
    attended = lax.dot_general(mixed, w_out, (((0,), (0,)), ((), ())), preferred_element_type=F32)
    updated = (residual.astype(F32) + attended).astype(BF16)

    top = routes.shape[1]
    experts = local_experts * blocks
    capacity = 2 * width * top // experts
    slots = experts * capacity
    chosen = [routes[:, k, None] == lax.iota(jnp.int32, experts)[None, :] for k in range(top)]
    named = sum(c.astype(BF16) for c in chosen)
    earlier = (lax.iota(jnp.int32, width)[:, None] > lax.iota(jnp.int32, width)[None, :]).astype(BF16)
    rank = jnp.dot(earlier, named, preferred_element_type=F32)
    picks = []
    for k in range(top):
        own = jnp.sum(jnp.where(chosen[k], rank, 0.0), axis=1).astype(jnp.int32)
        slot = routes[:, k] * capacity + own
        picks.append(slot[:, None] == lax.iota(jnp.int32, slots)[None, :])
    select = sum(p.astype(BF16) for p in picks)
    weights = sum(jnp.where(p, route_weight[:, k, None], 0.0) for k, p in enumerate(picks))
    weight_high = lax.reduce_precision(weights, 8, 7)
    weight_low = (weights - weight_high).astype(BF16)
    weight_high = weight_high.astype(BF16)

    outgoing = lax.dot_general(
        select, updated, (((0,), (0,)), ((), ())), preferred_element_type=F32
    ).astype(BF16)
    per_block = local_experts * capacity
    landed = exchange(outgoing.reshape(blocks, per_block, LANES), ("z", "x"))
    rounds = blocks // teams
    landed = landed.reshape(rounds, teams, local_experts, capacity, LANES)
    landed = jnp.transpose(landed, (2, 1, 0, 3, 4)).reshape(shards, rounds * capacity, LANES)
    routed_rows = rounds * capacity
    own_rows = width // shards
    mixed_rows = jnp.concatenate([landed, updated.reshape(shards, own_rows, LANES)], axis=1)
    rows = exchange(mixed_rows, "tp").astype(F32)
    inverse = rms_inverse(jnp.sum(rows * rows, axis=(0, 2), keepdims=True), features)
    normed = (rows * inverse * ffn_gain.reshape(shards, 1, LANES)).astype(BF16)
    normed = jnp.transpose(normed, (1, 0, 2)).reshape(routed_rows + own_rows, features)

    mine = shard // teams
    wide = features * hidden // LANES
    tall = inner
    at = 0

    def piece(base, size):
        return lax.dynamic_slice_in_dim(packed, base, size, 1)

    gate = joined_wide(piece(at + mine * wide, wide), hidden)
    at += local_experts * wide
    upward = joined_wide(piece(at + mine * wide, wide), hidden)
    at += local_experts * wide
    down = joined_tall(piece(at + mine * tall, tall))
    at += local_experts * tall
    shared_gate = joined_wide(packed[:, at : at + wide], hidden)
    at += wide
    shared_up = joined_wide(packed[:, at : at + wide], hidden)
    at += wide
    shared_down = joined_tall(packed[:, at : at + tall])

    routed_out = feed_forward(normed[:routed_rows], gate, upward, down)
    shared_out = feed_forward(normed[routed_rows:], shared_gate, shared_up, shared_down)
    returned = jnp.concatenate([routed_out, shared_out], axis=0)
    returned = jnp.transpose(returned.reshape(-1, shards, LANES), (1, 0, 2))
    returned = exchange(returned, "tp")
    shared = returned[:, routed_rows:].reshape(width, LANES).astype(F32)
    returned = returned[:, :routed_rows].reshape(local_experts, teams, rounds, capacity, LANES)
    returned = jnp.transpose(returned, (2, 1, 0, 3, 4)).reshape(blocks, per_block, LANES)
    answers = exchange(returned, ("z", "x")).reshape(slots, LANES)
    routed = jnp.dot(weight_high, answers, preferred_element_type=F32) + jnp.dot(
        weight_low, answers, preferred_element_type=F32
    )
    return (updated.astype(F32) + shared + routed).astype(BF16)


def solution(mesh):
    blocks, shards = mesh.devices.shape
    zones, columns = GRIDS[blocks]
    grid = Mesh(mesh.devices.reshape(zones, columns, shards), ("z", "x", "tp"))
    sp = ("z", "x")
    in_specs = (
        P(sp, "tp"),
        P(sp, "tp"),
        P(sp, "tp"),
        P("tp", None),
        P(sp, "tp"),
        P(),
        P(None, "tp"),
        P(),
        P(sp, None),
        P(sp, None),
        P(None, "tp"),
        P(None, "tp"),
        P(None, "tp"),
        P(sp, None, "tp"),
        P(sp, None, "tp"),
        P(sp, None, "tp"),
    )
    return jax.shard_map(
        per_device, mesh=grid, in_specs=in_specs, out_specs=P(sp, "tp"), check_vma=False
    )
```

time: 372 us -> 231 us (0.62)
  waiting for transfers between devices: 211 us -> 61.8 us
  matrix products: 29.4 us -> 12.3 us
  starting transfers between devices: 14.6 us -> 28.8 us
  blocking collectives: 65.2 us -> 73 us
  other arithmetic: 9.93 us -> 2.56 us
  local copies, waits for them, and re-layouts: 28.4 us -> 35.1 us
    all_gather x3 -> x1, waiting for transfers between devices: 179 us -> 0.02 us  [per_device(): packed = lax.all_gather(packed, 'tp', axis=0, tiled=False)]
    all_to_all x2 -> x5, waiting for transfers between devices: 32 us -> 61.7 us  [exchange(): return lax.all_to_all(value, axis, split_axis=0, concat_axis=0, tiled=True)]
    all_to_all x1 -> x2, blocking collectives: 24.7 us -> 45.2 us  [exchange(): return lax.all_to_all(value, axis, split_axis=0, concat_axis=0, tiled=True)]
    transpose x0 -> x8, local copies, waits for them, and re-layouts: none -> 18.6 us  [the longest x4 11 us: joined_wide(): return jnp.transpose(blocks, (0, 2, 1, 3)).reshape(shards * hidden, -1)]
    dot_general x9, matrix products: 29.4 us -> 12.3 us  [the longest x2 6.54 us: feed_forward(): return jnp.dot(hidden, down, preferred_element_type=F32).astype(BF16)]
    all_to_all x2 -> x5, starting transfers between devices: 14.6 us -> 28.8 us  [exchange(): return lax.all_to_all(value, axis, split_axis=0, concat_axis=0, tiled=True)]
    all_gather x2 -> x1, blocking collectives: 40.6 us -> 27.8 us  [per_device(): all_heads = lax.all_gather(head_out, 'tp', axis=0, tiled=True).astype(F32)]
    gather x2 -> x0, local copies, waits for them, and re-layouts: 8.96 us -> none  [the longest x1 7.09 us: per_device(): outgoing = padded[table].reshape(sp_count, expert_local * capacity, width)]
  transfers between devices with their start and end apart: 5 -> 6, of which waited for: 4 -> 5; matrix products, arithmetic and copies ran while one was open for 3% -> 3% of each run, Pallas kernels for 0% -> 1%
where the time goes in v1:
time: 231 us; the launch traced here: 230 us
  blocking collectives  73 us (32%)
  waiting for transfers between devices  61.8 us (27%)
  local copies, waits for them, and re-layouts  35.1 us (15%)
  starting transfers between devices  28.8 us (12%)
  between operations  13.8 us (6%)
  matrix products  12.3 us (5%)
  Pallas kernels  2.73 us (1%)
  other arithmetic  2.56 us (1%)
    all_to_all x5, waiting for transfers between devices, exchange(): return lax.all_to_all(value, axis, split_axis=0, concat_axis=0, tiled=True)  61.7 us
    all_to_all x2, blocking collectives, exchange(): return lax.all_to_all(value, axis, split_axis=0, concat_axis=0, tiled=True)  45.2 us
    all_to_all x5, starting transfers between devices, exchange(): return lax.all_to_all(value, axis, split_axis=0, concat_axis=0, tiled=True)  28.8 us
    all_gather x1, blocking collectives, per_device(): all_heads = lax.all_gather(head_out, 'tp', axis=0, tiled=True).astype(F32)  27.8 us
    transpose x4, local copies, waits for them, and re-layouts, joined_wide(): return jnp.transpose(blocks, (0, 2, 1, 3)).reshape(shards * hidden, -1)  11 us
    dynamic_slice x1, local copies, waits for them, and re-layouts, piece(): return lax.dynamic_slice_in_dim(packed, base, size, 1)  9.21 us
    transpose x2, local copies, waits for them, and re-layouts, joined_tall(): return jnp.transpose(pieces, (1, 0, 2)).reshape(inner, shards * LANES)  6.78 us
    dot_general x2, matrix products, feed_forward(): return jnp.dot(hidden, down, preferred_element_type=F32).astype(BF16)  6.54 us
  transfers between devices with their start and end apart: 6, of which 5 were waited for; matrix products, arithmetic and copies ran while one was open for 3% of the time, Pallas kernels for 1%

profile of v1, /device:TPU:1, one launch (start us, length us, event | category | flops | bytes accessed | tf_op | source)
XLA Modules:
  0.0 230.1 jit_solution(11558886057441520440)
XLA Ops:
  6.5 0.0 copy-start
  6.5 0.0 all-gather.3.cloned.1.call-start
  6.6 0.9 copy-done
  7.6 1.0 copy_bitcast_fusion
  8.6 0.0 copy-start.8
  8.6 0.9 copy.73
  9.6 0.0 copy-done.6
  9.6 0.0 copy-start.10
  9.6 0.0 copy-start.11
  9.8 0.0 copy-done.7
  9.9 0.0 copy-start.9
  9.9 1.0 copy-done.4
  10.9 0.0 all-gather.3.cloned.1.call-update
  10.9 0.0 copy-start.12
  11.0 0.7 broadcast_in_dim.48
  11.7 4.8 %all-to-all-start.1 = ((bf16[4,64,384]{2,1,0:T(8,128)(2,1)}), bf16[4,64,384]{2,1,0:T(8,128)(2,1)S(1)}, u32[]{:S(2)}, u32[]{:S(2)}) async-start(bf16[4,64,384]{2,1,0:T(8,128)(2,1)} %broadcast_in_dim.48), calls=%async_computation.1 | async-start | bytes 393216 | tf_op jit(solution)/shard_map/all_to_all | solution.py:18
  16.5 0.0 copy-done.11
  16.5 5.2 %all-to-all-done.1.refs_2_ = bf16[4,64,384]{2,1,0:T(8,128)(2,1)S(1)} async-done(((bf16[4,64,384]{2,1,0:T(8,128)(2,1)}), bf16[4,64,384]{2,1,0:T(8,128)(2,1)S(1)}, u32[]{:S(2)}, u32[]{:S(2)}) %all-to-all-start.1) | async-done | bytes 196640 | tf_op jit(solution)/shard_map/all_to_all | solution.py:18
  21.7 0.9 broadcast_in_dim.47
  22.6 10.0 %all-to-all-start = ((bf16[8,128,384]{2,1,0:T(8,128)(2,1)}), bf16[8,128,384]{2,1,0:T(8,128)(2,1)S(1)}, u32[]{:S(2)}, u32[]{:S(2)}) async-start(bf16[8,128,384]{2,1,0:T(8,128)(2,1)} %broadcast_in_dim.47), calls=%async_computation | async-start | bytes 1572864 | tf_op jit(solution)/shard_map/all_to_all | solution.py:18
  32.6 0.6 broadcast.53
  33.2 0.8 reduce.16
  34.1 0.1 pad_add_fusion.refs_0_
  34.1 0.0 copy-done.12
  34.2 20.1 %all-to-all-done.refs_1_ = bf16[8,128,384]{2,1,0:T(8,128)(2,1)S(1)} async-done(((bf16[8,128,384]{2,1,0:T(8,128)(2,1)}), bf16[8,128,384]{2,1,0:T(8,128)(2,1)S(1)}, u32[]{:S(2)}, u32[]{:S(2)}) %all-to-all-start) | async-done | bytes 786464 | tf_op jit(solution)/shard_map/all_to_all | solution.py:18
  54.3 2.7 %partial_attention.1 = bf16[4,80,384]{2,1,0:T(8,128)(2,1)} custom-call(s32[2]{0:T(128)S(1)} %pad_add_fusion.refs_0_, bf16[8,128,384]{2,1,0:T(8,128)(2,1)S(1)} %all-to-all-done.refs_1_, bf16[4,64,384]{2,1,0:T(8,128)(2,1)S(1)} %all-to-all-done.1.refs_2_, f32[8,384]{1,0:T(8,128)S(1)} %bitcast.157), custom_call_target="tpu_custom_call" | custom-call | tf_op jit(solution)/shard_map/partial_attention/pallas_call | solution.py:95
  57.0 3.5 %all-to-all-start.2 = ((bf16[4,80,384]{2,1,0:T(8,128)(2,1)}), bf16[4,80,384]{2,1,0:T(8,128)(2,1)S(1)}, u32[]{:S(2)}, u32[]{:S(2)}) async-start(bf16[4,80,384]{2,1,0:T(8,128)(2,1)} %partial_attention.1), calls=%async_computation.2 | async-start | bytes 491520 | tf_op jit(solution)/shard_map/all_to_all | solution.py:18
  60.5 0.2 select_reduce_fusion.1
  60.8 5.2 %all-to-all-done.2 = bf16[4,80,384]{2,1,0:T(8,128)(2,1)S(1)} async-done(((bf16[4,80,384]{2,1,0:T(8,128)(2,1)}), bf16[4,80,384]{2,1,0:T(8,128)(2,1)S(1)}, u32[]{:S(2)}, u32[]{:S(2)}) %all-to-all-start.2) | async-done | bytes 245792 | tf_op jit(solution)/shard_map/all_to_all | solution.py:18
  66.2 27.8 %all_gather.9 = bf16[1024,384]{1,0:T(8,128)(2,1)S(1)} all-gather(bf16[64,384]{1,0:T(8,128)(2,1)S(1)} %fusion.57), channel_id=1, replica_groups=mesh['z'=8,'x'=4,'tp'=16] {'tp'}, dimensions={0}, use_global_device_ids=true | all-gather | bytes 835584 | tf_op jit(solution)/shard_map/all_gather | solution.py:204
  94.0 0.2 fusion.15
  94.3 0.6 fusion.31
  94.9 0.9 convolution_convert_fusion
  95.8 0.0 copy-start.13
  95.8 25.9 %all_to_all.35 = bf16[32,48,128]{2,1,0:T(8,128)(2,1)S(1)} all-to-all(bf16[32,48,128]{2,1,0:T(8,128)(2,1)S(1)} %bitcast.180), channel_id=1, replica_groups=mesh['z'=8,'x'=4,'tp'=16] {'z','x'}, dimensions={0} | all-to-all | bytes 786432 | tf_op jit(solution)/shard_map/all_to_all | solution.py:18
  121.8 0.8 pad_maximum_fusion
  122.6 6.5 %all-to-all-start.4 = ((bf16[16,120,128]{2,1,0:T(8,128)(2,1)}), bf16[16,120,128]{2,1,0:T(8,128)(2,1)S(1)}, u32[]{:S(2)}, u32[]{:S(2)}) async-start(bf16[16,120,128]{2,1,0:T(8,128)(2,1)} %pad_maximum_fusion), calls=%async_computation.4 | async-start | bytes 983040 | tf_op jit(solution)/shard_map/all_to_all | solution.py:18
  129.0 16.5 %all-to-all-done.4 = bf16[16,120,128]{2,1,0:T(8,128)(2,1)S(1)} async-done(((bf16[16,120,128]{2,1,0:T(8,128)(2,1)}), bf16[16,120,128]{2,1,0:T(8,128)(2,1)S(1)}, u32[]{:S(2)}, u32[]{:S(2)}) %all-to-all-start.4) | async-done | bytes 491552 | tf_op jit(solution)/shard_map/all_to_all | solution.py:18
  145.6 0.2 fusion.46
  145.8 0.0 copy-done.13
  145.8 0.2 fusion.53
  146.0 0.0 all-gather.3.cloned.1.call-done
  146.0 9.2 %constant_dynamic-slice_fusion.1 = (bf16[16,512,128]{2,1,0:T(8,128)(2,1)}, bf16[512,16,128]{2,0,1:T(8,128)(2,1)}, bf16[16,512,128]{2,1,0:T(8,128)(2,1)}, bf16[16...) fusion(bf16[16,4608,128]{2,1,0:T(8,128)(2,1)} %bitcast.160, ...), kind=kLoop, calls=%fused_computation.116 | loop fusion | bytes 25165836 | tf_op jit(solution)/shard_map/dynamic_slice | solution.py:251
  155.2 2.9 %copy.62 = bf16[512,16,128]{0,2,1:T(8,128)(2,1)S(1)} copy(bf16[512,16,128]{2,0,1:T(8,128)(2,1)} %get-tuple-element.16) | data formatting | bytes 4194304 | tf_op jit(solution)/shard_map/transpose | solution.py:133
  158.1 4.0 %copy.61 = bf16[16,32,16,128]{3,2,1,0:T(8,128)(2,1)} copy(bf16[16,32,16,128]{3,1,2,0:T(8,128)(2,1)} %bitcast.164) | data formatting | bytes 4194304 | tf_op jit(solution)/shard_map/transpose | solution.py:128
  162.1 0.0 copy-done.2
  162.1 2.2 copy.60
  164.3 3.9 %copy.58 = bf16[512,16,128]{0,2,1:T(8,128)(2,1)} copy(bf16[512,16,128]{2,0,1:T(8,128)(2,1)} %get-tuple-element.19) | data formatting | bytes 4194304 | tf_op jit(solution)/shard_map/transpose | solution.py:133
  168.2 4.0 %copy.57 = bf16[16,32,16,128]{3,2,1,0:T(8,128)(2,1)} copy(bf16[16,32,16,128]{3,1,2,0:T(8,128)(2,1)} %bitcast.162) | data formatting | bytes 4194304 | tf_op jit(solution)/shard_map/transpose | solution.py:128
  172.2 0.0 copy-done.1
  172.2 0.9 copy.56
  173.1 0.7 copy-done.3
  173.8 0.7 fusion.6
  174.4 0.8 fusion.12
  175.2 2.8 %convolution_convert_fusion.2 = bf16[24,2048]{1,0:T(8,128)(2,1)S(1)} fusion(bf16[512,2048]{0,1:T(8,128)(2,1)S(1)} %bitcast.158, bf16[64,8,16,128]{3,2,1,0:T(8,128)(2,1)} %bitcast.159, f32[24,512]{1,0:T(8,128)S(1)} %fusion.6, bf16[120,16,128]{2,0,1:T(8,128)(2,1)S(1)} %fusion.53), kind=kOutput, calls=%fused_computation.10 | convolution fusion | flops 100786176 | bytes 4440064 | tf_op jit(solution)/shard_map/dot_general | solution.py:142
  178.1 3.7 %convolution_convert_fusion.1 = bf16[96,2048]{1,0:T(8,128)(2,1)S(1)} fusion(bf16[512,2048]{0,1:T(8,128)(2,1)} %bitcast.165, bf16[64,8,16,128]{3,2,1,0:T(8,128)(2,1)} %bitcast.166, f32[96,512]{1,0:T(8,128)S(1)} %fusion.12, bf16[120,16,128]{2,0,1:T(8,128)(2,1)S(1)} %fusion.53), kind=kOutput, calls=%fused_computation.9 | convolution fusion | flops 403144704 | bytes 5177344 | tf_op jit(solution)/shard_map/dot_general | solution.py:142
  181.7 0.0 copy-start.14
  181.8 0.1 bitcast_bitcast_fusion
  181.9 19.3 %all_to_all.36 = bf16[16,120,128]{2,1,0:T(8,128)(2,1)S(1)} all-to-all(bf16[16,120,128]{2,1,0:T(8,128)(2,1)S(1)} %bitcast_bitcast_fusion), channel_id=1, replica_groups=mesh['z'=8,'x'=4,'tp'=16] {'tp'}, dimensions={0} | all-to-all | bytes 983040 | tf_op jit(solution)/shard_map/all_to_all | solution.py:18
  201.2 0.8 copy.64
  201.9 3.9 %all-to-all-start.6 = ((bf16[32,48,128]{2,1,0:T(8,128)(2,1)}), bf16[32,48,128]{2,1,0:T(8,128)(2,1)S(1)}, u32[]{:S(2)}, u32[]{:S(2)}) async-start(bf16[32,48,128]{2,1,0:T(8,128)(2,1)} %bitcast.43), calls=%async_computation.6 | async-start | bytes 786432 | tf_op jit(solution)/shard_map/all_to_all | solution.py:18
  205.9 14.7 %all-to-all-done.6 = bf16[32,48,128]{2,1,0:T(8,128)(2,1)S(1)} async-done(((bf16[32,48,128]{2,1,0:T(8,128)(2,1)}), bf16[32,48,128]{2,1,0:T(8,128)(2,1)S(1)}, u32[]{:S(2)}, u32[]{:S(2)}) %all-to-all-start.6) | async-done | bytes 393248 | tf_op jit(solution)/shard_map/all_to_all | solution.py:18
  220.7 1.2 fusion.23
  221.9 1.4 fusion.32
  (49 shorter events, 0.7 us)
Async XLA Ops:
  6.5 1.0 copy-start
  6.5 3.0 %copy-start.6 = (bf16[2048,32]{0,1:T(8,128)(2,1)S(1)}, bf16[2048,32]{0,1:T(8,128)(2,1)}, u32[]{:S(2)}) copy-start(bf16[2048,32]{0,1:T(8,128)(2,1)} %param.27) | copy-start | bytes 393220
  6.5 3.2 %copy-start.5 = (bf16[2,512,128]{2,1,0:T(8,128)(2,1)S(1)}, bf16[2,512,128]{2,1,0:T(8,128)(2,1)}, u32[]{:S(2)}) copy-start(bf16[2,512,128]{2,1,0:T(8,128)(2,1)} %param.31) | copy-start | bytes 786436
  6.5 3.3 %copy-start.7 = (bf16[512,128]{1,0:T(8,128)(2,1)S(1)}, bf16[512,128]{1,0:T(8,128)(2,1)}, u32[]{:S(2)}) copy-start(bf16[512,128]{1,0:T(8,128)(2,1)} %param.28) | copy-start | bytes 393220
  6.5 139.4 %all-gather.3.cloned.1.call-start = ((), (), s32[]{:S(2)}) async-start(), calls=%async_computation.7 | async-start | bytes 20054016 | tf_op jit(solution)/shard_map/all_gather | solution.py:194
  8.6 2.4 %copy-start.8 = (bf16[384,64]{0,1:T(8,128)(2,1)S(1)}, bf16[384,64]{0,1:T(8,128)(2,1)}, u32[]{:S(2)}) copy-start(bf16[384,64]{0,1:T(8,128)(2,1)} %param.16) | copy-start | bytes 147460
  9.6 6.9 %copy-start.10 = (bf16[384,64]{0,1:T(8,128)(2,1)S(1)}, bf16[384,64]{0,1:T(8,128)(2,1)}, u32[]{:S(2)}) copy-start(bf16[384,64]{0,1:T(8,128)(2,1)} %param.18) | copy-start | bytes 147460
  9.6 6.9 %copy-start.11 = (bf16[384,64]{0,1:T(8,128)(2,1)S(1)}, bf16[384,64]{0,1:T(8,128)(2,1)}, u32[]{:S(2)}) copy-start(bf16[384,64]{0,1:T(8,128)(2,1)} %param.17) | copy-start | bytes 147460
  9.9 1.0 copy-start.4
  9.9 23.4 %copy-start.9 = (f32[1,12288]{1,0:T(1,128)S(1)}, f32[1,12288]{1,0:T(1,128)}, u32[]{:S(2)}) copy-start(f32[1,12288]{1,0:T(1,128)} %param.19) | copy-start | bytes 147460
  10.9 23.2 %copy-start.12 = (s32[384,2]{0,1:T(2,128)S(1)}, s32[384,2]{0,1:T(2,128)}, u32[]{:S(2)}) copy-start(s32[384,2]{0,1:T(2,128)} %param.24) | copy-start | bytes 9220
  11.7 10.0 %all-to-all-start.1 = ((bf16[4,64,384]{2,1,0:T(8,128)(2,1)}), bf16[4,64,384]{2,1,0:T(8,128)(2,1)S(1)}, u32[]{:S(2)}, u32[]{:S(2)}) async-start(bf16[4,64,384]{2,1,0:T(8,128)(2,1)} %broadcast_in_dim.48), calls=%async_computation.1 | async-start | bytes 393216 | tf_op jit(solution)/shard_map/all_to_all | solution.py:18
  22.6 31.6 %all-to-all-start = ((bf16[8,128,384]{2,1,0:T(8,128)(2,1)}), bf16[8,128,384]{2,1,0:T(8,128)(2,1)S(1)}, u32[]{:S(2)}, u32[]{:S(2)}) async-start(bf16[8,128,384]{2,1,0:T(8,128)(2,1)} %broadcast_in_dim.47), calls=%async_computation | async-start | bytes 1572864 | tf_op jit(solution)/shard_map/all_to_all | solution.py:18
  57.0 37.3 %copy-start.15 = (bf16[1024,128]{1,0:T(8,128)(2,1)S(1)}, bf16[1024,128]{1,0:T(8,128)(2,1)}, u32[]{:S(2)}) copy-start(bf16[1024,128]{1,0:T(8,128)(2,1)} %param.22) | copy-start | bytes 786436
  57.0 37.3 %copy-start.16 = (bf16[384,128]{1,0:T(8,128)(2,1)S(1)}, bf16[384,128]{1,0:T(8,128)(2,1)}, u32[]{:S(2)}) copy-start(bf16[384,128]{1,0:T(8,128)(2,1)} %param.20) | copy-start | bytes 294916
  57.0 37.3 %copy-start.17 = (f32[1024]{0:T(1024)S(1)}, f32[1024]{0:T(1024)}, u32[]{:S(2)}) copy-start(f32[1024]{0:T(1024)} %param.21) | copy-start | bytes 12292
  57.0 9.0 %all-to-all-start.2 = ((bf16[4,80,384]{2,1,0:T(8,128)(2,1)}), bf16[4,80,384]{2,1,0:T(8,128)(2,1)S(1)}, u32[]{:S(2)}, u32[]{:S(2)}) async-start(bf16[4,80,384]{2,1,0:T(8,128)(2,1)} %partial_attention.1), calls=%async_computation.2 | async-start | bytes 491520 | tf_op jit(solution)/shard_map/all_to_all | solution.py:18
  95.8 50.0 %copy-start.13 = (f32[2048]{0:T(1024)S(1)}, f32[2048]{0:T(1024)}, u32[]{:S(2)}) copy-start(f32[2048]{0:T(1024)} %param.23) | copy-start | bytes 24580
  122.6 23.0 %all-to-all-start.4 = ((bf16[16,120,128]{2,1,0:T(8,128)(2,1)}), bf16[16,120,128]{2,1,0:T(8,128)(2,1)S(1)}, u32[]{:S(2)}, u32[]{:S(2)}) async-start(bf16[16,120,128]{2,1,0:T(8,128)(2,1)} %pad_maximum_fusion), calls=%async_computation.4 | async-start | bytes 983040 | tf_op jit(solution)/shard_map/all_to_all | solution.py:18
  158.1 4.0 %copy-start.2 = (bf16[16,512,128]{2,1,0:T(8,128)(2,1)S(1)}, bf16[16,512,128]{2,1,0:T(8,128)(2,1)}, u32[]{:S(2)}) copy-start(bf16[16,512,128]{2,1,0:T(8,128)(2,1)} %get-tuple-element.18) | copy-start | bytes 6291460
  168.2 4.0 %copy-start.1 = (bf16[16,512,128]{2,1,0:T(8,128)(2,1)S(1)}, bf16[16,512,128]{2,1,0:T(8,128)(2,1)}, u32[]{:S(2)}) copy-start(bf16[16,512,128]{2,1,0:T(8,128)(2,1)} %get-tuple-element.15) | copy-start | bytes 6291460
  172.2 1.6 copy-start.3
  181.7 24.1 %copy-start.14 = (f32[384,2]{0,1:T(2,128)S(1)}, f32[384,2]{0,1:T(2,128)}, u32[]{:S(2)}) copy-start(f32[384,2]{0,1:T(2,128)} %param.25) | copy-start | bytes 9220
  201.9 18.8 %all-to-all-start.6 = ((bf16[32,48,128]{2,1,0:T(8,128)(2,1)}), bf16[32,48,128]{2,1,0:T(8,128)(2,1)S(1)}, u32[]{:S(2)}, u32[]{:S(2)}) async-start(bf16[32,48,128]{2,1,0:T(8,128)(2,1)} %bitcast.43), calls=%async_computation.6 | async-start | bytes 786432 | tf_op jit(solution)/shard_map/all_to_all | solution.py:18
Sparse Core Ops, SparseCore 0:
  11.0 117.6 all-gather.2

commit v2 on v1

--- a/solution.py
+++ b/solution.py
@@ -4,6 +4,7 @@
 from jax.experimental import pallas as pl
 from jax.experimental.pallas import tpu as pltpu
 from jax.sharding import Mesh, PartitionSpec as P
+
 
 EPS = 1e-06
 LANES = 128
@@ -107,39 +108,114 @@
     )(place, kv, query, cum)
 
 
-def rms_inverse(squares, count):
-    return lax.rsqrt(squares / count + EPS)
-
-
 def gated_hidden(gate, upward):
     return (jax.nn.silu(gate) * upward).astype(BF16)
 
 
-def wide_shard(matrix):
-    columns, rows = matrix.shape[-2], matrix.shape[-1]
-    turned = jnp.swapaxes(matrix, -1, -2)
-    split = turned.reshape(-1, rows, columns // LANES, LANES)
-    return jnp.swapaxes(split, 1, 2).reshape(-1, LANES)
-
-
-def joined_wide(pieces, hidden):
-    shards = pieces.shape[0]
-    blocks = pieces.reshape(shards, -1, hidden, LANES)
-    return jnp.transpose(blocks, (0, 2, 1, 3)).reshape(shards * hidden, -1)
-
-
-def joined_tall(pieces):
-    shards, inner = pieces.shape[0], pieces.shape[1]
-    return jnp.transpose(pieces, (1, 0, 2)).reshape(inner, shards * LANES)
-
-
-def feed_forward(rows, gate, upward, down):
+def pack_kernel(*refs, shapes):
+    sources, target, sem = refs[:-2], refs[-2], refs[-1]
+    at = 0
+    for source, shape in zip(sources, shapes):
+        if len(shape) == 3:
+            count, rows, columns = shape
+            for e in range(count):
+                for k in range(columns // LANES):
+                    pltpu.make_async_copy(
+                        source.at[e, :, pl.ds(k * LANES, LANES)],
+                        target.at[pl.ds(at, rows), :],
+                        sem,
+                    ).start()
+                    at += rows
+        else:
+            rows = shape[0]
+            pltpu.make_async_copy(source, target.at[pl.ds(at, rows), :], sem).start()
+            at += rows
+    pltpu.make_async_copy(target, target, sem).wait()
+
+
+def packed_shards(*sources):
+    shapes = [source.shape for source in sources]
+    total = sum(source.size for source in sources) // LANES
+    return pl.pallas_call(
+        lambda *refs: pack_kernel(*refs, shapes=shapes),
+        out_shape=jax.ShapeDtypeStruct((total, LANES), BF16),
+        in_specs=[pl.BlockSpec(memory_space=pltpu.HBM) for _ in sources],
+        out_specs=pl.BlockSpec(memory_space=pltpu.HBM),
+        scratch_shapes=[pltpu.SemaphoreType.DMA],
+        name="pack_shards",
+    )(*sources)
+
+
+def feed_kernel(which, rows, gain, weights, out, gate, upward, *rest, first, count, experts):
+    down, sems = rest if len(rest) == 2 else (None, rest[0])
+    shards, hidden = gate.shape[0], gate.shape[1]
+    inner = shards * hidden
+    features = shards * LANES
+    mine = which[0]
+    wide = features * hidden // LANES
+    bases = [mine * wide, (experts + mine) * wide, 2 * experts * wide + mine * inner]
+    for n, target in enumerate((gate, upward)):
+        base = pl.multiple_of(bases[n], hidden)
+        for k in range(features // LANES):
+            pltpu.make_async_copy(
+                weights.at[:, pl.ds(base + k * hidden, hidden), :],
+                target.at[:, :, pl.ds(k * LANES, LANES)],
+                sems.at[n],
+            ).start()
+    base = pl.multiple_of(bases[2], hidden)
+    for t in range(shards if down is not None else 0):
+        pltpu.make_async_copy(
+            weights.at[t, pl.ds(base, inner), :], down.at[:, pl.ds(t * LANES, LANES)], sems.at[2]
+        ).start()
+
+    floats = [rows[t, first : first + count, :].astype(F32) for t in range(shards)]
+    squares = sum(f * f for f in floats)
+    mean = jnp.sum(squares, axis=1, keepdims=True) / features
+    inverse = lax.rsqrt(mean + EPS)
+    normed = jnp.concatenate([(f * inverse * gain[t]).astype(BF16) for t, f in enumerate(floats)], axis=1)
     across = (((1,), (1,)), ((), ()))
-    hidden = gated_hidden(
-        lax.dot_general(rows, gate, across, preferred_element_type=F32),
-        lax.dot_general(rows, upward, across, preferred_element_type=F32),
-    )
-    return jnp.dot(hidden, down, preferred_element_type=F32).astype(BF16)
+    pltpu.make_async_copy(gate, gate, sems.at[0]).wait()
+    first_half = lax.dot_general(
+        normed, gate[...].reshape(inner, features), across, preferred_element_type=F32
+    )
+    pltpu.make_async_copy(upward, upward, sems.at[1]).wait()
+    second_half = lax.dot_general(
+        normed, upward[...].reshape(inner, features), across, preferred_element_type=F32
+    )
+    inside = gated_hidden(first_half, second_half)
+    if down is None:
+        out[...] = inside
+        return
+    pltpu.make_async_copy(down, down, sems.at[2]).wait()
+    for t in range(shards):
+        part = jnp.dot(inside, down[:, t * LANES : (t + 1) * LANES], preferred_element_type=F32)
+        out[t] = part.astype(BF16)
+
+
+def feed_forward(which, rows, gain, weights, hidden, first, count, experts, whole=True):
+    shards = rows.shape[0]
+    features = shards * LANES
+    inner = shards * hidden
+    shape = (shards, count, LANES) if whole else (count, inner)
+    down = [pltpu.VMEM((inner, features), BF16)] if whole else []
+    return pl.pallas_call(
+        lambda *refs: feed_kernel(*refs, first=first, count=count, experts=experts),
+        out_shape=jax.ShapeDtypeStruct(shape, BF16),
+        in_specs=[
+            pl.BlockSpec(memory_space=pltpu.SMEM),
+            pl.BlockSpec(memory_space=pltpu.VMEM),
+            pl.BlockSpec(memory_space=pltpu.VMEM),
+            pl.BlockSpec(memory_space=pltpu.HBM),
+        ],
+        out_specs=pl.BlockSpec(memory_space=pltpu.VMEM),
+        scratch_shapes=[
+            pltpu.VMEM((shards, hidden, features), BF16),
+            pltpu.VMEM((shards, hidden, features), BF16),
+            *down,
+            pltpu.SemaphoreType.DMA((3,)),
+        ],
+        compiler_params=pltpu.CompilerParams(vmem_limit_bytes=(54 if whole else 61) * 1024 * 1024),
+    )(which, rows, gain, weights)
 
 
 def per_device(
@@ -165,33 +241,24 @@
     shards = lax.axis_size("tp")
     blocks = zones * columns
     zone, column, shard = lax.axis_index("z"), lax.axis_index("x"), lax.axis_index("tp")
-    features = shards * LANES
     hidden = sh_gate.shape[1]
-    inner = hidden * shards
     local_experts = exp_gate.shape[0]
     teams = shards // local_experts
 
     scale = head ** (-0.5)
     key_value = jnp.concatenate([keys.T, values.T], axis=0)
+    key_value = copy_to_each(key_value, "z")
     query = (queries.T.astype(F32) * scale).astype(BF16)
-    key_value = copy_to_each(key_value, "z")
-    query = copy_to_each(query, "x")
+    query = lax.all_gather(query, "x", axis=0, tiled=False)
     cum = lax.dynamic_index_in_dim(
         log_cum.reshape(zones, columns, width), column, 1, keepdims=False
     )
-
-    packed = jnp.concatenate(
-        [
-            wide_shard(exp_gate),
-            wide_shard(exp_up),
-            exp_down.reshape(-1, LANES),
-            wide_shard(sh_gate),
-            wide_shard(sh_up),
-            sh_down,
-        ],
-        axis=0,
-    )
-    packed = lax.all_gather(packed, "tp", axis=0, tiled=False)
+    expert_weights = packed_shards(
+        jnp.swapaxes(exp_gate, 1, 2), jnp.swapaxes(exp_up, 1, 2), exp_down.reshape(-1, LANES)
+    )
+    expert_weights = lax.all_gather(expert_weights, "tp", axis=0, tiled=False)
+    shared_weights = packed_shards(sh_gate.T[None], sh_up.T[None])
+    shared_weights = lax.all_gather(shared_weights, "tp", axis=0, tiled=False)
 
     place = jnp.stack([zone, column]).astype(jnp.int32)
     partial = partial_attention(place, key_value, query, cum)
@@ -202,7 +269,8 @@
     head_out = jnp.sum(partial[:, :head] * share[:, None], axis=0).astype(BF16)
 
     all_heads = lax.all_gather(head_out, "tp", axis=0, tiled=True).astype(F32)
-    inverse = rms_inverse(jnp.sum(all_heads * all_heads, axis=0, keepdims=True), all_heads.shape[0])
+    mean = jnp.sum(all_heads * all_heads, axis=0, keepdims=True) / all_heads.shape[0]
+    inverse = lax.rsqrt(mean + EPS)
     mixed = (all_heads * inverse * out_gain[:, None]).astype(BF16)
     attended = lax.dot_general(mixed, w_out, (((0,), (0,)), ((), ())), preferred_element_type=F32)
     updated = (residual.astype(F32) + attended).astype(BF16)
@@ -237,40 +305,29 @@
     routed_rows = rounds * capacity
     own_rows = width // shards
     mixed_rows = jnp.concatenate([landed, updated.reshape(shards, own_rows, LANES)], axis=1)
-    rows = exchange(mixed_rows, "tp").astype(F32)
-    inverse = rms_inverse(jnp.sum(rows * rows, axis=(0, 2), keepdims=True), features)
-    normed = (rows * inverse * ffn_gain.reshape(shards, 1, LANES)).astype(BF16)
-    normed = jnp.transpose(normed, (1, 0, 2)).reshape(routed_rows + own_rows, features)
-
-    mine = shard // teams
-    wide = features * hidden // LANES
-    tall = inner
-    at = 0
-
-    def piece(base, size):
-        return lax.dynamic_slice_in_dim(packed, base, size, 1)
-
-    gate = joined_wide(piece(at + mine * wide, wide), hidden)
-    at += local_experts * wide
-    upward = joined_wide(piece(at + mine * wide, wide), hidden)
-    at += local_experts * wide
-    down = joined_tall(piece(at + mine * tall, tall))
-    at += local_experts * tall
-    shared_gate = joined_wide(packed[:, at : at + wide], hidden)
-    at += wide
-    shared_up = joined_wide(packed[:, at : at + wide], hidden)
-    at += wide
-    shared_down = joined_tall(packed[:, at : at + tall])
-
-    routed_out = feed_forward(normed[:routed_rows], gate, upward, down)
-    shared_out = feed_forward(normed[routed_rows:], shared_gate, shared_up, shared_down)
-    returned = jnp.concatenate([routed_out, shared_out], axis=0)
-    returned = jnp.transpose(returned.reshape(-1, shards, LANES), (1, 0, 2))
-    returned = exchange(returned, "tp")
-    shared = returned[:, routed_rows:].reshape(width, LANES).astype(F32)
-    returned = returned[:, :routed_rows].reshape(local_experts, teams, rounds, capacity, LANES)
+    rows = exchange(mixed_rows, "tp")
+    gain = ffn_gain.reshape(shards, 1, LANES)
+    mine = (shard // teams).astype(jnp.int32)[None]
+    routed_out = feed_forward(
+        mine, rows, gain, expert_weights, hidden, 0, routed_rows, local_experts
+    )
+    returned = exchange(routed_out, "tp")
+    returned = returned.reshape(local_experts, teams, rounds, capacity, LANES)
     returned = jnp.transpose(returned, (2, 1, 0, 3, 4)).reshape(blocks, per_block, LANES)
     answers = exchange(returned, ("z", "x")).reshape(slots, LANES)
+    share_hidden = feed_forward(
+        jnp.zeros((1,), jnp.int32),
+        rows,
+        gain,
+        shared_weights,
+        hidden,
+        routed_rows,
+        own_rows,
+        1,
+        whole=False,
+    )
+    share_hidden = lax.all_gather(share_hidden, "tp", axis=0, tiled=True)
+    shared = jnp.dot(share_hidden, sh_down, preferred_element_type=F32)
     routed = jnp.dot(weight_high, answers, preferred_element_type=F32) + jnp.dot(
         weight_low, answers, preferred_element_type=F32
     )

time: 231 us -> 231 us (level)
  Pallas kernels: 2.73 us -> 47 us
  local copies, waits for them, and re-layouts: 35.1 us -> 3.3 us
  waiting for transfers between devices: 61.8 us -> 37.4 us
  blocking collectives: 73 us -> 96.4 us
  matrix products: 12.3 us -> 4.8 us
  starting transfers between devices: 28.8 us -> 25.5 us
    pallas_call x0 -> x4, Pallas kernels: none -> 44.3 us  [the longest x2 34 us: packed_shards(): pl.pallas_call(lambda *refs: pack_kernel(*refs, shapes=shapes), out_shape...]
    all_gather x0 -> x2, blocking collectives: none -> 26.8 us  [the longest x1 15.8 us: per_device(): share_hidden = lax.all_gather(share_hidden, 'tp', axis=0, tiled=True)]
    all_to_all x5 -> x4, waiting for transfers between devices: 61.7 us -> 37.4 us  [exchange(): return lax.all_to_all(value, axis, split_axis=0, concat_axis=0, tiled=True)]
    transpose x7 -> x0, local copies, waits for them, and re-layouts: 18.6 us -> none  [the longest x4 11 us: joined_wide(): return jnp.transpose(blocks, (0, 2, 1, 3)).reshape(shards * hidden, -1)]
    dynamic_slice x1 -> x0, local copies, waits for them, and re-layouts: 9.21 us -> none  [piece(): return lax.dynamic_slice_in_dim(packed, base, size, 1)]
    dot_general x4 -> x1, matrix products: 7.98 us -> 0.91 us  [per_device(): shared = jnp.dot(share_hidden, sh_down, preferred_element_type=F32)]
    all_to_all x5 -> x4, starting transfers between devices: 28.8 us -> 25.4 us  [exchange(): return lax.all_to_all(value, axis, split_axis=0, concat_axis=0, tiled=True)]
    unnamed x46 -> x25, local copies, waits for them, and re-layouts: 4.37 us -> 1.42 us
  transfers between devices with their start and end apart: 6 -> 6, of which waited for: 5 -> 3; matrix products, arithmetic and copies ran while one was open for 3% -> 3% of each run, Pallas kernels for 1% -> 10%
where the time goes in v2:
time: 231 us; the launch traced here: 230 us
  blocking collectives  96.4 us (42%)
  Pallas kernels  47 us (20%)
  waiting for transfers between devices  37.4 us (16%)
  starting transfers between devices  25.5 us (11%)
  between operations  13.7 us (6%)
  matrix products  4.8 us (2%)
  local copies, waits for them, and re-layouts  3.3 us (1%)
    all_to_all x2, blocking collectives, exchange(): return lax.all_to_all(value, axis, split_axis=0, concat_axis=0, tiled=True)  43.5 us
    all_to_all x4, waiting for transfers between devices, exchange(): return lax.all_to_all(value, axis, split_axis=0, concat_axis=0, tiled=True)  37.4 us
    pallas_call x2, Pallas kernels, packed_shards(): pl.pallas_call(lambda *refs: pack_kernel(*refs, shapes=shapes), out_shape...  34 us
    all_gather x1, blocking collectives, per_device(): all_heads = lax.all_gather(head_out, 'tp', axis=0, tiled=True).astype(F32)  26.2 us
    all_to_all x4, starting transfers between devices, exchange(): return lax.all_to_all(value, axis, split_axis=0, concat_axis=0, tiled=True)  25.4 us
    all_gather x1, blocking collectives, per_device(): share_hidden = lax.all_gather(share_hidden, 'tp', axis=0, tiled=True)  15.8 us
    all_gather x1, blocking collectives, per_device(): query = lax.all_gather(query, 'x', axis=0, tiled=False)  11 us
    pallas_call x2, Pallas kernels, feed_forward(): pl.pallas_call(lambda *refs: feed_kernel(*refs, first=first, count=count,...  10.3 us
  transfers between devices with their start and end apart: 6, of which 3 were waited for; matrix products, arithmetic and copies ran while one was open for 3% of the time, Pallas kernels for 10%

profile of v2, /device:TPU:1, one launch (start us, length us, event | category | flops | bytes accessed | tf_op | source)
XLA Modules:
  0.0 230.3 jit_solution(1279357962115299504)
XLA Ops:
  6.5 0.0 copy-start
  6.5 0.0 copy-start.6
  6.5 0.0 copy-start.5
  6.5 0.0 all-gather.8.cloned.1.call-start
  6.5 25.0 %pack_shards.3 = bf16[3072,128]{1,0:T(8,128)(2,1)} custom-call(bf16[2,32,2048]{2,1,0:T(8,128)(2,1)} %bitcast.60, bf16[2,32,2048]{2,1,0:T(8,128)(2,1)} %bitcast.61, bf16[1024,128]{1,0:T(8,128)(2,1)} %bitcast.62), custom_call_target="tpu_custom_call" | custom-call | tf_op jit(solution)/shard_map/pack_shards/pallas_call | solution.py:139
  31.5 0.0 copy-start.3
  31.5 0.0 copy-start.4
  31.5 0.0 copy-start.7
  31.5 0.0 all-gather.8.cloned.1.call-update
  31.6 0.0 all-gather.6.cloned.1.call-start
  31.6 9.1 %pack_shards.2 = bf16[1024,128]{1,0:T(8,128)(2,1)} custom-call(bf16[1,32,2048]{2,1,0:T(8,128)(2,1)} %bitcast.63, bf16[1,32,2048]{2,1,0:T(8,128)(2,1)} %bitcast.64), custom_call_target="tpu_custom_call" | custom-call | tf_op jit(solution)/shard_map/pack_shards/pallas_call | solution.py:139
  40.7 0.0 all-gather.6.cloned.1.call-update
  40.7 0.0 copy-done.6
  40.7 0.0 copy-done.5
  40.7 1.0 broadcast_in_dim.52
  41.7 10.9 %all-to-all-start = ((bf16[8,128,384]{2,1,0:T(8,128)(2,1)}), bf16[8,128,384]{2,1,0:T(8,128)(2,1)S(1)}, u32[]{:S(2)}, u32[]{:S(2)}) async-start(bf16[8,128,384]{2,1,0:T(8,128)(2,1)} %broadcast_in_dim.52), calls=%async_computation | async-start | bytes 1572864 | tf_op jit(solution)/shard_map/all_to_all | solution.py:19
  52.6 0.6 broadcast.38
  53.2 0.0 copy-done.3
  53.2 0.8 reduce.16
  54.1 0.0 copy-done.4
  54.1 11.0 %all-gather = bf16[256,384]{1,0:T(8,128)(2,1)S(1)} all-gather(bf16[64,384]{1,0:T(8,128)(2,1)S(1)} %fusion.25), channel_id=2, replica_groups=mesh['z'=8,'x'=4,'tp'=16] {'x'}, dimensions={0}, use_global_device_ids=true | all-gather | bytes 245760 | tf_op jit(solution)/shard_map/all_gather | solution.py:252
  65.1 0.1 pad_add_fusion.refs_0_
  65.1 0.0 copy-done.7
  65.2 11.0 %all-to-all-done.refs_1_ = bf16[8,128,384]{2,1,0:T(8,128)(2,1)S(1)} async-done(((bf16[8,128,384]{2,1,0:T(8,128)(2,1)}), bf16[8,128,384]{2,1,0:T(8,128)(2,1)S(1)}, u32[]{:S(2)}, u32[]{:S(2)}) %all-to-all-start) | async-done | bytes 786464 | tf_op jit(solution)/shard_map/all_to_all | solution.py:19
  76.2 0.0 copy-start.9
  76.2 0.0 copy-start.10
  76.2 2.7 %partial_attention.1 = bf16[4,80,384]{2,1,0:T(8,128)(2,1)} custom-call(s32[2]{0:T(128)S(1)} %pad_add_fusion.refs_0_, bf16[8,128,384]{2,1,0:T(8,128)(2,1)S(1)} %all-to-all-done.refs_1_, bf16[4,64,384]{2,1,0:T(8,128)(2,1)S(1)} %bitcast.49, f32[8,384]{1,0:T(8,128)S(1)} %bitcast.50), custom_call_target="tpu_custom_call" | custom-call | tf_op jit(solution)/shard_map/partial_attention/pallas_call | solution.py:96
  78.9 4.0 %all-to-all-start.1 = ((bf16[4,80,384]{2,1,0:T(8,128)(2,1)}), bf16[4,80,384]{2,1,0:T(8,128)(2,1)S(1)}, u32[]{:S(2)}, u32[]{:S(2)}) async-start(bf16[4,80,384]{2,1,0:T(8,128)(2,1)} %partial_attention.1), calls=%async_computation.1 | async-start | bytes 491520 | tf_op jit(solution)/shard_map/all_to_all | solution.py:19
  82.9 0.2 select_reduce_fusion.1
  83.2 5.3 %all-to-all-done.1 = bf16[4,80,384]{2,1,0:T(8,128)(2,1)S(1)} async-done(((bf16[4,80,384]{2,1,0:T(8,128)(2,1)}), bf16[4,80,384]{2,1,0:T(8,128)(2,1)S(1)}, u32[]{:S(2)}, u32[]{:S(2)}) %all-to-all-start.1) | async-done | bytes 245792 | tf_op jit(solution)/shard_map/all_to_all | solution.py:19
  88.7 26.2 %all_gather.26 = bf16[1024,384]{1,0:T(8,128)(2,1)S(1)} all-gather(bf16[64,384]{1,0:T(8,128)(2,1)S(1)} %fusion.22), channel_id=1, replica_groups=mesh['z'=8,'x'=4,'tp'=16] {'tp'}, dimensions={0}, use_global_device_ids=true | all-gather | bytes 835584 | tf_op jit(solution)/shard_map/all_gather | solution.py:271
  114.8 0.2 fusion.3
  115.1 0.0 copy-done
  115.1 0.0 copy-done.9
  115.1 0.0 copy-done.10
  115.1 0.6 fusion.16
  115.7 0.9 convolution_convert_fusion
  116.6 25.3 %all_to_all.30 = bf16[32,48,128]{2,1,0:T(8,128)(2,1)S(1)} all-to-all(bf16[32,48,128]{2,1,0:T(8,128)(2,1)S(1)} %bitcast.58), channel_id=1, replica_groups=mesh['z'=8,'x'=4,'tp'=16] {'z','x'}, dimensions={0} | all-to-all | bytes 786432 | tf_op jit(solution)/shard_map/all_to_all | solution.py:19
  141.9 0.8 pad_maximum_fusion
  142.7 6.4 %all-to-all-start.3 = ((bf16[16,120,128]{2,1,0:T(8,128)(2,1)}), bf16[16,120,128]{2,1,0:T(8,128)(2,1)S(1)}, u32[]{:S(2)}, u32[]{:S(2)}) async-start(bf16[16,120,128]{2,1,0:T(8,128)(2,1)} %pad_maximum_fusion), calls=%async_computation.3 | async-start | bytes 983040 | tf_op jit(solution)/shard_map/all_to_all | solution.py:19
  149.1 21.1 %all-to-all-done.3.refs_1_ = bf16[16,120,128]{2,1,0:T(8,128)(2,1)S(1)} async-done(((bf16[16,120,128]{2,1,0:T(8,128)(2,1)}), bf16[16,120,128]{2,1,0:T(8,128)(2,1)S(1)}, u32[]{:S(2)}, u32[]{:S(2)}) %all-to-all-start.3) | async-done | bytes 491552 | tf_op jit(solution)/shard_map/all_to_all | solution.py:19
  170.2 0.0 copy-start.1
  170.2 0.0 all-gather.8.cloned.1.call-done
  170.2 0.8 copy-done.1
  171.0 5.5 %shard_map.155 = bf16[16,96,128]{2,1,0:T(8,128)(2,1)} custom-call(s32[1]{0:T(128)} %bitcast.18.refs_0_, bf16[16,120,128]{2,1,0:T(8,128)(2,1)} %copy-done.1, f32[16,1,128]{2,1,0:T(1,128)} %bitcast.67, bf16[16,3072,128]{2,1,0:T(8,128)(2,1)} %bitcast.51), custom_call_target="tpu_custom_call" | custom-call | tf_op jit(solution)/shard_map/pallas_call | solution.py:201
  176.5 0.0 copy-start.8
  176.5 18.2 %all_to_all.31 = bf16[16,96,128]{2,1,0:T(8,128)(2,1)S(1)} all-to-all(bf16[16,96,128]{2,1,0:T(8,128)(2,1)} %shard_map.155), channel_id=1, replica_groups=mesh['z'=8,'x'=4,'tp'=16] {'tp'}, dimensions={0} | all-to-all | bytes 786432 | tf_op jit(solution)/shard_map/all_to_all | solution.py:19
  194.8 0.8 copy.23
  195.6 4.1 %all-to-all-start.5 = ((bf16[32,48,128]{2,1,0:T(8,128)(2,1)}), bf16[32,48,128]{2,1,0:T(8,128)(2,1)S(1)}, u32[]{:S(2)}, u32[]{:S(2)}) async-start(bf16[32,48,128]{2,1,0:T(8,128)(2,1)} %bitcast.25), calls=%async_computation.5 | async-start | bytes 786432 | tf_op jit(solution)/shard_map/all_to_all | solution.py:19
  199.7 0.0 copy-done.8
  199.7 0.0 all-gather.6.cloned.1.call-done
  199.8 4.7 %shard_map.154 = bf16[24,512]{1,0:T(8,128)(2,1)} custom-call(s32[1]{0:T(128)} %constant.44.clone.1.refs_0_, bf16[16,120,128]{2,1,0:T(8,128)(2,1)} %copy-done.1, f32[16,1,128]{2,1,0:T(1,128)} %bitcast.68, bf16[16,1024,128]{2,1,0:T(8,128)(2,1)} %bitcast.52), custom_call_target="tpu_custom_call" | custom-call | tf_op jit(solution)/shard_map/pallas_call | solution.py:201
  204.5 15.8 %all_gather.29 = bf16[384,512]{1,0:T(8,128)(2,1)S(1)} all-gather(bf16[24,512]{1,0:T(8,128)(2,1)} %shard_map.154), channel_id=1, replica_groups=mesh['z'=8,'x'=4,'tp'=16] {'tp'}, dimensions={0}, use_global_device_ids=true | all-gather | bytes 417792 | tf_op jit(solution)/shard_map/all_gather | solution.py:329
  220.3 0.0 all-to-all-done.5
  220.3 1.2 fusion.11
  221.5 0.0 copy-start.2
  221.5 1.0 fusion.15
  222.5 0.0 copy-done.2
  222.5 0.9 fusion.17
  (18 shorter events, 0.3 us)
Async XLA Ops:
  6.5 108.5 %copy-start = (bf16[1024,128]{1,0:T(8,128)(2,1)S(1)}, bf16[1024,128]{1,0:T(8,128)(2,1)}, u32[]{:S(2)}) copy-start(bf16[1024,128]{1,0:T(8,128)(2,1)} %param.22) | copy-start | bytes 786436
  6.5 34.2 %copy-start.6 = (bf16[384,64]{0,1:T(8,128)(2,1)S(1)}, bf16[384,64]{0,1:T(8,128)(2,1)}, u32[]{:S(2)}) copy-start(bf16[384,64]{0,1:T(8,128)(2,1)} %param.17) | copy-start | bytes 147460
  6.5 34.2 %copy-start.5 = (bf16[384,64]{0,1:T(8,128)(2,1)S(1)}, bf16[384,64]{0,1:T(8,128)(2,1)}, u32[]{:S(2)}) copy-start(bf16[384,64]{0,1:T(8,128)(2,1)} %param.18) | copy-start | bytes 147460
  6.5 163.7 %all-gather.8.cloned.1.call-start = ((), (), s32[]{:S(2)}) async-start(), calls=%async_computation.7 | async-start | bytes 13369344 | tf_op jit(solution)/shard_map/all_gather | solution.py:259
  31.5 21.7 %copy-start.3 = (f32[1,12288]{1,0:T(1,128)S(1)}, f32[1,12288]{1,0:T(1,128)}, u32[]{:S(2)}) copy-start(f32[1,12288]{1,0:T(1,128)} %param.19) | copy-start | bytes 147460
  31.5 22.5 %copy-start.4 = (bf16[384,64]{0,1:T(8,128)(2,1)S(1)}, bf16[384,64]{0,1:T(8,128)(2,1)}, u32[]{:S(2)}) copy-start(bf16[384,64]{0,1:T(8,128)(2,1)} %param.16) | copy-start | bytes 147460
  31.5 33.6 %copy-start.7 = (s32[384,2]{0,1:T(2,128)S(1)}, s32[384,2]{0,1:T(2,128)}, u32[]{:S(2)}) copy-start(s32[384,2]{0,1:T(2,128)} %param.24) | copy-start | bytes 9220
  31.6 168.2 %all-gather.6.cloned.1.call-start = ((), (), s32[]{:S(2)}) async-start(), calls=%async_computation.6 | async-start | bytes 4456448 | tf_op jit(solution)/shard_map/all_gather | solution.py:261
  41.7 34.4 %all-to-all-start = ((bf16[8,128,384]{2,1,0:T(8,128)(2,1)}), bf16[8,128,384]{2,1,0:T(8,128)(2,1)S(1)}, u32[]{:S(2)}, u32[]{:S(2)}) async-start(bf16[8,128,384]{2,1,0:T(8,128)(2,1)} %broadcast_in_dim.52), calls=%async_computation | async-start | bytes 1572864 | tf_op jit(solution)/shard_map/all_to_all | solution.py:19
  76.2 38.9 %copy-start.9 = (bf16[384,128]{1,0:T(8,128)(2,1)S(1)}, bf16[384,128]{1,0:T(8,128)(2,1)}, u32[]{:S(2)}) copy-start(bf16[384,128]{1,0:T(8,128)(2,1)} %param.20) | copy-start | bytes 294916
  76.2 38.9 %copy-start.10 = (f32[1024]{0:T(1024)S(1)}, f32[1024]{0:T(1024)}, u32[]{:S(2)}) copy-start(f32[1024]{0:T(1024)} %param.21) | copy-start | bytes 12292
  78.9 9.6 %all-to-all-start.1 = ((bf16[4,80,384]{2,1,0:T(8,128)(2,1)}), bf16[4,80,384]{2,1,0:T(8,128)(2,1)S(1)}, u32[]{:S(2)}, u32[]{:S(2)}) async-start(bf16[4,80,384]{2,1,0:T(8,128)(2,1)} %partial_attention.1), calls=%async_computation.1 | async-start | bytes 491520 | tf_op jit(solution)/shard_map/all_to_all | solution.py:19
  142.7 27.5 %all-to-all-start.3 = ((bf16[16,120,128]{2,1,0:T(8,128)(2,1)}), bf16[16,120,128]{2,1,0:T(8,128)(2,1)S(1)}, u32[]{:S(2)}, u32[]{:S(2)}) async-start(bf16[16,120,128]{2,1,0:T(8,128)(2,1)} %pad_maximum_fusion), calls=%async_computation.3 | async-start | bytes 983040 | tf_op jit(solution)/shard_map/all_to_all | solution.py:19
  170.2 0.8 copy-start.1
  176.5 23.2 %copy-start.8 = (f32[384,2]{0,1:T(2,128)S(1)}, f32[384,2]{0,1:T(2,128)}, u32[]{:S(2)}) copy-start(f32[384,2]{0,1:T(2,128)} %param.25) | copy-start | bytes 9220
  195.6 24.7 %all-to-all-start.5 = ((bf16[32,48,128]{2,1,0:T(8,128)(2,1)}), bf16[32,48,128]{2,1,0:T(8,128)(2,1)S(1)}, u32[]{:S(2)}, u32[]{:S(2)}) async-start(bf16[32,48,128]{2,1,0:T(8,128)(2,1)} %bitcast.25), calls=%async_computation.5 | async-start | bytes 786432 | tf_op jit(solution)/shard_map/all_to_all | solution.py:19
  221.5 1.0 copy-start.2
Sparse Core Ops, SparseCore 0:
  31.7 87.9 all-gather.7
  121.8 52.0 all-gather.5

commit v3 on v2

--- a/solution.py
+++ b/solution.py
@@ -12,7 +12,7 @@
 PAD = 16
 BF16 = jnp.bfloat16
 F32 = jnp.float32
-GRIDS = {32: (8, 4), 4: (2, 2), 8: (4, 2)}
+GRIDS = {32: (4, 2, 4), 4: (2, 1, 2), 8: (2, 2, 2)}
 
 
 def exchange(value, axis):
@@ -31,71 +31,74 @@
     return [high, middle, low]
 
 
-def attention_kernel(place, kv, query, cum, out, *, width, query_tile):
-    zone, column = place[0], place[1]
-    head = query.shape[1]
-    count = query.shape[0]
-    keys_each = kv.shape[2]
-    total = count * width
-    queries = jnp.concatenate([query[j] for j in range(count)], axis=1)
-    ones = jnp.ones((PAD, total), BF16)
-    queries = jnp.concatenate([queries, ones], axis=0)
-    tiles = total // query_tile
-
-    def step(block, state, masked):
-        key_t = kv[block, :head, :]
-        value_t = kv[block, head:, :]
-        parts = three_parts(-cum[pl.ds(block, 1), :])
-        filler = jnp.zeros((PAD - 3, keys_each), BF16)
-        key_t = jnp.concatenate([key_t, *parts, filler], axis=0)
-        result = []
-        for i in range(tiles):
-            best, total_weight, acc = state[i]
-            part = queries[:, i * query_tile : (i + 1) * query_tile]
-            score = lax.dot_general(
-                key_t, part, (((0,), (0,)), ((), ())), preferred_element_type=F32
-            )
-            if masked:
-                key_pos = column * width + lax.broadcasted_iota(jnp.int32, score.shape, 0)
-                query_pos = i * query_tile + lax.broadcasted_iota(jnp.int32, score.shape, 1)
-                score = jnp.where(key_pos <= query_pos, score, LOW)
-            new_best = jnp.maximum(best, jnp.max(score, axis=0, keepdims=True))
-            weight = jnp.exp(score - new_best)
-            keep = jnp.exp(best - new_best)
-            total_weight = total_weight * keep + jnp.sum(weight, axis=0, keepdims=True)
-            acc = acc * keep + jnp.dot(
-                value_t, weight.astype(BF16), preferred_element_type=F32
-            )
-            result.append((new_best, total_weight, acc))
-        return tuple(result)
-
-    start = tuple(
-        (
-            jnp.full((1, query_tile), LOW, F32),
-            jnp.zeros((1, query_tile), F32),
-            jnp.zeros((head, query_tile), F32),
+def attention_kernel(place, kv, query, cum, out, key_rows, value_rows):
+    team, own = place[0], place[1]
+    teams, head, width = query.shape
+    count = kv.shape[0]
+
+    for b in range(count):
+        parts = three_parts(-cum[:, b * width : (b + 1) * width])
+        filler = jnp.zeros((LANES - head - 3, width), BF16)
+        key_rows[b] = jnp.concatenate([kv[b, :head, :], *parts, filler], axis=0).T
+        value_rows[b] = jnp.concatenate([kv[b, head:, :], jnp.ones((PAD, width), BF16)], axis=0)
+
+    def step(block, part, state, masked):
+        best, acc = state
+        score = jnp.dot(key_rows[block], part, preferred_element_type=F32)
+        if masked:
+            key_pos = lax.broadcasted_iota(jnp.int32, score.shape, 0)
+            query_pos = lax.broadcasted_iota(jnp.int32, score.shape, 1)
+            score = jnp.where(key_pos <= query_pos, score, LOW)
+        new_best = jnp.maximum(best, jnp.max(score, axis=0, keepdims=True))
+        weight = jnp.exp(score - new_best).astype(BF16)
+        added = jnp.dot(value_rows[block], weight, preferred_element_type=F32)
+        return new_best, acc * jnp.exp(best - new_best) + added
+
+    def fresh():
+        return jnp.full((1, width), LOW, F32), jnp.zeros((head + PAD, width), F32)
+
+    def extended(j):
+        return jnp.concatenate([query[j], jnp.ones((LANES - head, width), BF16)], axis=0)
+
+    def finish(j, states):
+        best = states[0][0]
+        for other, _ in states[1:]:
+            best = jnp.maximum(best, other)
+        acc = sum(a * jnp.exp(m - best) for m, a in states)
+        total = acc[head : head + 1]
+        parts = three_parts(best + jnp.log(total))
+        out[j] = jnp.concatenate(
+            [(acc[:head] / total).astype(BF16), *parts, jnp.zeros((PAD - 3, width), BF16)], axis=0
         )
-        for _ in range(tiles)
-    )
-    state = lax.fori_loop(0, zone, lambda block, s: step(block, s, False), start)
-    state = step(zone, state, True)
-    best = jnp.concatenate([s[0] for s in state], axis=1)
-    weight = jnp.concatenate([s[1] for s in state], axis=1)
-    acc = jnp.concatenate([s[2] for s in state], axis=1)
-    normal = (acc / weight).astype(BF16)
-    parts = three_parts(best + jnp.log(weight))
-    full = jnp.concatenate([normal, *parts, jnp.zeros((PAD - 3, total), BF16)], axis=0)
-    for j in range(count):
-        out[j] = full[:, j * width : (j + 1) * width]
+
+    def full_tile(j, nothing):
+        part = extended(j)
+
+        def pair(i, states):
+            return tuple(step(2 * i + n, part, s, False) for n, s in enumerate(states))
+
+        finish(j, lax.fori_loop(0, count // 2, pair, (fresh(), fresh())))
+        return nothing
+
+    def empty_tile(j, nothing):
+        out[j] = jnp.concatenate(
+            [jnp.zeros((head, width), BF16), jnp.full((PAD, width), LOW, BF16)], axis=0
+        )
+        return nothing
+
+    lax.fori_loop(0, team, empty_tile, 0)
+    part = extended(team)
+    state = lax.fori_loop(0, own, lambda b, s: step(b, part, s, False), fresh())
+    finish(team, [step(own, part, state, True)])
+    lax.fori_loop(team + 1, teams, full_tile, 0)
 
 
 def partial_attention(place, kv, query, cum):
-    count, head, width = query.shape
-    total = count * width
-    tile = 512 if total % 512 == 0 else width
+    teams, head, width = query.shape
+    count = kv.shape[0]
     return pl.pallas_call(
-        lambda *refs: attention_kernel(*refs, width=width, query_tile=tile),
-        out_shape=jax.ShapeDtypeStruct((count, head + PAD, width), BF16),
+        attention_kernel,
+        out_shape=jax.ShapeDtypeStruct((teams, head + PAD, width), BF16),
         in_specs=[
             pl.BlockSpec(memory_space=pltpu.SMEM),
             pl.BlockSpec(memory_space=pltpu.VMEM),
@@ -103,7 +106,11 @@
             pl.BlockSpec(memory_space=pltpu.VMEM),
         ],
         out_specs=pl.BlockSpec(memory_space=pltpu.VMEM),
-        compiler_params=pltpu.CompilerParams(vmem_limit_bytes=40 * 1024 * 1024),
+        scratch_shapes=[
+            pltpu.VMEM((count, width, LANES), BF16),
+            pltpu.VMEM((count, head + PAD, width), BF16),
+        ],
+        compiler_params=pltpu.CompilerParams(vmem_limit_bytes=32 * 1024 * 1024),
         name="partial_attention",
     )(place, kv, query, cum)
 
@@ -113,24 +120,19 @@
 
 
 def pack_kernel(*refs, shapes):
-    sources, target, sem = refs[:-2], refs[-2], refs[-1]
+    sources, target = refs[:-1], refs[-1]
     at = 0
     for source, shape in zip(sources, shapes):
         if len(shape) == 3:
             count, rows, columns = shape
             for e in range(count):
                 for k in range(columns // LANES):
-                    pltpu.make_async_copy(
-                        source.at[e, :, pl.ds(k * LANES, LANES)],
-                        target.at[pl.ds(at, rows), :],
-                        sem,
-                    ).start()
+                    target[at : at + rows, :] = source[e, :, k * LANES : (k + 1) * LANES]
                     at += rows
         else:
             rows = shape[0]
-            pltpu.make_async_copy(source, target.at[pl.ds(at, rows), :], sem).start()
+            target[at : at + rows, :] = source[...]
             at += rows
-    pltpu.make_async_copy(target, target, sem).wait()
 
 
 def packed_shards(*sources):
@@ -139,9 +141,8 @@
     return pl.pallas_call(
         lambda *refs: pack_kernel(*refs, shapes=shapes),
         out_shape=jax.ShapeDtypeStruct((total, LANES), BF16),
-        in_specs=[pl.BlockSpec(memory_space=pltpu.HBM) for _ in sources],
-        out_specs=pl.BlockSpec(memory_space=pltpu.HBM),
-        scratch_shapes=[pltpu.SemaphoreType.DMA],
+        in_specs=[pl.BlockSpec(memory_space=pltpu.VMEM) for _ in sources],
+        out_specs=pl.BlockSpec(memory_space=pltpu.VMEM),
         name="pack_shards",
     )(*sources)
 
@@ -237,22 +238,22 @@
     exp_down,
 ):
     width, head = queries.shape
-    zones, columns = lax.axis_size("z"), lax.axis_size("x")
+    near = ("zl", "x")
+    whole = ("zh", "zl", "x")
+    group = lax.axis_size(near)
     shards = lax.axis_size("tp")
-    blocks = zones * columns
-    zone, column, shard = lax.axis_index("z"), lax.axis_index("x"), lax.axis_index("tp")
+    blocks = lax.axis_size(whole)
+    team, own, shard = lax.axis_index("zh"), lax.axis_index(near), lax.axis_index("tp")
     hidden = sh_gate.shape[1]
     local_experts = exp_gate.shape[0]
     teams = shards // local_experts
 
     scale = head ** (-0.5)
     key_value = jnp.concatenate([keys.T, values.T], axis=0)
-    key_value = copy_to_each(key_value, "z")
+    key_value = copy_to_each(key_value, near)
     query = (queries.T.astype(F32) * scale).astype(BF16)
-    query = lax.all_gather(query, "x", axis=0, tiled=False)
-    cum = lax.dynamic_index_in_dim(
-        log_cum.reshape(zones, columns, width), column, 1, keepdims=False
-    )
+    query = lax.all_gather(query, "zh", axis=0, tiled=False)
+    cum = lax.dynamic_slice_in_dim(log_cum, team * group * width, group * width, 1)
     expert_weights = packed_shards(
         jnp.swapaxes(exp_gate, 1, 2), jnp.swapaxes(exp_up, 1, 2), exp_down.reshape(-1, LANES)
     )
@@ -260,18 +261,19 @@
     shared_weights = packed_shards(sh_gate.T[None], sh_up.T[None])
     shared_weights = lax.all_gather(shared_weights, "tp", axis=0, tiled=False)
 
-    place = jnp.stack([zone, column]).astype(jnp.int32)
+    place = jnp.stack([team, own]).astype(jnp.int32)
     partial = partial_attention(place, key_value, query, cum)
-    partial = exchange(partial, "x").astype(F32)
+    partial = exchange(partial, "zh").astype(F32)
     level = partial[:, head] + partial[:, head + 1] + partial[:, head + 2]
     share = jnp.exp(level - jnp.max(level, axis=0, keepdims=True))
     share = share / jnp.sum(share, axis=0, keepdims=True)
     head_out = jnp.sum(partial[:, :head] * share[:, None], axis=0).astype(BF16)
 
-    all_heads = lax.all_gather(head_out, "tp", axis=0, tiled=True).astype(F32)
-    mean = jnp.sum(all_heads * all_heads, axis=0, keepdims=True) / all_heads.shape[0]
+    all_heads = lax.all_gather(head_out[None], "tp", axis=0, tiled=True).astype(F32)
+    channels = shards * head
+    mean = jnp.sum(all_heads * all_heads, axis=(0, 1), keepdims=True) / channels
     inverse = lax.rsqrt(mean + EPS)
-    mixed = (all_heads * inverse * out_gain[:, None]).astype(BF16)
+    mixed = (all_heads * inverse * out_gain.reshape(shards, head, 1)).astype(BF16).reshape(channels, width)
     attended = lax.dot_general(mixed, w_out, (((0,), (0,)), ((), ())), preferred_element_type=F32)
     updated = (residual.astype(F32) + attended).astype(BF16)
 
@@ -298,7 +300,7 @@
         select, updated, (((0,), (0,)), ((), ())), preferred_element_type=F32
     ).astype(BF16)
     per_block = local_experts * capacity
-    landed = exchange(outgoing.reshape(blocks, per_block, LANES), ("z", "x"))
+    landed = exchange(outgoing.reshape(blocks, per_block, LANES), whole)
     rounds = blocks // teams
     landed = landed.reshape(rounds, teams, local_experts, capacity, LANES)
     landed = jnp.transpose(landed, (2, 1, 0, 3, 4)).reshape(shards, rounds * capacity, LANES)
@@ -314,7 +316,7 @@
     returned = exchange(routed_out, "tp")
     returned = returned.reshape(local_experts, teams, rounds, capacity, LANES)
     returned = jnp.transpose(returned, (2, 1, 0, 3, 4)).reshape(blocks, per_block, LANES)
-    answers = exchange(returned, ("z", "x")).reshape(slots, LANES)
+    answers = exchange(returned, whole).reshape(slots, LANES)
     share_hidden = feed_forward(
         jnp.zeros((1,), jnp.int32),
         rows,
@@ -336,9 +338,8 @@
 
 def solution(mesh):
     blocks, shards = mesh.devices.shape
-    zones, columns = GRIDS[blocks]
-    grid = Mesh(mesh.devices.reshape(zones, columns, shards), ("z", "x", "tp"))
-    sp = ("z", "x")
+    grid = Mesh(mesh.devices.reshape(*GRIDS[blocks], shards), ("zh", "zl", "x", "tp"))
+    sp = ("zh", "zl", "x")
     in_specs = (
         P(sp, "tp"),
         P(sp, "tp"),

time: 231 us -> 209 us (0.905)
  Pallas kernels: 47 us -> 26.8 us
  blocking collectives: 96.4 us -> 108 us
  waiting for transfers between devices: 37.4 us -> 29.2 us
  starting transfers between devices: 25.5 us -> 20.6 us
    pallas_call x2, Pallas kernels: 34 us -> 3.87 us  [packed_shards(): pl.pallas_call(lambda *refs: pack_kernel(*refs, shapes=shapes), out_shape...]
    all_gather x2, blocking collectives: 37.1 us -> 51.8 us  [the longest x1 28.4 us: per_device(): lax.all_gather(head_out[None], 'tp', axis=0, tiled=True).astype(F32)]
    pallas_call x1, Pallas kernels: 2.75 us -> 12.7 us  [partial_attention(): pl.pallas_call(attention_kernel, out_shape=jax.ShapeDtypeStruct((teams, h...]
    all_to_all x4, waiting for transfers between devices: 37.4 us -> 29.2 us  [exchange(): return lax.all_to_all(value, axis, split_axis=0, concat_axis=0, tiled=True)]
    all_to_all x4, starting transfers between devices: 25.4 us -> 20.5 us  [exchange(): return lax.all_to_all(value, axis, split_axis=0, concat_axis=0, tiled=True)]
    all_to_all x2, blocking collectives: 43.5 us -> 40.6 us  [exchange(): return lax.all_to_all(value, axis, split_axis=0, concat_axis=0, tiled=True)]
  transfers between devices with their start and end apart: 6 -> 6, of which waited for: 3 -> 2; matrix products, arithmetic and copies ran while one was open for 3% -> 3% of each run, Pallas kernels for 10% -> 12%
where the time goes in v3:
time: 209 us; the launch traced here: 208 us
  blocking collectives  108 us (52%)
  waiting for transfers between devices  29.2 us (14%)
  Pallas kernels  26.8 us (13%)
  starting transfers between devices  20.6 us (10%)
  between operations  13.7 us (7%)
  matrix products  4.58 us (2%)
  local copies, waits for them, and re-layouts  3.44 us (2%)
    all_to_all x2, blocking collectives, exchange(): return lax.all_to_all(value, axis, split_axis=0, concat_axis=0, tiled=True)  40.6 us
    all_to_all x4, waiting for transfers between devices, exchange(): return lax.all_to_all(value, axis, split_axis=0, concat_axis=0, tiled=True)  29.2 us
    all_gather x1, blocking collectives, per_device(): lax.all_gather(head_out[None], 'tp', axis=0, tiled=True).astype(F32)  28.4 us
    all_gather x1, blocking collectives, per_device(): query = lax.all_gather(query, 'zh', axis=0, tiled=False)  23.4 us
    all_to_all x4, starting transfers between devices, exchange(): return lax.all_to_all(value, axis, split_axis=0, concat_axis=0, tiled=True)  20.5 us
    all_gather x1, blocking collectives, per_device(): share_hidden = lax.all_gather(share_hidden, 'tp', axis=0, tiled=True)  15.8 us
    pallas_call x1, Pallas kernels, partial_attention(): pl.pallas_call(attention_kernel, out_shape=jax.ShapeDtypeStruct((teams, h...  12.7 us
    pallas_call x2, Pallas kernels, feed_forward(): pl.pallas_call(lambda *refs: feed_kernel(*refs, first=first, count=count,...  10.3 us
  transfers between devices with their start and end apart: 6, of which 2 were waited for; matrix products, arithmetic and copies ran while one was open for 3% of the time, Pallas kernels for 12%

profile of v3, /device:TPU:1, one launch (start us, length us, event | category | flops | bytes accessed | tf_op | source)
XLA Modules:
  0.0 208.0 jit_solution(2717975654367492965)
XLA Ops:
  6.5 0.0 copy-start
  6.5 0.0 copy-start.6
  6.5 0.0 copy-start.5
  6.5 0.0 all-gather.9.cloned.1.call-start
  6.5 2.1 %pack_shards.3 = bf16[3072,128]{1,0:T(8,128)(2,1)} custom-call(bf16[2,32,2048]{2,1,0:T(8,128)(2,1)} %bitcast.63, bf16[2,32,2048]{2,1,0:T(8,128)(2,1)} %bitcast.64, bf16[1024,128]{1,0:T(8,128)(2,1)} %bitcast.65), custom_call_target="tpu_custom_call" | custom-call | tf_op jit(solution)/shard_map/pack_shards/pallas_call | solution.py:141
  8.7 0.0 copy-start.4
  8.7 0.0 all-gather.9.cloned.1.call-update
  8.7 0.0 all-gather.7.cloned.1.call-start
  8.8 1.7 pack_shards.2
  10.5 0.0 all-gather.7.cloned.1.call-update
  10.5 0.0 copy-done.6
  10.5 0.0 copy-done.5
  10.5 0.0 copy-start.8
  10.5 0.0 copy-start.7
  10.6 1.0 broadcast_in_dim.52
  11.6 6.6 %all-to-all-start = ((bf16[8,128,384]{2,1,0:T(8,128)(2,1)}), bf16[8,128,384]{2,1,0:T(8,128)(2,1)S(1)}, u32[]{:S(2)}, u32[]{:S(2)}) async-start(bf16[8,128,384]{2,1,0:T(8,128)(2,1)} %broadcast_in_dim.52), calls=%async_computation | async-start | bytes 1572864 | tf_op jit(solution)/shard_map/all_to_all | solution.py:19
  18.2 0.0 copy-done.4
  18.2 23.4 %all-gather = bf16[256,384]{1,0:T(8,128)(2,1)S(1)} all-gather(bf16[64,384]{1,0:T(8,128)(2,1)S(1)} %fusion.22), channel_id=2, replica_groups=mesh['zh'=4,'zl'=2,'x'=4,'tp'=16] {'zh'}, dimensions={0}, use_global_device_ids=true | all-gather | bytes 245760 | tf_op jit(solution)/shard_map/all_gather | solution.py:255
  41.7 0.1 pad_add_fusion.place
  41.7 0.7 constant_dynamic-slice_fusion.cum
  42.4 0.0 all-to-all-done.kv
  42.4 12.7 %partial_attention.1 = bf16[4,80,384]{2,1,0:T(8,128)(2,1)} custom-call(s32[2]{0:T(128)S(1)} %pad_add_fusion.place, bf16[8,128,384]{2,1,0:T(8,128)(2,1)S(1)} %all-to-all-done.kv, bf16[4,64,384]{2,1,0:T(8,128)(2,1)S(1)} %bitcast.52, f32[1,3072]{1,0:T(1,128)S(1)} %constant_dynamic-slice_fusion.cum), custom_call_target="tpu_custom_call" | custom-call | tf_op jit(solution)/shard_map/partial_attention/pallas_call | solution.py:99
  55.1 3.4 %all-to-all-start.1 = ((bf16[4,80,384]{2,1,0:T(8,128)(2,1)}), bf16[4,80,384]{2,1,0:T(8,128)(2,1)S(1)}, u32[]{:S(2)}, u32[]{:S(2)}) async-start(bf16[4,80,384]{2,1,0:T(8,128)(2,1)} %partial_attention.1), calls=%async_computation.1 | async-start | bytes 491520 | tf_op jit(solution)/shard_map/all_to_all | solution.py:19
  58.5 0.0 copy-done.8
  58.5 0.1 mul.63
  58.6 0.0 copy-done.7
  58.6 0.2 select_reduce_fusion.1
  58.8 0.0 copy-start.3
  58.9 8.1 %all-to-all-done.1 = bf16[4,80,384]{2,1,0:T(8,128)(2,1)S(1)} async-done(((bf16[4,80,384]{2,1,0:T(8,128)(2,1)}), bf16[4,80,384]{2,1,0:T(8,128)(2,1)S(1)}, u32[]{:S(2)}, u32[]{:S(2)}) %all-to-all-start.1) | async-done | bytes 245792 | tf_op jit(solution)/shard_map/all_to_all | solution.py:19
  67.2 28.4 %all-gather.1 = bf16[1024,384]{1,0:T(8,128)(2,1)S(1)} all-gather(bf16[64,384]{1,0:T(8,128)(2,1)S(1)} %fusion.19), channel_id=3, replica_groups=mesh['zh'=4,'zl'=2,'x'=4,'tp'=16] {'tp'}, dimensions={0}, use_global_device_ids=true | all-gather | bytes 835584 | tf_op jit(solution)/shard_map/all_gather | solution.py:272
  95.5 0.2 fusion.3
  95.8 0.2 fusion.5
  96.0 0.0 copy-done
  96.0 0.0 copy-done.3
  96.0 0.4 fusion.16
  96.4 0.9 convolution_convert_fusion
  97.3 22.4 %all_to_all.30 = bf16[32,48,128]{2,1,0:T(8,128)(2,1)S(1)} all-to-all(bf16[32,48,128]{2,1,0:T(8,128)(2,1)S(1)} %bitcast.62), channel_id=1, replica_groups=mesh['zh'=4,'zl'=2,'x'=4,'tp'=16] {'zh','zl','x'}, dimensions={0} | all-to-all | bytes 786432 | tf_op jit(solution)/shard_map/all_to_all | solution.py:19
  119.7 0.8 pad_maximum_fusion
  120.5 6.4 %all-to-all-start.3 = ((bf16[16,120,128]{2,1,0:T(8,128)(2,1)}), bf16[16,120,128]{2,1,0:T(8,128)(2,1)S(1)}, u32[]{:S(2)}, u32[]{:S(2)}) async-start(bf16[16,120,128]{2,1,0:T(8,128)(2,1)} %pad_maximum_fusion), calls=%async_computation.3 | async-start | bytes 983040 | tf_op jit(solution)/shard_map/all_to_all | solution.py:19
  126.9 21.1 %all-to-all-done.3.refs_1_ = bf16[16,120,128]{2,1,0:T(8,128)(2,1)S(1)} async-done(((bf16[16,120,128]{2,1,0:T(8,128)(2,1)}), bf16[16,120,128]{2,1,0:T(8,128)(2,1)S(1)}, u32[]{:S(2)}, u32[]{:S(2)}) %all-to-all-start.3) | async-done | bytes 491552 | tf_op jit(solution)/shard_map/all_to_all | solution.py:19
  148.0 0.0 copy-start.1
  148.0 0.0 all-gather.9.cloned.1.call-done
  148.0 0.8 copy-done.1
  148.8 5.5 %shard_map.155 = bf16[16,96,128]{2,1,0:T(8,128)(2,1)} custom-call(s32[1]{0:T(128)} %bitcast.20.refs_0_, bf16[16,120,128]{2,1,0:T(8,128)(2,1)} %copy-done.1, f32[16,1,128]{2,1,0:T(1,128)} %bitcast.70, bf16[16,3072,128]{2,1,0:T(8,128)(2,1)} %bitcast.53), custom_call_target="tpu_custom_call" | custom-call | tf_op jit(solution)/shard_map/pallas_call | solution.py:202
  154.3 0.0 copy-start.9
  154.3 18.2 %all_to_all.31 = bf16[16,96,128]{2,1,0:T(8,128)(2,1)S(1)} all-to-all(bf16[16,96,128]{2,1,0:T(8,128)(2,1)} %shard_map.155), channel_id=1, replica_groups=mesh['zh'=4,'zl'=2,'x'=4,'tp'=16] {'tp'}, dimensions={0} | all-to-all | bytes 786432 | tf_op jit(solution)/shard_map/all_to_all | solution.py:19
  172.5 0.8 copy.20
  173.3 4.1 %all-to-all-start.5 = ((bf16[32,48,128]{2,1,0:T(8,128)(2,1)}), bf16[32,48,128]{2,1,0:T(8,128)(2,1)S(1)}, u32[]{:S(2)}, u32[]{:S(2)}) async-start(bf16[32,48,128]{2,1,0:T(8,128)(2,1)} %bitcast.27), calls=%async_computation.5 | async-start | bytes 786432 | tf_op jit(solution)/shard_map/all_to_all | solution.py:19
  177.4 0.0 copy-done.9
  177.5 0.0 all-gather.7.cloned.1.call-done
  177.5 4.7 %shard_map.154 = bf16[24,512]{1,0:T(8,128)(2,1)} custom-call(s32[1]{0:T(128)} %constant.51.clone.1.refs_0_, bf16[16,120,128]{2,1,0:T(8,128)(2,1)} %copy-done.1, f32[16,1,128]{2,1,0:T(1,128)} %bitcast.71, bf16[16,1024,128]{2,1,0:T(8,128)(2,1)} %bitcast.54), custom_call_target="tpu_custom_call" | custom-call | tf_op jit(solution)/shard_map/pallas_call | solution.py:202
  182.2 15.8 %all_gather.29 = bf16[384,512]{1,0:T(8,128)(2,1)S(1)} all-gather(bf16[24,512]{1,0:T(8,128)(2,1)} %shard_map.154), channel_id=1, replica_groups=mesh['zh'=4,'zl'=2,'x'=4,'tp'=16] {'tp'}, dimensions={0}, use_global_device_ids=true | all-gather | bytes 417792 | tf_op jit(solution)/shard_map/all_gather | solution.py:331
  198.0 0.0 all-to-all-done.5
  198.0 1.2 fusion.11
  199.2 0.0 copy-start.2
  199.2 1.0 fusion.15
  200.2 0.0 copy-done.2
  200.2 0.9 fusion.17
  (15 shorter events, 0.3 us)
Async XLA Ops:
  6.5 89.5 %copy-start = (bf16[1024,128]{1,0:T(8,128)(2,1)S(1)}, bf16[1024,128]{1,0:T(8,128)(2,1)}, u32[]{:S(2)}) copy-start(bf16[1024,128]{1,0:T(8,128)(2,1)} %param.22) | copy-start | bytes 786436
  6.5 4.0 %copy-start.6 = (bf16[384,64]{0,1:T(8,128)(2,1)S(1)}, bf16[384,64]{0,1:T(8,128)(2,1)}, u32[]{:S(2)}) copy-start(bf16[384,64]{0,1:T(8,128)(2,1)} %param.17) | copy-start | bytes 147460
  6.5 4.0 %copy-start.5 = (bf16[384,64]{0,1:T(8,128)(2,1)S(1)}, bf16[384,64]{0,1:T(8,128)(2,1)}, u32[]{:S(2)}) copy-start(bf16[384,64]{0,1:T(8,128)(2,1)} %param.18) | copy-start | bytes 147460
  6.5 141.4 %all-gather.9.cloned.1.call-start = ((), (), s32[]{:S(2)}) async-start(), calls=%async_computation.7 | async-start | bytes 13369344 | tf_op jit(solution)/shard_map/all_gather | solution.py:260
  8.7 9.5 %copy-start.4 = (bf16[384,64]{0,1:T(8,128)(2,1)S(1)}, bf16[384,64]{0,1:T(8,128)(2,1)}, u32[]{:S(2)}) copy-start(bf16[384,64]{0,1:T(8,128)(2,1)} %param.16) | copy-start | bytes 147460
  8.7 168.8 %all-gather.7.cloned.1.call-start = ((), (), s32[]{:S(2)}) async-start(), calls=%async_computation.6 | async-start | bytes 4456448 | tf_op jit(solution)/shard_map/all_gather | solution.py:262
  10.5 48.0 %copy-start.8 = (f32[1024]{0:T(1024)S(1)}, f32[1024]{0:T(1024)}, u32[]{:S(2)}) copy-start(f32[1024]{0:T(1024)} %param.21) | copy-start | bytes 12292
  10.5 48.0 %copy-start.7 = (s32[384,2]{0,1:T(2,128)S(1)}, s32[384,2]{0,1:T(2,128)}, u32[]{:S(2)}) copy-start(s32[384,2]{0,1:T(2,128)} %param.24) | copy-start | bytes 9220
  11.6 30.9 %all-to-all-start = ((bf16[8,128,384]{2,1,0:T(8,128)(2,1)}), bf16[8,128,384]{2,1,0:T(8,128)(2,1)S(1)}, u32[]{:S(2)}, u32[]{:S(2)}) async-start(bf16[8,128,384]{2,1,0:T(8,128)(2,1)} %broadcast_in_dim.52), calls=%async_computation | async-start | bytes 1572864 | tf_op jit(solution)/shard_map/all_to_all | solution.py:19
  55.1 11.9 %all-to-all-start.1 = ((bf16[4,80,384]{2,1,0:T(8,128)(2,1)}), bf16[4,80,384]{2,1,0:T(8,128)(2,1)S(1)}, u32[]{:S(2)}, u32[]{:S(2)}) async-start(bf16[4,80,384]{2,1,0:T(8,128)(2,1)} %partial_attention.1), calls=%async_computation.1 | async-start | bytes 491520 | tf_op jit(solution)/shard_map/all_to_all | solution.py:19
  58.8 37.2 %copy-start.3 = (bf16[384,128]{1,0:T(8,128)(2,1)S(1)}, bf16[384,128]{1,0:T(8,128)(2,1)}, u32[]{:S(2)}) copy-start(bf16[384,128]{1,0:T(8,128)(2,1)} %param.20) | copy-start | bytes 294916
  120.5 27.5 %all-to-all-start.3 = ((bf16[16,120,128]{2,1,0:T(8,128)(2,1)}), bf16[16,120,128]{2,1,0:T(8,128)(2,1)S(1)}, u32[]{:S(2)}, u32[]{:S(2)}) async-start(bf16[16,120,128]{2,1,0:T(8,128)(2,1)} %pad_maximum_fusion), calls=%async_computation.3 | async-start | bytes 983040 | tf_op jit(solution)/shard_map/all_to_all | solution.py:19
  148.0 0.8 copy-start.1
  154.3 23.1 %copy-start.9 = (f32[384,2]{0,1:T(2,128)S(1)}, f32[384,2]{0,1:T(2,128)}, u32[]{:S(2)}) copy-start(f32[384,2]{0,1:T(2,128)} %param.25) | copy-start | bytes 9220
  173.3 24.7 %all-to-all-start.5 = ((bf16[32,48,128]{2,1,0:T(8,128)(2,1)}), bf16[32,48,128]{2,1,0:T(8,128)(2,1)S(1)}, u32[]{:S(2)}, u32[]{:S(2)}) async-start(bf16[32,48,128]{2,1,0:T(8,128)(2,1)} %bitcast.27), calls=%async_computation.5 | async-start | bytes 786432 | tf_op jit(solution)/shard_map/all_to_all | solution.py:19
  199.2 1.0 copy-start.2
Sparse Core Ops, SparseCore 0:
  9.5 87.9 all-gather.8
  99.6 52.0 all-gather.6

commit v4 on v3

--- a/solution.py
+++ b/solution.py
@@ -58,7 +58,8 @@
         return jnp.full((1, width), LOW, F32), jnp.zeros((head + PAD, width), F32)
 
     def extended(j):
-        return jnp.concatenate([query[j], jnp.ones((LANES - head, width), BF16)], axis=0)
+        turn = lax.rem(team - j + teams, teams)
+        return jnp.concatenate([query[turn], jnp.ones((LANES - head, width), BF16)], axis=0)
 
     def finish(j, states):
         best = states[0][0]
@@ -147,8 +148,7 @@
     )(*sources)
 
 
-def feed_kernel(which, rows, gain, weights, out, gate, upward, *rest, first, count, experts):
-    down, sems = rest if len(rest) == 2 else (None, rest[0])
+def feed_kernel(which, rows, gain, weights, out, gate, upward, down, sems, *, experts):
     shards, hidden = gate.shape[0], gate.shape[1]
     inner = shards * hidden
     features = shards * LANES
@@ -164,12 +164,12 @@
                 sems.at[n],
             ).start()
     base = pl.multiple_of(bases[2], hidden)
-    for t in range(shards if down is not None else 0):
+    for t in range(shards):
         pltpu.make_async_copy(
             weights.at[t, pl.ds(base, inner), :], down.at[:, pl.ds(t * LANES, LANES)], sems.at[2]
         ).start()
 
-    floats = [rows[t, first : first + count, :].astype(F32) for t in range(shards)]
+    floats = [rows[t].astype(F32) for t in range(shards)]
     squares = sum(f * f for f in floats)
     mean = jnp.sum(squares, axis=1, keepdims=True) / features
     inverse = lax.rsqrt(mean + EPS)
@@ -184,24 +184,19 @@
         normed, upward[...].reshape(inner, features), across, preferred_element_type=F32
     )
     inside = gated_hidden(first_half, second_half)
-    if down is None:
-        out[...] = inside
-        return
     pltpu.make_async_copy(down, down, sems.at[2]).wait()
     for t in range(shards):
         part = jnp.dot(inside, down[:, t * LANES : (t + 1) * LANES], preferred_element_type=F32)
         out[t] = part.astype(BF16)
 
 
-def feed_forward(which, rows, gain, weights, hidden, first, count, experts, whole=True):
+def feed_forward(which, rows, gain, weights, hidden, experts):
     shards = rows.shape[0]
     features = shards * LANES
     inner = shards * hidden
-    shape = (shards, count, LANES) if whole else (count, inner)
-    down = [pltpu.VMEM((inner, features), BF16)] if whole else []
     return pl.pallas_call(
-        lambda *refs: feed_kernel(*refs, first=first, count=count, experts=experts),
-        out_shape=jax.ShapeDtypeStruct(shape, BF16),
+        lambda *refs: feed_kernel(*refs, experts=experts),
+        out_shape=jax.ShapeDtypeStruct(rows.shape, BF16),
         in_specs=[
             pl.BlockSpec(memory_space=pltpu.SMEM),
             pl.BlockSpec(memory_space=pltpu.VMEM),
@@ -212,11 +207,36 @@
         scratch_shapes=[
             pltpu.VMEM((shards, hidden, features), BF16),
             pltpu.VMEM((shards, hidden, features), BF16),
-            *down,
+            pltpu.VMEM((inner, features), BF16),
             pltpu.SemaphoreType.DMA((3,)),
         ],
-        compiler_params=pltpu.CompilerParams(vmem_limit_bytes=(54 if whole else 61) * 1024 * 1024),
+        compiler_params=pltpu.CompilerParams(vmem_limit_bytes=52 * 1024 * 1024),
+        name="routed_feed",
     )(which, rows, gain, weights)
+
+
+def shared_kernel(rows, gain, gate, upward, out):
+    shards = rows.shape[0]
+    floats = [rows[t].astype(F32) for t in range(shards)]
+    squares = sum(f * f for f in floats)
+    inverse = lax.rsqrt(jnp.sum(squares, axis=1, keepdims=True) / (shards * LANES) + EPS)
+    normed = jnp.concatenate([(f * inverse * gain[t]).astype(BF16) for t, f in enumerate(floats)], axis=1)
+    across = (((1,), (1,)), ((), ()))
+    out[...] = gated_hidden(
+        lax.dot_general(gate[...], normed, across, preferred_element_type=F32),
+        lax.dot_general(upward[...], normed, across, preferred_element_type=F32),
+    )
+
+
+def shared_feed(rows, gain, gate, upward):
+    return pl.pallas_call(
+        shared_kernel,
+        out_shape=jax.ShapeDtypeStruct((gate.shape[0], rows.shape[1]), BF16),
+        in_specs=[pl.BlockSpec(memory_space=pltpu.VMEM) for _ in range(4)],
+        out_specs=pl.BlockSpec(memory_space=pltpu.VMEM),
+        compiler_params=pltpu.CompilerParams(vmem_limit_bytes=24 * 1024 * 1024),
+        name="shared_feed",
+    )(rows, gain, gate, upward)
 
 
 def per_device(
@@ -246,20 +266,23 @@
     team, own, shard = lax.axis_index("zh"), lax.axis_index(near), lax.axis_index("tp")
     hidden = sh_gate.shape[1]
     local_experts = exp_gate.shape[0]
-    teams = shards // local_experts
+    owners = shards // local_experts
 
     scale = head ** (-0.5)
     key_value = jnp.concatenate([keys.T, values.T], axis=0)
     key_value = copy_to_each(key_value, near)
     query = (queries.T.astype(F32) * scale).astype(BF16)
-    query = lax.all_gather(query, "zh", axis=0, tiled=False)
+    teams = lax.axis_size("zh")
+    moved = [
+        lax.ppermute(query, "zh", [(i, (i + n) % teams) for i in range(teams)])
+        for n in range(1, teams)
+    ]
+    query = jnp.stack([query, *moved])
     cum = lax.dynamic_slice_in_dim(log_cum, team * group * width, group * width, 1)
     expert_weights = packed_shards(
         jnp.swapaxes(exp_gate, 1, 2), jnp.swapaxes(exp_up, 1, 2), exp_down.reshape(-1, LANES)
     )
     expert_weights = lax.all_gather(expert_weights, "tp", axis=0, tiled=False)
-    shared_weights = packed_shards(sh_gate.T[None], sh_up.T[None])
-    shared_weights = lax.all_gather(shared_weights, "tp", axis=0, tiled=False)
 
     place = jnp.stack([team, own]).astype(jnp.int32)
     partial = partial_attention(place, key_value, query, cum)
@@ -276,6 +299,7 @@
     mixed = (all_heads * inverse * out_gain.reshape(shards, head, 1)).astype(BF16).reshape(channels, width)
     attended = lax.dot_general(mixed, w_out, (((0,), (0,)), ((), ())), preferred_element_type=F32)
     updated = (residual.astype(F32) + attended).astype(BF16)
+    all_rows = lax.all_gather(updated[None], "tp", axis=0, tiled=True)
 
     top = routes.shape[1]
     experts = local_experts * blocks
@@ -301,35 +325,22 @@
     ).astype(BF16)
     per_block = local_experts * capacity
     landed = exchange(outgoing.reshape(blocks, per_block, LANES), whole)
-    rounds = blocks // teams
-    landed = landed.reshape(rounds, teams, local_experts, capacity, LANES)
+    rounds = blocks // owners
+    landed = landed.reshape(rounds, owners, local_experts, capacity, LANES)
     landed = jnp.transpose(landed, (2, 1, 0, 3, 4)).reshape(shards, rounds * capacity, LANES)
-    routed_rows = rounds * capacity
-    own_rows = width // shards
-    mixed_rows = jnp.concatenate([landed, updated.reshape(shards, own_rows, LANES)], axis=1)
-    rows = exchange(mixed_rows, "tp")
+    rows = exchange(landed, "tp")
     gain = ffn_gain.reshape(shards, 1, LANES)
-    mine = (shard // teams).astype(jnp.int32)[None]
-    routed_out = feed_forward(
-        mine, rows, gain, expert_weights, hidden, 0, routed_rows, local_experts
-    )
+    mine = (shard // owners).astype(jnp.int32)[None]
+    routed_out = feed_forward(mine, rows, gain, expert_weights, hidden, local_experts)
     returned = exchange(routed_out, "tp")
-    returned = returned.reshape(local_experts, teams, rounds, capacity, LANES)
+    returned = returned.reshape(local_experts, owners, rounds, capacity, LANES)
     returned = jnp.transpose(returned, (2, 1, 0, 3, 4)).reshape(blocks, per_block, LANES)
     answers = exchange(returned, whole).reshape(slots, LANES)
-    share_hidden = feed_forward(
-        jnp.zeros((1,), jnp.int32),
-        rows,
-        gain,
-        shared_weights,
-        hidden,
-        routed_rows,
-        own_rows,
-        1,
-        whole=False,
-    )
+    share_hidden = shared_feed(all_rows, gain, sh_gate.T, sh_up.T)
     share_hidden = lax.all_gather(share_hidden, "tp", axis=0, tiled=True)
-    shared = jnp.dot(share_hidden, sh_down, preferred_element_type=F32)
+    shared = lax.dot_general(
+        share_hidden, sh_down, (((0,), (0,)), ((), ())), preferred_element_type=F32
+    )
     routed = jnp.dot(weight_high, answers, preferred_element_type=F32) + jnp.dot(
         weight_low, answers, preferred_element_type=F32
     )

time: 209 us -> 195 us (0.933)
  blocking collectives: 108 us -> 85.8 us
  starting transfers between devices: 20.6 us -> 37.6 us
  Pallas kernels: 26.8 us -> 19.8 us
  waiting for transfers between devices: 29.2 us -> 25.6 us
    all_gather x1 -> x0, blocking collectives: 23.4 us -> none  [per_device(): query = lax.all_gather(query, 'zh', axis=0, tiled=False)]
    ppermute x0 -> x3, starting transfers between devices: none -> 17.1 us  [per_device(): lax.ppermute(query, 'zh', [(i, (i + n) % teams) for i in range(teams)])]
    all_to_all x4, waiting for transfers between devices: 29.2 us -> 23 us  [exchange(): return lax.all_to_all(value, axis, split_axis=0, concat_axis=0, tiled=True)]
    pallas_call x2, Pallas kernels: 10.3 us -> 5 us  [the longest x1 3.78 us: feed_forward(): pl.pallas_call(lambda *refs: feed_kernel(*refs, experts=experts), out_sha...]
    ppermute x0 -> x3, waiting for transfers between devices: none -> 2.51 us  [per_device(): lax.ppermute(query, 'zh', [(i, (i + n) % teams) for i in range(teams)])]
    all_to_all x2, blocking collectives: 40.6 us -> 42.7 us  [exchange(): return lax.all_to_all(value, axis, split_axis=0, concat_axis=0, tiled=True)]
  transfers between devices with their start and end apart: 6 -> 9, of which waited for: 2 -> 4; matrix products, arithmetic and copies ran while one was open for 3% -> 4% of each run, Pallas kernels for 12% -> 9%
where the time goes in v4:
time: 195 us; the launch traced here: 194 us
  blocking collectives  85.8 us (44%)
  starting transfers between devices  37.6 us (19%)
  waiting for transfers between devices  25.6 us (13%)
  Pallas kernels  19.8 us (10%)
  between operations  13.8 us (7%)
  matrix products  6.17 us (3%)
  local copies, waits for them, and re-layouts  4.85 us (2%)
    all_to_all x2, blocking collectives, exchange(): return lax.all_to_all(value, axis, split_axis=0, concat_axis=0, tiled=True)  42.7 us
    all_gather x1, blocking collectives, per_device(): lax.all_gather(head_out[None], 'tp', axis=0, tiled=True).astype(F32)  27.6 us
    all_to_all x4, waiting for transfers between devices, exchange(): return lax.all_to_all(value, axis, split_axis=0, concat_axis=0, tiled=True)  23 us
    all_to_all x4, starting transfers between devices, exchange(): return lax.all_to_all(value, axis, split_axis=0, concat_axis=0, tiled=True)  20.4 us
    ppermute x3, starting transfers between devices, per_device(): lax.ppermute(query, 'zh', [(i, (i + n) % teams) for i in range(teams)])  17.1 us
    all_gather x1, blocking collectives, per_device(): share_hidden = lax.all_gather(share_hidden, 'tp', axis=0, tiled=True)  15.5 us
    pallas_call x1, Pallas kernels, partial_attention(): pl.pallas_call(attention_kernel, out_shape=jax.ShapeDtypeStruct((teams, h...  12.6 us
  transfers between devices with their start and end apart: 9, of which 4 were waited for; matrix products, arithmetic and copies ran while one was open for 4% of the time, Pallas kernels for 9%

profile of v4, /device:TPU:1, one launch (start us, length us, event | category | flops | bytes accessed | tf_op | source)
XLA Modules:
  0.0 194.4 jit_solution(1042594417084365075)
XLA Ops:
  6.5 0.0 copy-start
  6.5 0.0 all-gather.8.cloned.1.call-start
  6.5 0.0 copy-start.10
  6.6 2.1 %pack_shards.1 = bf16[3072,128]{1,0:T(8,128)(2,1)} custom-call(bf16[2,32,2048]{2,1,0:T(8,128)(2,1)} %bitcast.64, bf16[2,32,2048]{2,1,0:T(8,128)(2,1)} %bitcast.65, bf16[1024,128]{1,0:T(8,128)(2,1)} %bitcast.66), custom_call_target="tpu_custom_call" | custom-call | tf_op jit(solution)/shard_map/pack_shards/pallas_call | solution.py:142
  8.7 0.0 all-gather.8.cloned.1.call-update
  8.7 0.0 copy-done.9
  8.7 0.0 copy-done.8
  8.8 0.0 copy-start.12
  8.8 0.0 copy-start.11
  8.8 1.0 broadcast_in_dim.49
  9.8 6.6 %all-to-all-start = ((bf16[8,128,384]{2,1,0:T(8,128)(2,1)}), bf16[8,128,384]{2,1,0:T(8,128)(2,1)S(1)}, u32[]{:S(2)}, u32[]{:S(2)}) async-start(bf16[8,128,384]{2,1,0:T(8,128)(2,1)} %broadcast_in_dim.49), calls=%async_computation | async-start | bytes 1572864 | tf_op jit(solution)/shard_map/all_to_all | solution.py:19
  16.4 0.0 copy-done.10
  16.4 5.8 %collective-permute-start = (bf16[64,384]{1,0:T(8,128)(2,1)S(1)}, bf16[64,384]{1,0:T(8,128)(2,1)S(1)}, u32[]{:S(2)}, u32[]{:S(2)}) collective-permute-start(bf16[64,384]{1,0:T(8,128)(2,1)S(1)} %get-tuple-element.16), channel_id=1, source_target_pairs={{0,128},{128,256},{256,384},{384,0},{1,129},{129,257},{257,385},{3... | collective-permute-start | bytes 147464 | tf_op jit(solution)/shard_map/ppermute | solution.py:277
  22.3 7.9 %collective-permute-start.1 = (bf16[64,384]{1,0:T(8,128)(2,1)S(1)}, bf16[64,384]{1,0:T(8,128)(2,1)S(1)}, u32[]{:S(2)}, u32[]{:S(2)}) collective-permute-start(bf16[64,384]{1,0:T(8,128)(2,1)S(1)} %get-tuple-element.16), channel_id=1, source_target_pairs={{0,256},{128,384},{256,0},{384,128},{1,257},{129,385},{257,1},{385... | collective-permute-start | bytes 147464 | tf_op jit(solution)/shard_map/ppermute | solution.py:277
  30.2 3.4 %collective-permute-start.2 = (bf16[64,384]{1,0:T(8,128)(2,1)S(1)}, bf16[64,384]{1,0:T(8,128)(2,1)S(1)}, u32[]{:S(2)}, u32[]{:S(2)}) collective-permute-start(bf16[64,384]{1,0:T(8,128)(2,1)S(1)} %get-tuple-element.16), channel_id=1, source_target_pairs={{0,384},{128,0},{256,128},{384,256},{1,385},{129,1},{257,129},{385... | collective-permute-start | bytes 147464 | tf_op jit(solution)/shard_map/ppermute | solution.py:277
  33.6 0.7 constant_dynamic-slice_fusion.cum
  34.3 0.1 pad_add_fusion.place
  34.4 0.5 collective-permute-done
  34.9 2.0 %collective-permute-done.1 = bf16[64,384]{1,0:T(8,128)(2,1)S(1)} collective-permute-done((bf16[64,384]{1,0:T(8,128)(2,1)S(1)}, bf16[64,384]{1,0:T(8,128)(2,1)S(1)}, u32[]{:S(2)}, u32[]{:S(2)}) %collective-permute-start.1) | collective-permute-done | bytes 49184 | tf_op jit(solution)/shard_map/ppermute | solution.py:277
  36.9 0.0 collective-permute-done.2
  36.9 0.0 all-to-all-done.kv
  37.0 12.6 %partial_attention.1 = bf16[4,80,384]{2,1,0:T(8,128)(2,1)} custom-call(s32[2]{0:T(128)S(1)} %pad_add_fusion.place, bf16[8,128,384]{2,1,0:T(8,128)(2,1)S(1)} %all-to-all-done.kv, bf16[4,64,384]{2,1,0:T(8,128)(2,1)S(1)} %pad_maximum_fusion.query, f32[1,3072]{1,0:T(1,128)S(1)} %constant_dynamic-slice_fusion.cum), custom_call_target="tpu_custom_call" | custom-call | tf_op jit(solution)/shard_map/partial_attention/pallas_call | solution.py:100
  49.6 3.4 %all-to-all-start.1 = ((bf16[4,80,384]{2,1,0:T(8,128)(2,1)}), bf16[4,80,384]{2,1,0:T(8,128)(2,1)S(1)}, u32[]{:S(2)}, u32[]{:S(2)}) async-start(bf16[4,80,384]{2,1,0:T(8,128)(2,1)} %partial_attention.1), calls=%async_computation.1 | async-start | bytes 491520 | tf_op jit(solution)/shard_map/all_to_all | solution.py:19
  53.0 0.0 all-gather.6.cloned.1.call-start
  53.1 0.0 copy-done.12
  53.1 0.1 mul.63
  53.1 0.0 copy-done.11
  53.2 0.2 select_reduce_fusion.1
  53.4 0.0 copy-start.7
  53.5 7.6 %all-to-all-done.1 = bf16[4,80,384]{2,1,0:T(8,128)(2,1)S(1)} async-done(((bf16[4,80,384]{2,1,0:T(8,128)(2,1)}), bf16[4,80,384]{2,1,0:T(8,128)(2,1)S(1)}, u32[]{:S(2)}, u32[]{:S(2)}) %all-to-all-start.1) | async-done | bytes 245792 | tf_op jit(solution)/shard_map/all_to_all | solution.py:19
  61.2 27.6 %all-gather = bf16[1024,384]{1,0:T(8,128)(2,1)S(1)} all-gather(bf16[64,384]{1,0:T(8,128)(2,1)S(1)} %fusion.19), channel_id=2, replica_groups=mesh['zh'=4,'zl'=2,'x'=4,'tp'=16] {'tp'}, dimensions={0}, use_global_device_ids=true | all-gather | bytes 835584 | tf_op jit(solution)/shard_map/all_gather | solution.py:295
  88.8 0.2 fusion.3
  89.1 0.2 fusion.5
  89.3 0.0 copy-done
  89.3 0.0 copy-done.7
  89.3 1.1 fusion.16
  90.4 0.0 all-gather.6.cloned.1.call-update
  90.4 0.0 copy-start.4
  90.4 1.8 convolution_convert_fusion
  92.2 23.5 %all_to_all.30 = bf16[32,48,128]{2,1,0:T(8,128)(2,1)S(1)} all-to-all(bf16[32,48,128]{2,1,0:T(8,128)(2,1)S(1)} %bitcast.63), channel_id=1, replica_groups=mesh['zh'=4,'zl'=2,'x'=4,'tp'=16] {'zh','zl','x'}, dimensions={0} | all-to-all | bytes 786432 | tf_op jit(solution)/shard_map/all_to_all | solution.py:19
  115.6 0.8 copy.19
  116.4 6.5 %all-to-all-start.3 = ((bf16[16,96,128]{2,1,0:T(8,128)(2,1)}), bf16[16,96,128]{2,1,0:T(8,128)(2,1)S(1)}, u32[]{:S(2)}, u32[]{:S(2)}) async-start(bf16[16,96,128]{2,1,0:T(8,128)(2,1)} %bitcast.20), calls=%async_computation.3 | async-start | bytes 786432 | tf_op jit(solution)/shard_map/all_to_all | solution.py:19
  122.9 15.4 %all-to-all-done.3.refs_1_ = bf16[16,96,128]{2,1,0:T(8,128)(2,1)S(1)} async-done(((bf16[16,96,128]{2,1,0:T(8,128)(2,1)}), bf16[16,96,128]{2,1,0:T(8,128)(2,1)S(1)}, u32[]{:S(2)}, u32[]{:S(2)}) %all-to-all-start.3) | async-done | bytes 393248 | tf_op jit(solution)/shard_map/all_to_all | solution.py:19
  138.4 0.0 copy-done.4
  138.4 3.8 %routed_feed.1 = bf16[16,96,128]{2,1,0:T(8,128)(2,1)S(1)} custom-call(s32[1]{0:T(128)} %bitcast.16.refs_0_, bf16[16,96,128]{2,1,0:T(8,128)(2,1)S(1)} %all-to-all-done.3.refs_1_, f32[16,1,128]{2,1,0:T(1,128)S(1)} %bitcast.55, bf16[16,3072,128]{2,1,0:T(8,128)(2,1)} %bitcast.57), custom_call_target="tpu_custom_call" | custom-call | tf_op jit(solution)/shard_map/routed_feed/pallas_call | solution.py:197
  142.1 0.0 copy-start.13
  142.2 0.0 copy-start.2
  142.2 0.0 copy-start.3
  142.2 19.2 %all_to_all.31 = bf16[16,96,128]{2,1,0:T(8,128)(2,1)S(1)} all-to-all(bf16[16,96,128]{2,1,0:T(8,128)(2,1)S(1)} %routed_feed.1), channel_id=1, replica_groups=mesh['zh'=4,'zl'=2,'x'=4,'tp'=16] {'tp'}, dimensions={0} | all-to-all | bytes 786432 | tf_op jit(solution)/shard_map/all_to_all | solution.py:19
  161.4 0.8 copy.20
  162.2 3.9 %all-to-all-start.5 = ((bf16[32,48,128]{2,1,0:T(8,128)(2,1)}), bf16[32,48,128]{2,1,0:T(8,128)(2,1)S(1)}, u32[]{:S(2)}, u32[]{:S(2)}) async-start(bf16[32,48,128]{2,1,0:T(8,128)(2,1)} %bitcast.27), calls=%async_computation.5 | async-start | bytes 786432 | tf_op jit(solution)/shard_map/all_to_all | solution.py:19
  166.1 0.0 copy-done.13
  166.1 0.0 all-gather.6.cloned.1.call-done
  166.1 0.0 copy-done.2
  166.1 0.0 copy-done.3
  166.2 1.4 copy-done.1
  167.6 1.2 shared_feed.1
  168.8 15.5 %all_gather.17 = bf16[512,384]{1,0:T(8,128)(2,1)S(1)} all-gather(bf16[32,384]{1,0:T(8,128)(2,1)S(1)} %shared_feed.1), channel_id=1, replica_groups=mesh['zh'=4,'zl'=2,'x'=4,'tp'=16] {'tp'}, dimensions={0}, use_global_device_ids=true | all-gather | bytes 417792 | tf_op jit(solution)/shard_map/all_gather | solution.py:340
  184.3 0.0 all-to-all-done.5
  184.3 1.2 fusion.11
  185.5 0.0 copy-start.5
  185.5 0.0 copy-start.6
  185.5 1.0 fusion.15
  186.6 1.0 fusion.17
  (21 shorter events, 0.3 us)
Async XLA Ops:
  6.5 82.8 %copy-start = (bf16[1024,128]{1,0:T(8,128)(2,1)S(1)}, bf16[1024,128]{1,0:T(8,128)(2,1)}, u32[]{:S(2)}) copy-start(bf16[1024,128]{1,0:T(8,128)(2,1)} %param.22) | copy-start | bytes 786436
  6.5 2.2 %copy-start.9 = (bf16[384,64]{0,1:T(8,128)(2,1)S(1)}, bf16[384,64]{0,1:T(8,128)(2,1)}, u32[]{:S(2)}) copy-start(bf16[384,64]{0,1:T(8,128)(2,1)} %param.17) | copy-start | bytes 147460
  6.5 2.2 %copy-start.8 = (bf16[384,64]{0,1:T(8,128)(2,1)S(1)}, bf16[384,64]{0,1:T(8,128)(2,1)}, u32[]{:S(2)}) copy-start(bf16[384,64]{0,1:T(8,128)(2,1)} %param.18) | copy-start | bytes 147460
  6.5 131.8 %all-gather.8.cloned.1.call-start = ((), (), s32[]{:S(2)}) async-start(), calls=%async_computation.7 | async-start | bytes 13369344 | tf_op jit(solution)/shard_map/all_gather | solution.py:285
  6.5 9.9 %copy-start.10 = (bf16[384,64]{0,1:T(8,128)(2,1)S(1)}, bf16[384,64]{0,1:T(8,128)(2,1)}, u32[]{:S(2)}) copy-start(bf16[384,64]{0,1:T(8,128)(2,1)} %param.16) | copy-start | bytes 147460
  8.8 44.3 %copy-start.12 = (f32[1024]{0:T(1024)S(1)}, f32[1024]{0:T(1024)}, u32[]{:S(2)}) copy-start(f32[1024]{0:T(1024)} %param.21) | copy-start | bytes 12292
  8.8 44.4 %copy-start.11 = (s32[384,2]{0,1:T(2,128)S(1)}, s32[384,2]{0,1:T(2,128)}, u32[]{:S(2)}) copy-start(s32[384,2]{0,1:T(2,128)} %param.24) | copy-start | bytes 9220
  9.8 27.2 %all-to-all-start = ((bf16[8,128,384]{2,1,0:T(8,128)(2,1)}), bf16[8,128,384]{2,1,0:T(8,128)(2,1)S(1)}, u32[]{:S(2)}, u32[]{:S(2)}) async-start(bf16[8,128,384]{2,1,0:T(8,128)(2,1)} %broadcast_in_dim.49), calls=%async_computation | async-start | bytes 1572864 | tf_op jit(solution)/shard_map/all_to_all | solution.py:19
  16.4 18.5 %collective-permute-start = (bf16[64,384]{1,0:T(8,128)(2,1)S(1)}, bf16[64,384]{1,0:T(8,128)(2,1)S(1)}, u32[]{:S(2)}, u32[]{:S(2)}) collective-permute-start(bf16[64,384]{1,0:T(8,128)(2,1)S(1)} %get-tuple-element.16), channel_id=1, source_target_pairs={{0,128},{128,256},{256,384},{384,0},{1,129},{129,257},{257,385},{3... | collective-permute-start | bytes 147464 | tf_op jit(solution)/shard_map/ppermute | solution.py:277
  22.3 14.6 %collective-permute-start.1 = (bf16[64,384]{1,0:T(8,128)(2,1)S(1)}, bf16[64,384]{1,0:T(8,128)(2,1)S(1)}, u32[]{:S(2)}, u32[]{:S(2)}) collective-permute-start(bf16[64,384]{1,0:T(8,128)(2,1)S(1)} %get-tuple-element.16), channel_id=1, source_target_pairs={{0,256},{128,384},{256,0},{384,128},{1,257},{129,385},{257,1},{385... | collective-permute-start | bytes 147464 | tf_op jit(solution)/shard_map/ppermute | solution.py:277
  30.2 6.7 %collective-permute-start.2 = (bf16[64,384]{1,0:T(8,128)(2,1)S(1)}, bf16[64,384]{1,0:T(8,128)(2,1)S(1)}, u32[]{:S(2)}, u32[]{:S(2)}) collective-permute-start(bf16[64,384]{1,0:T(8,128)(2,1)S(1)} %get-tuple-element.16), channel_id=1, source_target_pairs={{0,384},{128,0},{256,128},{384,256},{1,385},{129,1},{257,129},{385... | collective-permute-start | bytes 147464 | tf_op jit(solution)/shard_map/ppermute | solution.py:277
  49.6 11.4 %all-to-all-start.1 = ((bf16[4,80,384]{2,1,0:T(8,128)(2,1)}), bf16[4,80,384]{2,1,0:T(8,128)(2,1)S(1)}, u32[]{:S(2)}, u32[]{:S(2)}) async-start(bf16[4,80,384]{2,1,0:T(8,128)(2,1)} %partial_attention.1), calls=%async_computation.1 | async-start | bytes 491520 | tf_op jit(solution)/shard_map/all_to_all | solution.py:19
  53.0 113.1 %all-gather.6.cloned.1.call-start = ((), (), s32[]{:S(2)}) async-start(), calls=%async_computation.6 | async-start | bytes 1671168 | tf_op jit(solution)/shard_map/all_gather | solution.py:302
  53.4 35.9 %copy-start.7 = (bf16[384,128]{1,0:T(8,128)(2,1)S(1)}, bf16[384,128]{1,0:T(8,128)(2,1)}, u32[]{:S(2)}) copy-start(bf16[384,128]{1,0:T(8,128)(2,1)} %param.20) | copy-start | bytes 294916
  90.4 48.0 %copy-start.4 = (f32[2048]{0:T(1024)S(1)}, f32[2048]{0:T(1024)}, u32[]{:S(2)}) copy-start(f32[2048]{0:T(1024)} %param.23) | copy-start | bytes 24580
  116.4 21.9 %all-to-all-start.3 = ((bf16[16,96,128]{2,1,0:T(8,128)(2,1)}), bf16[16,96,128]{2,1,0:T(8,128)(2,1)S(1)}, u32[]{:S(2)}, u32[]{:S(2)}) async-start(bf16[16,96,128]{2,1,0:T(8,128)(2,1)} %bitcast.20), calls=%async_computation.3 | async-start | bytes 786432 | tf_op jit(solution)/shard_map/all_to_all | solution.py:19
  142.1 23.9 %copy-start.13 = (f32[384,2]{0,1:T(2,128)S(1)}, f32[384,2]{0,1:T(2,128)}, u32[]{:S(2)}) copy-start(f32[384,2]{0,1:T(2,128)} %param.25) | copy-start | bytes 9220
  142.2 24.0 %copy-start.2 = (bf16[2048,32]{0,1:T(8,128)(2,1)S(1)}, bf16[2048,32]{0,1:T(8,128)(2,1)}, u32[]{:S(2)}) copy-start(bf16[2048,32]{0,1:T(8,128)(2,1)} %param.26) | copy-start | bytes 393220
  142.2 24.0 %copy-start.3 = (bf16[2048,32]{0,1:T(8,128)(2,1)S(1)}, bf16[2048,32]{0,1:T(8,128)(2,1)}, u32[]{:S(2)}) copy-start(bf16[2048,32]{0,1:T(8,128)(2,1)} %param.27) | copy-start | bytes 393220
  162.2 22.2 %all-to-all-start.5 = ((bf16[32,48,128]{2,1,0:T(8,128)(2,1)}), bf16[32,48,128]{2,1,0:T(8,128)(2,1)S(1)}, u32[]{:S(2)}, u32[]{:S(2)}) async-start(bf16[32,48,128]{2,1,0:T(8,128)(2,1)} %bitcast.27), calls=%async_computation.5 | async-start | bytes 786432 | tf_op jit(solution)/shard_map/all_to_all | solution.py:19
  166.1 1.4 copy-start.1
  185.5 1.0 copy-start.5
  185.5 1.0 copy-start.6
Sparse Core Ops, SparseCore 0:
  9.5 87.9 all-gather.7
  99.6 42.9 all-gather.5

commit v5 on v4

--- a/solution.py
+++ b/solution.py
@@ -10,6 +10,7 @@
 LANES = 128
 LOW = -1e30
 PAD = 16
+CHAIN = 768
 BF16 = jnp.bfloat16
 F32 = jnp.float32
 GRIDS = {32: (4, 2, 4), 4: (2, 1, 2), 8: (2, 2, 2)}
@@ -35,63 +36,83 @@
     team, own = place[0], place[1]
     teams, head, width = query.shape
     count = kv.shape[0]
+    span = 2 * width
+    reach = min(count, 8) * width
+    piece = min(span, CHAIN)
+    chains = span // piece
 
     for b in range(count):
         parts = three_parts(-cum[:, b * width : (b + 1) * width])
         filler = jnp.zeros((LANES - head - 3, width), BF16)
-        key_rows[b] = jnp.concatenate([kv[b, :head, :], *parts, filler], axis=0).T
-        value_rows[b] = jnp.concatenate([kv[b, head:, :], jnp.ones((PAD, width), BF16)], axis=0)
-
-    def step(block, part, state, masked):
+        key_rows[b * width : (b + 1) * width] = jnp.concatenate(
+            [kv[b, :head, :], *parts, filler], axis=0
+        ).T
+        value_rows[:, b * width : (b + 1) * width] = jnp.concatenate(
+            [kv[b, head:, :], jnp.ones((PAD, width), BF16)], axis=0
+        )
+
+    def step(i, part, state, limit):
         best, acc = state
-        score = jnp.dot(key_rows[block], part, preferred_element_type=F32)
-        if masked:
-            key_pos = lax.broadcasted_iota(jnp.int32, score.shape, 0)
-            query_pos = lax.broadcasted_iota(jnp.int32, score.shape, 1)
-            score = jnp.where(key_pos <= query_pos, score, LOW)
+        at = pl.ds(pl.multiple_of(i * reach, reach), reach)
+        score = jnp.dot(key_rows[at, :], part, preferred_element_type=F32)
+        if limit is not None:
+            key_pos = i * reach + lax.broadcasted_iota(jnp.int32, score.shape, 0)
+            score = jnp.where(key_pos <= limit, score, LOW)
         new_best = jnp.maximum(best, jnp.max(score, axis=0, keepdims=True))
         weight = jnp.exp(score - new_best).astype(BF16)
-        added = jnp.dot(value_rows[block], weight, preferred_element_type=F32)
+        added = jnp.dot(value_rows[:, at], weight, preferred_element_type=F32)
         return new_best, acc * jnp.exp(best - new_best) + added
 
-    def fresh():
-        return jnp.full((1, width), LOW, F32), jnp.zeros((head + PAD, width), F32)
-
-    def extended(j):
-        turn = lax.rem(team - j + teams, teams)
-        return jnp.concatenate([query[turn], jnp.ones((LANES - head, width), BF16)], axis=0)
-
-    def finish(j, states):
-        best = states[0][0]
-        for other, _ in states[1:]:
-            best = jnp.maximum(best, other)
-        acc = sum(a * jnp.exp(m - best) for m, a in states)
+    def run(tile, steps, masked):
+        turns = [lax.rem(team - (2 * tile + n) + teams, teams) for n in range(2)]
+        both = jnp.concatenate([query[turn] for turn in turns], axis=1)
+        both = jnp.concatenate([both, jnp.ones((LANES - head, span), BF16)], axis=0)
+        limits = [None] * chains
+        if masked:
+            lane = lax.broadcasted_iota(jnp.int32, (1, span), 1)
+            block = 2 * tile + jnp.where(lane >= width, 1, 0)
+            at = own * width + jnp.where(lane >= width, lane - width, lane)
+            limit = jnp.where(block < team, -1, jnp.where(block == team, at, count * width))
+            limits = [limit[:, c * piece : (c + 1) * piece] for c in range(chains)]
+        parts = [both[:, c * piece : (c + 1) * piece] for c in range(chains)]
+        first = tuple(
+            (jnp.full((1, piece), LOW, F32), jnp.zeros((head + PAD, piece), F32)) for _ in range(chains)
+        )
+        states = lax.fori_loop(
+            0,
+            steps,
+            lambda i, s: tuple(step(i, parts[c], s[c], limits[c]) for c in range(chains)),
+            first,
+        )
+        best = jnp.concatenate([m for m, _ in states], axis=1)
+        acc = jnp.concatenate([a for _, a in states], axis=1)
         total = acc[head : head + 1]
-        parts = three_parts(best + jnp.log(total))
-        out[j] = jnp.concatenate(
-            [(acc[:head] / total).astype(BF16), *parts, jnp.zeros((PAD - 3, width), BF16)], axis=0
-        )
-
-    def full_tile(j, nothing):
-        part = extended(j)
-
-        def pair(i, states):
-            return tuple(step(2 * i + n, part, s, False) for n, s in enumerate(states))
-
-        finish(j, lax.fori_loop(0, count // 2, pair, (fresh(), fresh())))
+        levels = three_parts(best + jnp.log(total))
+        full = jnp.concatenate(
+            [(acc[:head] / total).astype(BF16), *levels, jnp.zeros((PAD - 3, span), BF16)], axis=0
+        )
+        for n in range(2):
+            out[2 * tile + n] = full[:, n * width : (n + 1) * width]
+
+    mixed_tile = lax.div(team, 2)
+
+    def empty_tile(tile, nothing):
+        blank = jnp.concatenate(
+            [jnp.zeros((head, width), BF16), jnp.full((PAD, width), LOW, BF16)], axis=0
+        )
+        out[2 * tile] = blank
+        out[2 * tile + 1] = blank
         return nothing
 
-    def empty_tile(j, nothing):
-        out[j] = jnp.concatenate(
-            [jnp.zeros((head, width), BF16), jnp.full((PAD, width), LOW, BF16)], axis=0
-        )
+    def full_tile(tile, nothing):
+        run(tile, count * width // reach, False)
         return nothing
 
-    lax.fori_loop(0, team, empty_tile, 0)
-    part = extended(team)
-    state = lax.fori_loop(0, own, lambda b, s: step(b, part, s, False), fresh())
-    finish(team, [step(own, part, state, True)])
-    lax.fori_loop(team + 1, teams, full_tile, 0)
+    lax.fori_loop(0, mixed_tile, empty_tile, 0)
+    whole = count * width // reach
+    steps = jnp.where(lax.rem(team, 2) == 1, lax.div(own * width, reach) + 1, whole)
+    run(mixed_tile, steps, True)
+    lax.fori_loop(mixed_tile + 1, teams // 2, full_tile, 0)
 
 
 def partial_attention(place, kv, query, cum):
@@ -108,8 +129,8 @@
         ],
         out_specs=pl.BlockSpec(memory_space=pltpu.VMEM),
         scratch_shapes=[
-            pltpu.VMEM((count, width, LANES), BF16),
-            pltpu.VMEM((count, head + PAD, width), BF16),
+            pltpu.VMEM((count * width, LANES), BF16),
+            pltpu.VMEM((head + PAD, count * width), BF16),
         ],
         compiler_params=pltpu.CompilerParams(vmem_limit_bytes=32 * 1024 * 1024),
         name="partial_attention",
@@ -319,6 +340,7 @@
     weight_high = lax.reduce_precision(weights, 8, 7)
     weight_low = (weights - weight_high).astype(BF16)
     weight_high = weight_high.astype(BF16)
+    select, weight_high, weight_low = lax.optimization_barrier((select, weight_high, weight_low))
 
     outgoing = lax.dot_general(
         select, updated, (((0,), (0,)), ((), ())), preferred_element_type=F32

time: 195 us -> 187 us (0.959)
  blocking collectives: 85.8 us -> 81.3 us
  Pallas kernels: 19.8 us -> 15.7 us
    all_to_all x2, blocking collectives: 42.7 us -> 38 us  [exchange(): return lax.all_to_all(value, axis, split_axis=0, concat_axis=0, tiled=True)]
    pallas_call x1, Pallas kernels: 12.6 us -> 8.46 us  [partial_attention(): pl.pallas_call(attention_kernel, out_shape=jax.ShapeDtypeStruct((teams, h...]
  transfers between devices with their start and end apart: 9 -> 9, of which waited for: 4 -> 4; matrix products, arithmetic and copies ran while one was open for 4% -> 5% of each run, Pallas kernels for 9% -> 7%
where the time goes in v5:
time: 187 us; the launch traced here: 186 us
  blocking collectives  81.3 us (43%)
  starting transfers between devices  37.5 us (20%)
  waiting for transfers between devices  26.6 us (14%)
  Pallas kernels  15.7 us (8%)
  between operations  13.8 us (7%)
  local copies, waits for them, and re-layouts  4.88 us (3%)
  matrix products  4.58 us (2%)
  other arithmetic  2.05 us (1%)
    all_to_all x2, blocking collectives, exchange(): return lax.all_to_all(value, axis, split_axis=0, concat_axis=0, tiled=True)  38 us
    all_gather x1, blocking collectives, per_device(): lax.all_gather(head_out[None], 'tp', axis=0, tiled=True).astype(F32)  27.7 us
    all_to_all x4, waiting for transfers between devices, exchange(): return lax.all_to_all(value, axis, split_axis=0, concat_axis=0, tiled=True)  24.4 us
    all_to_all x4, starting transfers between devices, exchange(): return lax.all_to_all(value, axis, split_axis=0, concat_axis=0, tiled=True)  20.3 us
    ppermute x3, starting transfers between devices, per_device(): lax.ppermute(query, 'zh', [(i, (i + n) % teams) for i in range(teams)])  17.1 us
    all_gather x1, blocking collectives, per_device(): share_hidden = lax.all_gather(share_hidden, 'tp', axis=0, tiled=True)  15.5 us
    pallas_call x1, Pallas kernels, partial_attention(): pl.pallas_call(attention_kernel, out_shape=jax.ShapeDtypeStruct((teams, h...  8.46 us
    pallas_call x1, Pallas kernels, feed_forward(): pl.pallas_call(lambda *refs: feed_kernel(*refs, experts=experts), out_sha...  3.82 us
  transfers between devices with their start and end apart: 9, of which 4 were waited for; matrix products, arithmetic and copies ran while one was open for 5% of the time, Pallas kernels for 7%

profile of v5, /device:TPU:1, one launch (start us, length us, event | category | flops | bytes accessed | tf_op | source)
XLA Modules:
  0.0 186.3 jit_solution(14861137024433552217)
XLA Ops:
  6.5 0.0 copy-start
  6.5 0.0 all-gather.8.cloned.1.call-start
  6.5 2.1 %pack_shards.1 = bf16[3072,128]{1,0:T(8,128)(2,1)} custom-call(bf16[2,32,2048]{2,1,0:T(8,128)(2,1)} %bitcast.68, bf16[2,32,2048]{2,1,0:T(8,128)(2,1)} %bitcast.69, bf16[1024,128]{1,0:T(8,128)(2,1)} %bitcast.70), custom_call_target="tpu_custom_call" | custom-call | tf_op jit(solution)/shard_map/pack_shards/pallas_call | solution.py:163
  8.7 0.0 all-gather.8.cloned.1.call-update
  8.7 0.0 copy-start.11
  8.7 0.0 copy-done.9
  8.7 0.0 copy-done.8
  8.8 0.0 copy-start.13
  8.8 0.0 copy-start.12
  8.8 1.0 broadcast_in_dim.49
  9.8 6.6 %all-to-all-start = ((bf16[8,128,384]{2,1,0:T(8,128)(2,1)}), bf16[8,128,384]{2,1,0:T(8,128)(2,1)S(1)}, u32[]{:S(2)}, u32[]{:S(2)}) async-start(bf16[8,128,384]{2,1,0:T(8,128)(2,1)} %broadcast_in_dim.49), calls=%async_computation | async-start | bytes 1572864 | tf_op jit(solution)/shard_map/all_to_all | solution.py:20
  16.4 0.0 copy-done.10
  16.5 5.8 %collective-permute-start = (bf16[64,384]{1,0:T(8,128)(2,1)S(1)}, bf16[64,384]{1,0:T(8,128)(2,1)S(1)}, u32[]{:S(2)}, u32[]{:S(2)}) collective-permute-start(bf16[64,384]{1,0:T(8,128)(2,1)S(1)} %get-tuple-element.22), channel_id=1, source_target_pairs={{0,128},{128,256},{256,384},{384,0},{1,129},{129,257},{257,385},{3... | collective-permute-start | bytes 147464 | tf_op jit(solution)/shard_map/ppermute | solution.py:298
  22.3 7.9 %collective-permute-start.1 = (bf16[64,384]{1,0:T(8,128)(2,1)S(1)}, bf16[64,384]{1,0:T(8,128)(2,1)S(1)}, u32[]{:S(2)}, u32[]{:S(2)}) collective-permute-start(bf16[64,384]{1,0:T(8,128)(2,1)S(1)} %get-tuple-element.22), channel_id=1, source_target_pairs={{0,256},{128,384},{256,0},{384,128},{1,257},{129,385},{257,1},{385... | collective-permute-start | bytes 147464 | tf_op jit(solution)/shard_map/ppermute | solution.py:298
  30.2 3.4 %collective-permute-start.2 = (bf16[64,384]{1,0:T(8,128)(2,1)S(1)}, bf16[64,384]{1,0:T(8,128)(2,1)S(1)}, u32[]{:S(2)}, u32[]{:S(2)}) collective-permute-start(bf16[64,384]{1,0:T(8,128)(2,1)S(1)} %get-tuple-element.22), channel_id=1, source_target_pairs={{0,384},{128,0},{256,128},{384,256},{1,385},{129,1},{257,129},{385... | collective-permute-start | bytes 147464 | tf_op jit(solution)/shard_map/ppermute | solution.py:298
  33.6 0.0 copy-done.11
  33.7 0.2 select_reduce_fusion.1
  33.9 0.0 copy-done.13
  34.0 0.7 constant_dynamic-slice_fusion.cum
  34.7 0.1 pad_add_fusion.place
  34.8 0.0 copy-done.12
  34.8 0.1 mul.63
  34.9 0.1 collective-permute-done
  34.9 2.0 %collective-permute-done.1 = bf16[64,384]{1,0:T(8,128)(2,1)S(1)} collective-permute-done((bf16[64,384]{1,0:T(8,128)(2,1)S(1)}, bf16[64,384]{1,0:T(8,128)(2,1)S(1)}, u32[]{:S(2)}, u32[]{:S(2)}) %collective-permute-start.1) | collective-permute-done | bytes 49184 | tf_op jit(solution)/shard_map/ppermute | solution.py:298
  36.9 0.0 collective-permute-done.2
  37.0 0.0 all-to-all-done.kv
  37.0 8.5 %partial_attention.1 = bf16[4,80,384]{2,1,0:T(8,128)(2,1)} custom-call(s32[2]{0:T(128)S(1)} %pad_add_fusion.place, bf16[8,128,384]{2,1,0:T(8,128)(2,1)S(1)} %all-to-all-done.kv, bf16[4,64,384]{2,1,0:T(8,128)(2,1)S(1)} %pad_maximum_fusion.query, f32[1,3072]{1,0:T(1,128)S(1)} %constant_dynamic-slice_fusion.cum), custom_call_target="tpu_custom_call" | custom-call | tf_op jit(solution)/shard_map/partial_attention/pallas_call | solution.py:121
  45.4 3.4 %all-to-all-start.1 = ((bf16[4,80,384]{2,1,0:T(8,128)(2,1)}), bf16[4,80,384]{2,1,0:T(8,128)(2,1)S(1)}, u32[]{:S(2)}, u32[]{:S(2)}) async-start(bf16[4,80,384]{2,1,0:T(8,128)(2,1)} %partial_attention.1), calls=%async_computation.1 | async-start | bytes 491520 | tf_op jit(solution)/shard_map/all_to_all | solution.py:20
  48.9 0.0 all-gather.6.cloned.1.call-start
  48.9 0.8 fusion
  49.7 7.7 %all-to-all-done.1 = bf16[4,80,384]{2,1,0:T(8,128)(2,1)S(1)} async-done(((bf16[4,80,384]{2,1,0:T(8,128)(2,1)}), bf16[4,80,384]{2,1,0:T(8,128)(2,1)S(1)}, u32[]{:S(2)}, u32[]{:S(2)}) %all-to-all-start.1) | async-done | bytes 245792 | tf_op jit(solution)/shard_map/all_to_all | solution.py:20
  57.6 0.0 copy-start.7
  57.6 27.7 %all-gather = bf16[1024,384]{1,0:T(8,128)(2,1)S(1)} all-gather(bf16[64,384]{1,0:T(8,128)(2,1)S(1)} %fusion.11), channel_id=2, replica_groups=mesh['zh'=4,'zl'=2,'x'=4,'tp'=16] {'tp'}, dimensions={0}, use_global_device_ids=true | all-gather | bytes 835584 | tf_op jit(solution)/shard_map/all_gather | solution.py:316
  85.3 0.2 fusion.3
  85.5 0.2 fusion.5
  85.8 0.0 copy-done
  85.8 0.0 copy-done.7
  85.8 1.1 fusion.8
  86.8 0.0 all-gather.6.cloned.1.call-update
  86.9 0.5 fusion.6
  87.4 1.4 convolution_convert_fusion
  88.8 0.0 copy-start.4
  88.8 20.2 %all_to_all.30 = bf16[32,48,128]{2,1,0:T(8,128)(2,1)S(1)} all-to-all(bf16[32,48,128]{2,1,0:T(8,128)(2,1)S(1)} %bitcast.67), channel_id=1, replica_groups=mesh['zh'=4,'zl'=2,'x'=4,'tp'=16] {'zh','zl','x'}, dimensions={0} | all-to-all | bytes 786432 | tf_op jit(solution)/shard_map/all_to_all | solution.py:20
  109.0 0.8 copy.19
  109.7 6.3 %all-to-all-start.3 = ((bf16[16,96,128]{2,1,0:T(8,128)(2,1)}), bf16[16,96,128]{2,1,0:T(8,128)(2,1)S(1)}, u32[]{:S(2)}, u32[]{:S(2)}) async-start(bf16[16,96,128]{2,1,0:T(8,128)(2,1)} %bitcast.20), calls=%async_computation.3 | async-start | bytes 786432 | tf_op jit(solution)/shard_map/all_to_all | solution.py:20
  116.0 16.7 %all-to-all-done.3.refs_1_ = bf16[16,96,128]{2,1,0:T(8,128)(2,1)S(1)} async-done(((bf16[16,96,128]{2,1,0:T(8,128)(2,1)}), bf16[16,96,128]{2,1,0:T(8,128)(2,1)S(1)}, u32[]{:S(2)}, u32[]{:S(2)}) %all-to-all-start.3) | async-done | bytes 393248 | tf_op jit(solution)/shard_map/all_to_all | solution.py:20
  132.7 0.0 copy-done.4
  132.7 3.8 %routed_feed.1 = bf16[16,96,128]{2,1,0:T(8,128)(2,1)S(1)} custom-call(s32[1]{0:T(128)} %bitcast.16.refs_0_, bf16[16,96,128]{2,1,0:T(8,128)(2,1)S(1)} %all-to-all-done.3.refs_1_, f32[16,1,128]{2,1,0:T(1,128)S(1)} %bitcast.58, bf16[16,3072,128]{2,1,0:T(8,128)(2,1)} %bitcast.60), custom_call_target="tpu_custom_call" | custom-call | tf_op jit(solution)/shard_map/routed_feed/pallas_call | solution.py:218
  136.6 0.0 copy-start.2
  136.6 0.0 copy-start.3
  136.6 17.8 %all_to_all.31 = bf16[16,96,128]{2,1,0:T(8,128)(2,1)S(1)} all-to-all(bf16[16,96,128]{2,1,0:T(8,128)(2,1)S(1)} %routed_feed.1), channel_id=1, replica_groups=mesh['zh'=4,'zl'=2,'x'=4,'tp'=16] {'tp'}, dimensions={0} | all-to-all | bytes 786432 | tf_op jit(solution)/shard_map/all_to_all | solution.py:20
  154.4 0.8 copy.20
  155.2 4.0 %all-to-all-start.5 = ((bf16[32,48,128]{2,1,0:T(8,128)(2,1)}), bf16[32,48,128]{2,1,0:T(8,128)(2,1)S(1)}, u32[]{:S(2)}, u32[]{:S(2)}) async-start(bf16[32,48,128]{2,1,0:T(8,128)(2,1)} %bitcast.64), calls=%async_computation.5 | async-start | bytes 786432 | tf_op jit(solution)/shard_map/all_to_all | solution.py:20
  159.3 0.0 all-gather.6.cloned.1.call-done
  159.3 0.0 copy-done.2
  159.3 0.0 copy-done.3
  159.3 1.4 copy-done.1
  160.7 1.2 shared_feed.1
  162.0 15.5 %all_gather.17 = bf16[512,384]{1,0:T(8,128)(2,1)S(1)} all-gather(bf16[32,384]{1,0:T(8,128)(2,1)S(1)} %shared_feed.1), channel_id=1, replica_groups=mesh['zh'=4,'zl'=2,'x'=4,'tp'=16] {'tp'}, dimensions={0}, use_global_device_ids=true | all-gather | bytes 417792 | tf_op jit(solution)/shard_map/all_gather | solution.py:362
  177.5 0.0 copy-done.5
  177.5 0.3 convolution_add_fusion.1
  177.8 0.0 all-to-all-done.5
  177.8 0.5 fusion.24
  178.3 1.1 fusion.9
  (23 shorter events, 0.3 us)
Async XLA Ops:
  6.5 79.2 %copy-start = (bf16[1024,128]{1,0:T(8,128)(2,1)S(1)}, bf16[1024,128]{1,0:T(8,128)(2,1)}, u32[]{:S(2)}) copy-start(bf16[1024,128]{1,0:T(8,128)(2,1)} %param.22) | copy-start | bytes 786436
  6.5 2.2 %copy-start.9 = (bf16[384,64]{0,1:T(8,128)(2,1)S(1)}, bf16[384,64]{0,1:T(8,128)(2,1)}, u32[]{:S(2)}) copy-start(bf16[384,64]{0,1:T(8,128)(2,1)} %param.17) | copy-start | bytes 147460
  6.5 2.2 %copy-start.8 = (bf16[384,64]{0,1:T(8,128)(2,1)S(1)}, bf16[384,64]{0,1:T(8,128)(2,1)}, u32[]{:S(2)}) copy-start(bf16[384,64]{0,1:T(8,128)(2,1)} %param.18) | copy-start | bytes 147460
  6.5 126.2 %all-gather.8.cloned.1.call-start = ((), (), s32[]{:S(2)}) async-start(), calls=%async_computation.7 | async-start | bytes 13369344 | tf_op jit(solution)/shard_map/all_gather | solution.py:306
  8.7 7.8 %copy-start.10 = (bf16[384,64]{0,1:T(8,128)(2,1)S(1)}, bf16[384,64]{0,1:T(8,128)(2,1)}, u32[]{:S(2)}) copy-start(bf16[384,64]{0,1:T(8,128)(2,1)} %param.16) | copy-start | bytes 147460
  8.7 24.9 %copy-start.11 = (s32[384,2]{0,1:T(2,128)S(1)}, s32[384,2]{0,1:T(2,128)}, u32[]{:S(2)}) copy-start(s32[384,2]{0,1:T(2,128)} %param.24) | copy-start | bytes 9220
  8.8 25.2 %copy-start.13 = (f32[384,2]{0,1:T(2,128)S(1)}, f32[384,2]{0,1:T(2,128)}, u32[]{:S(2)}) copy-start(f32[384,2]{0,1:T(2,128)} %param.25) | copy-start | bytes 9220
  8.8 26.0 %copy-start.12 = (f32[1024]{0:T(1024)S(1)}, f32[1024]{0:T(1024)}, u32[]{:S(2)}) copy-start(f32[1024]{0:T(1024)} %param.21) | copy-start | bytes 12292
  9.8 27.2 %all-to-all-start = ((bf16[8,128,384]{2,1,0:T(8,128)(2,1)}), bf16[8,128,384]{2,1,0:T(8,128)(2,1)S(1)}, u32[]{:S(2)}, u32[]{:S(2)}) async-start(bf16[8,128,384]{2,1,0:T(8,128)(2,1)} %broadcast_in_dim.49), calls=%async_computation | async-start | bytes 1572864 | tf_op jit(solution)/shard_map/all_to_all | solution.py:20
  16.5 18.5 %collective-permute-start = (bf16[64,384]{1,0:T(8,128)(2,1)S(1)}, bf16[64,384]{1,0:T(8,128)(2,1)S(1)}, u32[]{:S(2)}, u32[]{:S(2)}) collective-permute-start(bf16[64,384]{1,0:T(8,128)(2,1)S(1)} %get-tuple-element.22), channel_id=1, source_target_pairs={{0,128},{128,256},{256,384},{384,0},{1,129},{129,257},{257,385},{3... | collective-permute-start | bytes 147464 | tf_op jit(solution)/shard_map/ppermute | solution.py:298
  22.3 14.6 %collective-permute-start.1 = (bf16[64,384]{1,0:T(8,128)(2,1)S(1)}, bf16[64,384]{1,0:T(8,128)(2,1)S(1)}, u32[]{:S(2)}, u32[]{:S(2)}) collective-permute-start(bf16[64,384]{1,0:T(8,128)(2,1)S(1)} %get-tuple-element.22), channel_id=1, source_target_pairs={{0,256},{128,384},{256,0},{384,128},{1,257},{129,385},{257,1},{385... | collective-permute-start | bytes 147464 | tf_op jit(solution)/shard_map/ppermute | solution.py:298
  30.2 6.7 %collective-permute-start.2 = (bf16[64,384]{1,0:T(8,128)(2,1)S(1)}, bf16[64,384]{1,0:T(8,128)(2,1)S(1)}, u32[]{:S(2)}, u32[]{:S(2)}) collective-permute-start(bf16[64,384]{1,0:T(8,128)(2,1)S(1)} %get-tuple-element.22), channel_id=1, source_target_pairs={{0,384},{128,0},{256,128},{384,256},{1,385},{129,1},{257,129},{385... | collective-permute-start | bytes 147464 | tf_op jit(solution)/shard_map/ppermute | solution.py:298
  45.4 12.0 %all-to-all-start.1 = ((bf16[4,80,384]{2,1,0:T(8,128)(2,1)}), bf16[4,80,384]{2,1,0:T(8,128)(2,1)S(1)}, u32[]{:S(2)}, u32[]{:S(2)}) async-start(bf16[4,80,384]{2,1,0:T(8,128)(2,1)} %partial_attention.1), calls=%async_computation.1 | async-start | bytes 491520 | tf_op jit(solution)/shard_map/all_to_all | solution.py:20
  48.9 110.4 %all-gather.6.cloned.1.call-start = ((), (), s32[]{:S(2)}) async-start(), calls=%async_computation.6 | async-start | bytes 1671168 | tf_op jit(solution)/shard_map/all_gather | solution.py:323
  57.6 28.2 %copy-start.7 = (bf16[384,128]{1,0:T(8,128)(2,1)S(1)}, bf16[384,128]{1,0:T(8,128)(2,1)}, u32[]{:S(2)}) copy-start(bf16[384,128]{1,0:T(8,128)(2,1)} %param.20) | copy-start | bytes 294916
  88.8 44.0 %copy-start.4 = (f32[2048]{0:T(1024)S(1)}, f32[2048]{0:T(1024)}, u32[]{:S(2)}) copy-start(f32[2048]{0:T(1024)} %param.23) | copy-start | bytes 24580
  109.7 23.0 %all-to-all-start.3 = ((bf16[16,96,128]{2,1,0:T(8,128)(2,1)}), bf16[16,96,128]{2,1,0:T(8,128)(2,1)S(1)}, u32[]{:S(2)}, u32[]{:S(2)}) async-start(bf16[16,96,128]{2,1,0:T(8,128)(2,1)} %bitcast.20), calls=%async_computation.3 | async-start | bytes 786432 | tf_op jit(solution)/shard_map/all_to_all | solution.py:20
  136.6 22.7 %copy-start.2 = (bf16[2048,32]{0,1:T(8,128)(2,1)S(1)}, bf16[2048,32]{0,1:T(8,128)(2,1)}, u32[]{:S(2)}) copy-start(bf16[2048,32]{0,1:T(8,128)(2,1)} %param.26) | copy-start | bytes 393220
  136.6 22.7 %copy-start.3 = (bf16[2048,32]{0,1:T(8,128)(2,1)S(1)}, bf16[2048,32]{0,1:T(8,128)(2,1)}, u32[]{:S(2)}) copy-start(bf16[2048,32]{0,1:T(8,128)(2,1)} %param.27) | copy-start | bytes 393220
  155.2 22.3 %copy-start.5 = (bf16[384,128]{1,0:T(8,128)(2,1)S(1)}, bf16[384,128]{1,0:T(8,128)(2,1)}, u32[]{:S(2)}) copy-start(bf16[384,128]{1,0:T(8,128)(2,1)} %fusion.8) | copy-start | bytes 294916
  155.2 22.3 %copy-start.6 = (bf16[512,128]{1,0:T(8,128)(2,1)S(1)}, bf16[512,128]{1,0:T(8,128)(2,1)}, u32[]{:S(2)}) copy-start(bf16[512,128]{1,0:T(8,128)(2,1)} %param.28) | copy-start | bytes 393220
  155.2 22.6 %all-to-all-start.5 = ((bf16[32,48,128]{2,1,0:T(8,128)(2,1)}), bf16[32,48,128]{2,1,0:T(8,128)(2,1)S(1)}, u32[]{:S(2)}, u32[]{:S(2)}) async-start(bf16[32,48,128]{2,1,0:T(8,128)(2,1)} %bitcast.64), calls=%async_computation.5 | async-start | bytes 786432 | tf_op jit(solution)/shard_map/all_to_all | solution.py:20
  159.3 1.4 copy-start.1
Sparse Core Ops, SparseCore 0:
  9.5 87.9 all-gather.7
  99.6 43.1 all-gather.5

commit v6 on v5

--- a/solution.py
+++ b/solution.py
@@ -169,28 +169,32 @@
     )(*sources)
 
 
-def feed_kernel(which, rows, gain, weights, out, gate, upward, down, sems, *, experts):
+def feed_kernel(which, rows, gain, weights, out, gate, upward, *rest, first, count, experts):
+    down, sems = rest if len(rest) == 2 else (None, rest[0])
     shards, hidden = gate.shape[0], gate.shape[1]
     inner = shards * hidden
     features = shards * LANES
     mine = which[0]
     wide = features * hidden // LANES
     bases = [mine * wide, (experts + mine) * wide, 2 * experts * wide + mine * inner]
+    if down is None:
+        shared = experts * (2 * wide + inner)
+        bases = [shared, shared + wide, 0]
     for n, target in enumerate((gate, upward)):
-        base = pl.multiple_of(bases[n], hidden)
+        base = bases[n] if down is None else pl.multiple_of(bases[n], hidden)
         for k in range(features // LANES):
             pltpu.make_async_copy(
                 weights.at[:, pl.ds(base + k * hidden, hidden), :],
                 target.at[:, :, pl.ds(k * LANES, LANES)],
                 sems.at[n],
             ).start()
-    base = pl.multiple_of(bases[2], hidden)
-    for t in range(shards):
+    base = 0 if down is None else pl.multiple_of(bases[2], hidden)
+    for t in range(0 if down is None else shards):
         pltpu.make_async_copy(
             weights.at[t, pl.ds(base, inner), :], down.at[:, pl.ds(t * LANES, LANES)], sems.at[2]
         ).start()
 
-    floats = [rows[t].astype(F32) for t in range(shards)]
+    floats = [rows[t, first : first + count].astype(F32) for t in range(shards)]
     squares = sum(f * f for f in floats)
     mean = jnp.sum(squares, axis=1, keepdims=True) / features
     inverse = lax.rsqrt(mean + EPS)
@@ -205,19 +209,24 @@
         normed, upward[...].reshape(inner, features), across, preferred_element_type=F32
     )
     inside = gated_hidden(first_half, second_half)
+    if down is None:
+        out[...] = inside
+        return
     pltpu.make_async_copy(down, down, sems.at[2]).wait()
     for t in range(shards):
         part = jnp.dot(inside, down[:, t * LANES : (t + 1) * LANES], preferred_element_type=F32)
         out[t] = part.astype(BF16)
 
 
-def feed_forward(which, rows, gain, weights, hidden, experts):
+def feed_forward(which, rows, gain, weights, hidden, experts, first, count, whole):
     shards = rows.shape[0]
     features = shards * LANES
     inner = shards * hidden
+    shape = (shards, count, LANES) if whole else (count, inner)
+    down = [pltpu.VMEM((inner, features), BF16)] if whole else []
     return pl.pallas_call(
-        lambda *refs: feed_kernel(*refs, experts=experts),
-        out_shape=jax.ShapeDtypeStruct(rows.shape, BF16),
+        lambda *refs: feed_kernel(*refs, first=first, count=count, experts=experts),
+        out_shape=jax.ShapeDtypeStruct(shape, BF16),
         in_specs=[
             pl.BlockSpec(memory_space=pltpu.SMEM),
             pl.BlockSpec(memory_space=pltpu.VMEM),
@@ -228,36 +237,12 @@
         scratch_shapes=[
             pltpu.VMEM((shards, hidden, features), BF16),
             pltpu.VMEM((shards, hidden, features), BF16),
-            pltpu.VMEM((inner, features), BF16),
+            *down,
             pltpu.SemaphoreType.DMA((3,)),
         ],
         compiler_params=pltpu.CompilerParams(vmem_limit_bytes=52 * 1024 * 1024),
-        name="routed_feed",
+        name="routed_feed" if whole else "shared_feed",
     )(which, rows, gain, weights)
-
-
-def shared_kernel(rows, gain, gate, upward, out):
-    shards = rows.shape[0]
-    floats = [rows[t].astype(F32) for t in range(shards)]
-    squares = sum(f * f for f in floats)
-    inverse = lax.rsqrt(jnp.sum(squares, axis=1, keepdims=True) / (shards * LANES) + EPS)
-    normed = jnp.concatenate([(f * inverse * gain[t]).astype(BF16) for t, f in enumerate(floats)], axis=1)
-    across = (((1,), (1,)), ((), ()))
-    out[...] = gated_hidden(
-        lax.dot_general(gate[...], normed, across, preferred_element_type=F32),
-        lax.dot_general(upward[...], normed, across, preferred_element_type=F32),
-    )
-
-
-def shared_feed(rows, gain, gate, upward):
-    return pl.pallas_call(
-        shared_kernel,
-        out_shape=jax.ShapeDtypeStruct((gate.shape[0], rows.shape[1]), BF16),
-        in_specs=[pl.BlockSpec(memory_space=pltpu.VMEM) for _ in range(4)],
-        out_specs=pl.BlockSpec(memory_space=pltpu.VMEM),
-        compiler_params=pltpu.CompilerParams(vmem_limit_bytes=24 * 1024 * 1024),
-        name="shared_feed",
-    )(rows, gain, gate, upward)
 
 
 def per_device(
@@ -301,7 +286,11 @@
     query = jnp.stack([query, *moved])
     cum = lax.dynamic_slice_in_dim(log_cum, team * group * width, group * width, 1)
     expert_weights = packed_shards(
-        jnp.swapaxes(exp_gate, 1, 2), jnp.swapaxes(exp_up, 1, 2), exp_down.reshape(-1, LANES)
+        jnp.swapaxes(exp_gate, 1, 2),
+        jnp.swapaxes(exp_up, 1, 2),
+        exp_down.reshape(-1, LANES),
+        sh_gate.T[None],
+        sh_up.T[None],
     )
     expert_weights = lax.all_gather(expert_weights, "tp", axis=0, tiled=False)
 
@@ -320,7 +309,6 @@
     mixed = (all_heads * inverse * out_gain.reshape(shards, head, 1)).astype(BF16).reshape(channels, width)
     attended = lax.dot_general(mixed, w_out, (((0,), (0,)), ((), ())), preferred_element_type=F32)
     updated = (residual.astype(F32) + attended).astype(BF16)
-    all_rows = lax.all_gather(updated[None], "tp", axis=0, tiled=True)
 
     top = routes.shape[1]
     experts = local_experts * blocks
@@ -330,39 +318,42 @@
     named = sum(c.astype(BF16) for c in chosen)
     earlier = (lax.iota(jnp.int32, width)[:, None] > lax.iota(jnp.int32, width)[None, :]).astype(BF16)
     rank = jnp.dot(earlier, named, preferred_element_type=F32)
-    picks = []
+    picks, turned = [], []
     for k in range(top):
         own = jnp.sum(jnp.where(chosen[k], rank, 0.0), axis=1).astype(jnp.int32)
         slot = routes[:, k] * capacity + own
         picks.append(slot[:, None] == lax.iota(jnp.int32, slots)[None, :])
-    select = sum(p.astype(BF16) for p in picks)
+        turned.append(lax.iota(jnp.int32, slots)[:, None] == slot[None, :])
+    select = sum(t.astype(BF16) for t in turned)
     weights = sum(jnp.where(p, route_weight[:, k, None], 0.0) for k, p in enumerate(picks))
     weight_high = lax.reduce_precision(weights, 8, 7)
     weight_low = (weights - weight_high).astype(BF16)
     weight_high = weight_high.astype(BF16)
     select, weight_high, weight_low = lax.optimization_barrier((select, weight_high, weight_low))
 
-    outgoing = lax.dot_general(
-        select, updated, (((0,), (0,)), ((), ())), preferred_element_type=F32
-    ).astype(BF16)
+    outgoing = jnp.dot(select, updated, preferred_element_type=F32).astype(BF16)
     per_block = local_experts * capacity
     landed = exchange(outgoing.reshape(blocks, per_block, LANES), whole)
     rounds = blocks // owners
     landed = landed.reshape(rounds, owners, local_experts, capacity, LANES)
     landed = jnp.transpose(landed, (2, 1, 0, 3, 4)).reshape(shards, rounds * capacity, LANES)
-    rows = exchange(landed, "tp")
+    own_rows = updated.reshape(shards, width // shards, LANES)
+    rows = exchange(jnp.concatenate([landed, own_rows], axis=1), "tp")
     gain = ffn_gain.reshape(shards, 1, LANES)
     mine = (shard // owners).astype(jnp.int32)[None]
-    routed_out = feed_forward(mine, rows, gain, expert_weights, hidden, local_experts)
+    routed_rows = rounds * capacity
+    routed_out = feed_forward(
+        mine, rows, gain, expert_weights, hidden, local_experts, 0, routed_rows, True
+    )
     returned = exchange(routed_out, "tp")
     returned = returned.reshape(local_experts, owners, rounds, capacity, LANES)
     returned = jnp.transpose(returned, (2, 1, 0, 3, 4)).reshape(blocks, per_block, LANES)
     answers = exchange(returned, whole).reshape(slots, LANES)
-    share_hidden = shared_feed(all_rows, gain, sh_gate.T, sh_up.T)
+    share_hidden = feed_forward(
+        mine, rows, gain, expert_weights, hidden, local_experts, routed_rows, width // shards, False
+    )
     share_hidden = lax.all_gather(share_hidden, "tp", axis=0, tiled=True)
-    shared = lax.dot_general(
-        share_hidden, sh_down, (((0,), (0,)), ((), ())), preferred_element_type=F32
-    )
+    shared = jnp.dot(share_hidden, sh_down, preferred_element_type=F32)
     routed = jnp.dot(weight_high, answers, preferred_element_type=F32) + jnp.dot(
         weight_low, answers, preferred_element_type=F32
     )

time: 187 us -> 192 us (1.027)
  other arithmetic: 2.05 us -> 5.14 us
  waiting for transfers between devices: 26.6 us -> 28.8 us
  Pallas kernels: 15.7 us -> 17.7 us
    all_to_all x4, waiting for transfers between devices: 24.4 us -> 28.8 us  [exchange(): return lax.all_to_all(value, axis, split_axis=0, concat_axis=0, tiled=True)]
    ppermute x3, waiting for transfers between devices: 2.08 us -> 0.01 us  [per_device(): lax.ppermute(query, 'zh', [(i, (i + n) % teams) for i in range(teams)])]
    all_gather x1, blocking collectives: 27.7 us -> 29.7 us  [per_device(): lax.all_gather(head_out[None], 'tp', axis=0, tiled=True).astype(F32)]
  transfers between devices with their start and end apart: 9 -> 8, of which waited for: 4 -> 3; matrix products, arithmetic and copies ran while one was open for 5% -> 4% of each run, Pallas kernels for 7% -> 6%
where the time goes in v6:
time: 192 us
  blocking collectives  82.3 us (43%)
  starting transfers between devices  37.6 us (20%)
  waiting for transfers between devices  28.8 us (15%)
  Pallas kernels  17.7 us (9%)
  between operations  13.7 us (7%)
  other arithmetic  5.14 us (3%)
  local copies, waits for them, and re-layouts  3.36 us (2%)
  matrix products  2.94 us (2%)
    all_to_all x2, blocking collectives, exchange(): return lax.all_to_all(value, axis, split_axis=0, concat_axis=0, tiled=True)  36.9 us
    all_gather x1, blocking collectives, per_device(): lax.all_gather(head_out[None], 'tp', axis=0, tiled=True).astype(F32)  29.7 us
    all_to_all x4, waiting for transfers between devices, exchange(): return lax.all_to_all(value, axis, split_axis=0, concat_axis=0, tiled=True)  28.8 us
    ppermute x3, starting transfers between devices, per_device(): lax.ppermute(query, 'zh', [(i, (i + n) % teams) for i in range(teams)])  18.8 us
    all_to_all x4, starting transfers between devices, exchange(): return lax.all_to_all(value, axis, split_axis=0, concat_axis=0, tiled=True)  18.7 us
    all_gather x1, blocking collectives, per_device(): share_hidden = lax.all_gather(share_hidden, 'tp', axis=0, tiled=True)  15.7 us
    pallas_call x1, Pallas kernels, partial_attention(): pl.pallas_call(attention_kernel, out_shape=jax.ShapeDtypeStruct((teams, h...  8.43 us
    pallas_call x2, Pallas kernels, feed_forward(): pl.pallas_call(lambda *refs: feed_kernel(*refs, first=first, count=count,...  6.91 us
  transfers between devices with their start and end apart: 8, of which 3 were waited for; matrix products, arithmetic and copies ran while one was open for 4% of the time, Pallas kernels for 6%

profile of v6, /device:TPU:1, one launch (start us, length us, event | category | flops | bytes accessed | tf_op | source)
XLA Modules:
  0.0 191.6 jit_solution(3478940138945045892)
XLA Ops:
  6.5 0.0 copy-start
  6.5 0.0 all-gather.4.cloned.1.call-start
  6.5 0.0 copy-start.6
  6.5 0.0 copy-start.7
  6.5 0.0 copy-start.8
  6.6 2.4 %pack_shards.1 = bf16[4096,128]{1,0:T(8,128)(2,1)} custom-call(bf16[2,32,2048]{2,1,0:T(8,128)(2,1)} %bitcast.71, bf16[2,32,2048]{2,1,0:T(8,128)(2,1)} %bitcast.72, bf16[1024,128]{1,0:T(8,128)(2,1)} %bitcast.73, bf16[1,32,2048]{2,1,0:T(8,128)(2,1)} %bitcast.74, bf16[1,32,2048]{2,1,0:T(8,128)(2,1)} %bitcast.75), custom_call_target="tpu_custom_call" | custom-call | tf_op jit(solution)/shard_map/pack_shards/pallas_call | solution.py:163
  8.9 0.0 all-gather.4.cloned.1.call-update
  8.9 0.0 copy-done.6
  9.0 0.0 copy-start.9
  9.0 6.6 %collective-permute-start = (bf16[64,384]{1,0:T(8,128)(2,1)S(1)}, bf16[64,384]{1,0:T(8,128)(2,1)S(1)}, u32[]{:S(2)}, u32[]{:S(2)}) collective-permute-start(bf16[64,384]{1,0:T(8,128)(2,1)S(1)} %get-tuple-element.22), channel_id=1, source_target_pairs={{0,128},{128,256},{256,384},{384,0},{1,129},{129,257},{257,385},{3... | collective-permute-start | bytes 147464 | tf_op jit(solution)/shard_map/ppermute | solution.py:283
  15.6 8.8 %collective-permute-start.1 = (bf16[64,384]{1,0:T(8,128)(2,1)S(1)}, bf16[64,384]{1,0:T(8,128)(2,1)S(1)}, u32[]{:S(2)}, u32[]{:S(2)}) collective-permute-start(bf16[64,384]{1,0:T(8,128)(2,1)S(1)} %get-tuple-element.22), channel_id=1, source_target_pairs={{0,256},{128,384},{256,0},{384,128},{1,257},{129,385},{257,1},{385... | collective-permute-start | bytes 147464 | tf_op jit(solution)/shard_map/ppermute | solution.py:283
  24.5 3.4 %collective-permute-start.2 = (bf16[64,384]{1,0:T(8,128)(2,1)S(1)}, bf16[64,384]{1,0:T(8,128)(2,1)S(1)}, u32[]{:S(2)}, u32[]{:S(2)}) collective-permute-start(bf16[64,384]{1,0:T(8,128)(2,1)S(1)} %get-tuple-element.22), channel_id=1, source_target_pairs={{0,384},{128,0},{256,128},{384,256},{1,385},{129,1},{257,129},{385... | collective-permute-start | bytes 147464 | tf_op jit(solution)/shard_map/ppermute | solution.py:283
  27.9 0.0 copy-done.7
  27.9 0.0 copy-done.8
  27.9 0.0 copy-start.11
  27.9 1.0 broadcast_in_dim.56
  28.9 4.9 %all-to-all-start = ((bf16[8,128,384]{2,1,0:T(8,128)(2,1)}), bf16[8,128,384]{2,1,0:T(8,128)(2,1)S(1)}, u32[]{:S(2)}, u32[]{:S(2)}) async-start(bf16[8,128,384]{2,1,0:T(8,128)(2,1)} %broadcast_in_dim.56), calls=%async_computation | async-start | bytes 1572864 | tf_op jit(solution)/shard_map/all_to_all | solution.py:20
  33.8 0.0 copy-start.10
  33.9 0.0 copy-done.9
  33.9 0.2 select_reduce_fusion.1
  34.2 0.0 copy-done.11
  34.2 0.7 constant_dynamic-slice_fusion.cum
  34.9 1.8 fusion
  36.7 0.1 pad_add_fusion.place
  36.8 0.0 copy-done.10
  36.8 0.1 mul.75
  36.9 0.0 collective-permute-done
  36.9 0.0 collective-permute-done.1
  36.9 0.0 collective-permute-done.2
  36.9 6.2 %all-to-all-done.kv = bf16[8,128,384]{2,1,0:T(8,128)(2,1)S(1)} async-done(((bf16[8,128,384]{2,1,0:T(8,128)(2,1)}), bf16[8,128,384]{2,1,0:T(8,128)(2,1)S(1)}, u32[]{:S(2)}, u32[]{:S(2)}) %all-to-all-start) | async-done | bytes 786464 | tf_op jit(solution)/shard_map/all_to_all | solution.py:20
  43.1 8.4 %partial_attention.1 = bf16[4,80,384]{2,1,0:T(8,128)(2,1)} custom-call(s32[2]{0:T(128)S(1)} %pad_add_fusion.place, bf16[8,128,384]{2,1,0:T(8,128)(2,1)S(1)} %all-to-all-done.kv, bf16[4,64,384]{2,1,0:T(8,128)(2,1)S(1)} %pad_maximum_fusion.1.query, f32[1,3072]{1,0:T(1,128)S(1)} %constant_dynamic-slice_fusion.cum), custom_call_target="tpu_custom_call" | custom-call | tf_op jit(solution)/shard_map/partial_attention/pallas_call | solution.py:121
  51.6 3.4 %all-to-all-start.1 = ((bf16[4,80,384]{2,1,0:T(8,128)(2,1)}), bf16[4,80,384]{2,1,0:T(8,128)(2,1)S(1)}, u32[]{:S(2)}, u32[]{:S(2)}) async-start(bf16[4,80,384]{2,1,0:T(8,128)(2,1)} %partial_attention.1), calls=%async_computation.1 | async-start | bytes 491520 | tf_op jit(solution)/shard_map/all_to_all | solution.py:20
  55.0 1.8 fusion.6
  56.7 6.1 %all-to-all-done.1 = bf16[4,80,384]{2,1,0:T(8,128)(2,1)S(1)} async-done(((bf16[4,80,384]{2,1,0:T(8,128)(2,1)}), bf16[4,80,384]{2,1,0:T(8,128)(2,1)S(1)}, u32[]{:S(2)}, u32[]{:S(2)}) %all-to-all-start.1) | async-done | bytes 245792 | tf_op jit(solution)/shard_map/all_to_all | solution.py:20
  63.0 0.0 copy-start.5
  63.0 29.7 %all-gather = bf16[1024,384]{1,0:T(8,128)(2,1)S(1)} all-gather(bf16[64,384]{1,0:T(8,128)(2,1)S(1)} %fusion.11), channel_id=2, replica_groups=mesh['zh'=4,'zl'=2,'x'=4,'tp'=16] {'tp'}, dimensions={0}, use_global_device_ids=true | all-gather | bytes 835584 | tf_op jit(solution)/shard_map/all_gather | solution.py:305
  92.7 0.2 fusion.3
  92.9 0.0 copy-start.2
  92.9 0.2 fusion.5
  93.2 0.0 copy-done
  93.2 0.0 copy-done.5
  93.2 0.4 fusion.8
  93.6 0.6 copy-done.2
  94.2 0.5 convolution_convert_fusion
  94.7 19.6 %all_to_all.30 = bf16[32,48,128]{2,1,0:T(8,128)(2,1)S(1)} all-to-all(bf16[32,48,128]{2,1,0:T(8,128)(2,1)S(1)} %bitcast.68), channel_id=1, replica_groups=mesh['zh'=4,'zl'=2,'x'=4,'tp'=16] {'zh','zl','x'}, dimensions={0} | all-to-all | bytes 786432 | tf_op jit(solution)/shard_map/all_to_all | solution.py:20
  114.4 0.0 copy-start.1
  114.4 0.8 pad_maximum_fusion
  115.2 6.4 %all-to-all-start.3 = ((bf16[16,120,128]{2,1,0:T(8,128)(2,1)}), bf16[16,120,128]{2,1,0:T(8,128)(2,1)S(1)}, u32[]{:S(2)}, u32[]{:S(2)}) async-start(bf16[16,120,128]{2,1,0:T(8,128)(2,1)} %pad_maximum_fusion), calls=%async_computation.3 | async-start | bytes 983040 | tf_op jit(solution)/shard_map/all_to_all | solution.py:20
  121.7 16.5 %all-to-all-done.3.refs_1_ = bf16[16,120,128]{2,1,0:T(8,128)(2,1)S(1)} async-done(((bf16[16,120,128]{2,1,0:T(8,128)(2,1)}), bf16[16,120,128]{2,1,0:T(8,128)(2,1)S(1)}, u32[]{:S(2)}, u32[]{:S(2)}) %all-to-all-start.3) | async-done | bytes 491552 | tf_op jit(solution)/shard_map/all_to_all | solution.py:20
  138.2 0.0 copy-done.1
  138.2 3.8 %routed_feed.1 = bf16[16,96,128]{2,1,0:T(8,128)(2,1)S(1)} custom-call(s32[1]{0:T(128)} %bitcast.12.refs_0_, bf16[16,120,128]{2,1,0:T(8,128)(2,1)S(1)} %all-to-all-done.3.refs_1_, f32[16,1,128]{2,1,0:T(1,128)S(1)} %bitcast.59, bf16[16,4096,128]{2,1,0:T(8,128)(2,1)} %bitcast.61), custom_call_target="tpu_custom_call" | custom-call | tf_op jit(solution)/shard_map/routed_feed/pallas_call | solution.py:227
  142.0 17.2 %all_to_all.31 = bf16[16,96,128]{2,1,0:T(8,128)(2,1)S(1)} all-to-all(bf16[16,96,128]{2,1,0:T(8,128)(2,1)S(1)} %routed_feed.1), channel_id=1, replica_groups=mesh['zh'=4,'zl'=2,'x'=4,'tp'=16] {'tp'}, dimensions={0} | all-to-all | bytes 786432 | tf_op jit(solution)/shard_map/all_to_all | solution.py:20
  159.2 0.8 copy.20
  160.1 3.9 %all-to-all-start.5 = ((bf16[32,48,128]{2,1,0:T(8,128)(2,1)}), bf16[32,48,128]{2,1,0:T(8,128)(2,1)S(1)}, u32[]{:S(2)}, u32[]{:S(2)}) async-start(bf16[32,48,128]{2,1,0:T(8,128)(2,1)} %bitcast.29), calls=%async_computation.5 | async-start | bytes 786432 | tf_op jit(solution)/shard_map/all_to_all | solution.py:20
  164.0 0.0 copy-start.4
  164.0 3.1 %shared_feed.1 = bf16[24,512]{1,0:T(8,128)(2,1)S(1)} custom-call(s32[1]{0:T(128)} %bitcast.12.refs_0_, bf16[16,120,128]{2,1,0:T(8,128)(2,1)S(1)} %all-to-all-done.3.refs_1_, f32[16,1,128]{2,1,0:T(1,128)S(1)} %bitcast.60, bf16[16,4096,128]{2,1,0:T(8,128)(2,1)} %bitcast.62), custom_call_target="tpu_custom_call" | custom-call | tf_op jit(solution)/shard_map/shared_feed/pallas_call | solution.py:227
  167.2 0.0 copy-start.3
  167.2 15.7 %all_gather.15 = bf16[384,512]{1,0:T(8,128)(2,1)S(1)} all-gather(bf16[24,512]{1,0:T(8,128)(2,1)S(1)} %shared_feed.1), channel_id=1, replica_groups=mesh['zh'=4,'zl'=2,'x'=4,'tp'=16] {'tp'}, dimensions={0}, use_global_device_ids=true | all-gather | bytes 417792 | tf_op jit(solution)/shard_map/all_gather | solution.py:355
  182.8 0.0 copy-done.4
  182.8 0.3 convolution_add_fusion.1
  183.1 0.0 all-to-all-done.5
  183.1 0.5 fusion.24
  183.6 0.0 copy-done.3
  183.6 1.1 fusion.9
  (18 shorter events, 0.3 us)
Async XLA Ops:
  6.5 86.6 %copy-start = (bf16[1024,128]{1,0:T(8,128)(2,1)S(1)}, bf16[1024,128]{1,0:T(8,128)(2,1)}, u32[]{:S(2)}) copy-start(bf16[1024,128]{1,0:T(8,128)(2,1)} %param.22) | copy-start | bytes 786436
  6.5 131.7 %all-gather.4.cloned.1.call-start = ((), (), s32[]{:S(2)}) async-start(), calls=%async_computation.6 | async-start | bytes 17825792 | tf_op jit(solution)/shard_map/all_gather | solution.py:295
  6.5 2.4 %copy-start.6 = (bf16[384,64]{0,1:T(8,128)(2,1)S(1)}, bf16[384,64]{0,1:T(8,128)(2,1)}, u32[]{:S(2)}) copy-start(bf16[384,64]{0,1:T(8,128)(2,1)} %param.16) | copy-start | bytes 147460
  6.5 21.3 %copy-start.7 = (bf16[384,64]{0,1:T(8,128)(2,1)S(1)}, bf16[384,64]{0,1:T(8,128)(2,1)}, u32[]{:S(2)}) copy-start(bf16[384,64]{0,1:T(8,128)(2,1)} %param.18) | copy-start | bytes 147460
  6.5 21.3 %copy-start.8 = (bf16[384,64]{0,1:T(8,128)(2,1)S(1)}, bf16[384,64]{0,1:T(8,128)(2,1)}, u32[]{:S(2)}) copy-start(bf16[384,64]{0,1:T(8,128)(2,1)} %param.17) | copy-start | bytes 147460
  9.0 24.9 %copy-start.9 = (s32[384,2]{0,1:T(2,128)S(1)}, s32[384,2]{0,1:T(2,128)}, u32[]{:S(2)}) copy-start(s32[384,2]{0,1:T(2,128)} %param.24) | copy-start | bytes 9220
  9.0 27.9 %collective-permute-start = (bf16[64,384]{1,0:T(8,128)(2,1)S(1)}, bf16[64,384]{1,0:T(8,128)(2,1)S(1)}, u32[]{:S(2)}, u32[]{:S(2)}) collective-permute-start(bf16[64,384]{1,0:T(8,128)(2,1)S(1)} %get-tuple-element.22), channel_id=1, source_target_pairs={{0,128},{128,256},{256,384},{384,0},{1,129},{129,257},{257,385},{3... | collective-permute-start | bytes 147464 | tf_op jit(solution)/shard_map/ppermute | solution.py:283
  15.6 21.2 %collective-permute-start.1 = (bf16[64,384]{1,0:T(8,128)(2,1)S(1)}, bf16[64,384]{1,0:T(8,128)(2,1)S(1)}, u32[]{:S(2)}, u32[]{:S(2)}) collective-permute-start(bf16[64,384]{1,0:T(8,128)(2,1)S(1)} %get-tuple-element.22), channel_id=1, source_target_pairs={{0,256},{128,384},{256,0},{384,128},{1,257},{129,385},{257,1},{385... | collective-permute-start | bytes 147464 | tf_op jit(solution)/shard_map/ppermute | solution.py:283
  24.5 12.4 %collective-permute-start.2 = (bf16[64,384]{1,0:T(8,128)(2,1)S(1)}, bf16[64,384]{1,0:T(8,128)(2,1)S(1)}, u32[]{:S(2)}, u32[]{:S(2)}) collective-permute-start(bf16[64,384]{1,0:T(8,128)(2,1)S(1)} %get-tuple-element.22), channel_id=1, source_target_pairs={{0,384},{128,0},{256,128},{384,256},{1,385},{129,1},{257,129},{385... | collective-permute-start | bytes 147464 | tf_op jit(solution)/shard_map/ppermute | solution.py:283
  27.9 6.3 %copy-start.11 = (f32[384,2]{0,1:T(2,128)S(1)}, f32[384,2]{0,1:T(2,128)}, u32[]{:S(2)}) copy-start(f32[384,2]{0,1:T(2,128)} %param.25) | copy-start | bytes 9220
  28.9 14.2 %all-to-all-start = ((bf16[8,128,384]{2,1,0:T(8,128)(2,1)}), bf16[8,128,384]{2,1,0:T(8,128)(2,1)S(1)}, u32[]{:S(2)}, u32[]{:S(2)}) async-start(bf16[8,128,384]{2,1,0:T(8,128)(2,1)} %broadcast_in_dim.56), calls=%async_computation | async-start | bytes 1572864 | tf_op jit(solution)/shard_map/all_to_all | solution.py:20
  33.8 2.9 %copy-start.10 = (f32[1024]{0:T(1024)S(1)}, f32[1024]{0:T(1024)}, u32[]{:S(2)}) copy-start(f32[1024]{0:T(1024)} %param.21) | copy-start | bytes 12292
  51.6 11.2 %all-to-all-start.1 = ((bf16[4,80,384]{2,1,0:T(8,128)(2,1)}), bf16[4,80,384]{2,1,0:T(8,128)(2,1)S(1)}, u32[]{:S(2)}, u32[]{:S(2)}) async-start(bf16[4,80,384]{2,1,0:T(8,128)(2,1)} %partial_attention.1), calls=%async_computation.1 | async-start | bytes 491520 | tf_op jit(solution)/shard_map/all_to_all | solution.py:20
  63.0 30.2 %copy-start.5 = (bf16[384,128]{1,0:T(8,128)(2,1)S(1)}, bf16[384,128]{1,0:T(8,128)(2,1)}, u32[]{:S(2)}) copy-start(bf16[384,128]{1,0:T(8,128)(2,1)} %param.20) | copy-start | bytes 294916
  92.9 1.3 copy-start.2
  114.4 23.9 %copy-start.1 = (f32[2048]{0:T(1024)S(1)}, f32[2048]{0:T(1024)}, u32[]{:S(2)}) copy-start(f32[2048]{0:T(1024)} %param.23) | copy-start | bytes 24580
  115.2 23.0 %all-to-all-start.3 = ((bf16[16,120,128]{2,1,0:T(8,128)(2,1)}), bf16[16,120,128]{2,1,0:T(8,128)(2,1)S(1)}, u32[]{:S(2)}, u32[]{:S(2)}) async-start(bf16[16,120,128]{2,1,0:T(8,128)(2,1)} %pad_maximum_fusion), calls=%async_computation.3 | async-start | bytes 983040 | tf_op jit(solution)/shard_map/all_to_all | solution.py:20
  160.1 23.1 %all-to-all-start.5 = ((bf16[32,48,128]{2,1,0:T(8,128)(2,1)}), bf16[32,48,128]{2,1,0:T(8,128)(2,1)S(1)}, u32[]{:S(2)}, u32[]{:S(2)}) async-start(bf16[32,48,128]{2,1,0:T(8,128)(2,1)} %bitcast.29), calls=%async_computation.5 | async-start | bytes 786432 | tf_op jit(solution)/shard_map/all_to_all | solution.py:20
  164.0 18.8 %copy-start.4 = (bf16[512,128]{1,0:T(8,128)(2,1)S(1)}, bf16[512,128]{1,0:T(8,128)(2,1)}, u32[]{:S(2)}) copy-start(bf16[512,128]{1,0:T(8,128)(2,1)} %param.28) | copy-start | bytes 393220
  167.2 16.4 %copy-start.3 = (bf16[384,1536]{1,0:T(8,128)(2,1)S(1)}, bf16[384,1536]{1,0:T(8,128)(2,1)}, u32[]{:S(2)}) copy-start(bf16[384,1536]{1,0:T(8,128)(2,1)} %get-tuple-element.10) | copy-start | bytes 3538948
Sparse Core Ops, SparseCore 0:
  9.4 107.7 all-gather.3

commit v7 on v5

--- a/solution.py
+++ b/solution.py
@@ -307,7 +307,8 @@
 
     place = jnp.stack([team, own]).astype(jnp.int32)
     partial = partial_attention(place, key_value, query, cum)
-    partial = exchange(partial, "zh").astype(F32)
+    partial = exchange(partial, "zh")
+    partial = partial.astype(F32)
     level = partial[:, head] + partial[:, head + 1] + partial[:, head + 2]
     share = jnp.exp(level - jnp.max(level, axis=0, keepdims=True))
     share = share / jnp.sum(share, axis=0, keepdims=True)
@@ -330,21 +331,20 @@
     named = sum(c.astype(BF16) for c in chosen)
     earlier = (lax.iota(jnp.int32, width)[:, None] > lax.iota(jnp.int32, width)[None, :]).astype(BF16)
     rank = jnp.dot(earlier, named, preferred_element_type=F32)
-    picks = []
+    picks, turned = [], []
     for k in range(top):
         own = jnp.sum(jnp.where(chosen[k], rank, 0.0), axis=1).astype(jnp.int32)
         slot = routes[:, k] * capacity + own
         picks.append(slot[:, None] == lax.iota(jnp.int32, slots)[None, :])
-    select = sum(p.astype(BF16) for p in picks)
+        turned.append(lax.iota(jnp.int32, slots)[:, None] == slot[None, :])
+    select = lax.optimization_barrier(sum(t.astype(BF16) for t in turned))
     weights = sum(jnp.where(p, route_weight[:, k, None], 0.0) for k, p in enumerate(picks))
     weight_high = lax.reduce_precision(weights, 8, 7)
     weight_low = (weights - weight_high).astype(BF16)
     weight_high = weight_high.astype(BF16)
-    select, weight_high, weight_low = lax.optimization_barrier((select, weight_high, weight_low))
-
-    outgoing = lax.dot_general(
-        select, updated, (((0,), (0,)), ((), ())), preferred_element_type=F32
-    ).astype(BF16)
+    weight_high, weight_low = lax.optimization_barrier((weight_high, weight_low))
+
+    outgoing = jnp.dot(select, updated, preferred_element_type=F32).astype(BF16)
     per_block = local_experts * capacity
     landed = exchange(outgoing.reshape(blocks, per_block, LANES), whole)
     rounds = blocks // owners

time: 187 us -> 190 us (1.016)
  blocking collectives: 81.3 us -> 63.4 us
  waiting for transfers between devices: 26.6 us -> 39.9 us
  starting transfers between devices: 37.5 us -> 42.4 us
    all_to_all x2 -> x1, blocking collectives: 38 us -> 20.2 us  [exchange(): return lax.all_to_all(value, axis, split_axis=0, concat_axis=0, tiled=True)]
    all_to_all x4 -> x5, waiting for transfers between devices: 24.4 us -> 37.7 us  [exchange(): return lax.all_to_all(value, axis, split_axis=0, concat_axis=0, tiled=True)]
    all_to_all x4 -> x5, starting transfers between devices: 20.3 us -> 25.2 us  [exchange(): return lax.all_to_all(value, axis, split_axis=0, concat_axis=0, tiled=True)]
  transfers between devices with their start and end apart: 9 -> 10, of which waited for: 4 -> 5; matrix products, arithmetic and copies ran while one was open for 5% -> 5% of each run, Pallas kernels for 7% -> 8%
where the time goes in v7:
time: 190 us; the launch traced here: 189 us
  blocking collectives  63.4 us (33%)
  starting transfers between devices  42.4 us (22%)
  waiting for transfers between devices  39.9 us (21%)
  Pallas kernels  16.4 us (9%)
  between operations  13.7 us (7%)
  local copies, waits for them, and re-layouts  5.37 us (3%)
  matrix products  5.23 us (3%)
  other arithmetic  2.28 us (1%)
    all_to_all x5, waiting for transfers between devices, exchange(): return lax.all_to_all(value, axis, split_axis=0, concat_axis=0, tiled=True)  37.7 us
    all_gather x1, blocking collectives, per_device(): lax.all_gather(head_out[None], 'tp', axis=0, tiled=True).astype(F32)  27.7 us
    all_to_all x5, starting transfers between devices, exchange(): return lax.all_to_all(value, axis, split_axis=0, concat_axis=0, tiled=True)  25.2 us
    all_to_all x1, blocking collectives, exchange(): return lax.all_to_all(value, axis, split_axis=0, concat_axis=0, tiled=True)  20.2 us
    ppermute x3, starting transfers between devices, per_device(): lax.ppermute(query, 'zh', [(i, (i + n) % teams) for i in range(teams)])  17.1 us
    all_gather x1, blocking collectives, per_device(): share_hidden = lax.all_gather(share_hidden, 'tp', axis=0, tiled=True)  15.5 us
    pallas_call x1, Pallas kernels, partial_attention(): pl.pallas_call(attention_kernel, out_shape=jax.ShapeDtypeStruct((teams, h...  8.49 us
    pallas_call x1, Pallas kernels, feed_forward(): pl.pallas_call(lambda *refs: feed_kernel(*refs, experts=experts), out_sha...  4.53 us
  transfers between devices with their start and end apart: 10, of which 5 were waited for; matrix products, arithmetic and copies ran while one was open for 5% of the time, Pallas kernels for 8%

profile of v7, /device:TPU:1, one launch (start us, length us, event | category | flops | bytes accessed | tf_op | source)
XLA Modules:
  0.0 188.8 jit_solution(12103883671736806714)
XLA Ops:
  6.5 0.0 copy-start
  6.5 0.0 all-gather.8.cloned.1.call-start
  6.5 2.2 %pack_shards.1 = bf16[3072,128]{1,0:T(8,128)(2,1)} custom-call(bf16[2,32,2048]{2,1,0:T(8,128)(2,1)} %bitcast.67, bf16[2,32,2048]{2,1,0:T(8,128)(2,1)} %bitcast.68, bf16[1024,128]{1,0:T(8,128)(2,1)} %bitcast.69), custom_call_target="tpu_custom_call" | custom-call | tf_op jit(solution)/shard_map/pack_shards/pallas_call | solution.py:163
  8.7 0.0 all-gather.8.cloned.1.call-update
  8.7 0.0 copy-start.12
  8.7 0.0 copy-done.10
  8.8 0.0 copy-done.9
  8.8 0.0 copy-start.13
  8.8 1.0 broadcast_in_dim.53
  9.8 6.6 %all-to-all-start = ((bf16[8,128,384]{2,1,0:T(8,128)(2,1)}), bf16[8,128,384]{2,1,0:T(8,128)(2,1)S(1)}, u32[]{:S(2)}, u32[]{:S(2)}) async-start(bf16[8,128,384]{2,1,0:T(8,128)(2,1)} %broadcast_in_dim.53), calls=%async_computation | async-start | bytes 1572864 | tf_op jit(solution)/shard_map/all_to_all | solution.py:20
  16.5 0.0 copy-done.11
  16.5 5.8 %collective-permute-start = (bf16[64,384]{1,0:T(8,128)(2,1)S(1)}, bf16[64,384]{1,0:T(8,128)(2,1)S(1)}, u32[]{:S(2)}, u32[]{:S(2)}) collective-permute-start(bf16[64,384]{1,0:T(8,128)(2,1)S(1)} %get-tuple-element.20), channel_id=1, source_target_pairs={{0,128},{128,256},{256,384},{384,0},{1,129},{129,257},{257,385},{3... | collective-permute-start | bytes 147464 | tf_op jit(solution)/shard_map/ppermute | solution.py:298
  22.3 7.9 %collective-permute-start.1 = (bf16[64,384]{1,0:T(8,128)(2,1)S(1)}, bf16[64,384]{1,0:T(8,128)(2,1)S(1)}, u32[]{:S(2)}, u32[]{:S(2)}) collective-permute-start(bf16[64,384]{1,0:T(8,128)(2,1)S(1)} %get-tuple-element.20), channel_id=1, source_target_pairs={{0,256},{128,384},{256,0},{384,128},{1,257},{129,385},{257,1},{385... | collective-permute-start | bytes 147464 | tf_op jit(solution)/shard_map/ppermute | solution.py:298
  30.3 3.4 %collective-permute-start.2 = (bf16[64,384]{1,0:T(8,128)(2,1)S(1)}, bf16[64,384]{1,0:T(8,128)(2,1)S(1)}, u32[]{:S(2)}, u32[]{:S(2)}) collective-permute-start(bf16[64,384]{1,0:T(8,128)(2,1)S(1)} %get-tuple-element.20), channel_id=1, source_target_pairs={{0,384},{128,0},{256,128},{384,256},{1,385},{129,1},{257,129},{385... | collective-permute-start | bytes 147464 | tf_op jit(solution)/shard_map/ppermute | solution.py:298
  33.7 0.0 copy-done.12
  33.7 0.2 select_reduce_fusion.1
  33.9 0.7 constant_dynamic-slice_fusion.cum
  34.7 0.1 pad_add_fusion.place
  34.7 0.0 copy-done.13
  34.7 0.1 mul.75
  34.8 0.2 collective-permute-done
  35.0 2.0 %collective-permute-done.1 = bf16[64,384]{1,0:T(8,128)(2,1)S(1)} collective-permute-done((bf16[64,384]{1,0:T(8,128)(2,1)S(1)}, bf16[64,384]{1,0:T(8,128)(2,1)S(1)}, u32[]{:S(2)}, u32[]{:S(2)}) %collective-permute-start.1) | collective-permute-done | bytes 49184 | tf_op jit(solution)/shard_map/ppermute | solution.py:298
  37.0 0.0 collective-permute-done.2
  37.0 0.0 all-to-all-done.kv
  37.0 8.5 %partial_attention.1 = bf16[4,80,384]{2,1,0:T(8,128)(2,1)} custom-call(s32[2]{0:T(128)S(1)} %pad_add_fusion.place, bf16[8,128,384]{2,1,0:T(8,128)(2,1)S(1)} %all-to-all-done.kv, bf16[4,64,384]{2,1,0:T(8,128)(2,1)S(1)} %pad_maximum_fusion.query, f32[1,3072]{1,0:T(1,128)S(1)} %constant_dynamic-slice_fusion.cum), custom_call_target="tpu_custom_call" | custom-call | tf_op jit(solution)/shard_map/partial_attention/pallas_call | solution.py:121
  45.5 3.4 %all-to-all-start.1 = ((bf16[4,80,384]{2,1,0:T(8,128)(2,1)}), bf16[4,80,384]{2,1,0:T(8,128)(2,1)S(1)}, u32[]{:S(2)}, u32[]{:S(2)}) async-start(bf16[4,80,384]{2,1,0:T(8,128)(2,1)} %partial_attention.1), calls=%async_computation.1 | async-start | bytes 491520 | tf_op jit(solution)/shard_map/all_to_all | solution.py:20
  48.9 0.0 all-gather.6.cloned.1.call-start
  48.9 0.7 fusion.6
  49.7 7.8 %all-to-all-done.1 = bf16[4,80,384]{2,1,0:T(8,128)(2,1)S(1)} async-done(((bf16[4,80,384]{2,1,0:T(8,128)(2,1)}), bf16[4,80,384]{2,1,0:T(8,128)(2,1)S(1)}, u32[]{:S(2)}, u32[]{:S(2)}) %all-to-all-start.1) | async-done | bytes 245792 | tf_op jit(solution)/shard_map/all_to_all | solution.py:20
  57.6 0.0 copy-start.8
  57.7 27.7 %all-gather = bf16[1024,384]{1,0:T(8,128)(2,1)S(1)} all-gather(bf16[64,384]{1,0:T(8,128)(2,1)S(1)} %fusion.11), channel_id=2, replica_groups=mesh['zh'=4,'zl'=2,'x'=4,'tp'=16] {'tp'}, dimensions={0}, use_global_device_ids=true | all-gather | bytes 835584 | tf_op jit(solution)/shard_map/all_gather | solution.py:317
  85.3 0.2 fusion.3
  85.6 0.2 fusion.5
  85.8 0.0 copy-done
  85.8 0.0 copy-done.8
  85.8 1.1 fusion.8
  86.9 0.0 all-gather.6.cloned.1.call-update
  86.9 1.4 convolution_convert_fusion
  88.3 0.0 copy-start.4
  88.3 20.2 %all_to_all.30 = bf16[32,48,128]{2,1,0:T(8,128)(2,1)S(1)} all-to-all(bf16[32,48,128]{2,1,0:T(8,128)(2,1)S(1)} %bitcast.66), channel_id=1, replica_groups=mesh['zh'=4,'zl'=2,'x'=4,'tp'=16] {'zh','zl','x'}, dimensions={0} | all-to-all | bytes 786432 | tf_op jit(solution)/shard_map/all_to_all | solution.py:20
  108.5 0.8 copy.19
  109.3 6.3 %all-to-all-start.3 = ((bf16[16,96,128]{2,1,0:T(8,128)(2,1)}), bf16[16,96,128]{2,1,0:T(8,128)(2,1)S(1)}, u32[]{:S(2)}, u32[]{:S(2)}) async-start(bf16[16,96,128]{2,1,0:T(8,128)(2,1)} %bitcast.20), calls=%async_computation.3 | async-start | bytes 786432 | tf_op jit(solution)/shard_map/all_to_all | solution.py:20
  115.6 15.5 %all-to-all-done.3.refs_1_ = bf16[16,96,128]{2,1,0:T(8,128)(2,1)S(1)} async-done(((bf16[16,96,128]{2,1,0:T(8,128)(2,1)}), bf16[16,96,128]{2,1,0:T(8,128)(2,1)S(1)}, u32[]{:S(2)}, u32[]{:S(2)}) %all-to-all-start.3) | async-done | bytes 393248 | tf_op jit(solution)/shard_map/all_to_all | solution.py:20
  131.1 0.0 copy-done.4
  131.1 4.5 %routed_feed.1 = bf16[16,96,128]{2,1,0:T(8,128)(2,1)} custom-call(s32[1]{0:T(128)} %bitcast.16.refs_0_, bf16[16,96,128]{2,1,0:T(8,128)(2,1)S(1)} %all-to-all-done.3.refs_1_, f32[16,1,128]{2,1,0:T(1,128)S(1)} %bitcast.58, bf16[16,3072,128]{2,1,0:T(8,128)(2,1)} %bitcast.60), custom_call_target="tpu_custom_call" | custom-call | tf_op jit(solution)/shard_map/routed_feed/pallas_call | solution.py:218
  135.6 4.9 %all-to-all-start.4 = ((bf16[16,96,128]{2,1,0:T(8,128)(2,1)}), bf16[16,96,128]{2,1,0:T(8,128)(2,1)S(1)}, u32[]{:S(2)}, u32[]{:S(2)}) async-start(bf16[16,96,128]{2,1,0:T(8,128)(2,1)} %routed_feed.1), calls=%async_computation.4 | async-start | bytes 786432 | tf_op jit(solution)/shard_map/all_to_all | solution.py:20
  140.5 0.0 copy-done.14
  140.6 14.4 %all-to-all-done.4 = bf16[16,96,128]{2,1,0:T(8,128)(2,1)S(1)} async-done(((bf16[16,96,128]{2,1,0:T(8,128)(2,1)}), bf16[16,96,128]{2,1,0:T(8,128)(2,1)S(1)}, u32[]{:S(2)}, u32[]{:S(2)}) %all-to-all-start.4) | async-done | bytes 393248 | tf_op jit(solution)/shard_map/all_to_all | solution.py:20
  155.0 0.8 copy.20
  155.8 4.0 %all-to-all-start.5 = ((bf16[32,48,128]{2,1,0:T(8,128)(2,1)}), bf16[32,48,128]{2,1,0:T(8,128)(2,1)S(1)}, u32[]{:S(2)}, u32[]{:S(2)}) async-start(bf16[32,48,128]{2,1,0:T(8,128)(2,1)} %bitcast.27), calls=%async_computation.5 | async-start | bytes 786432 | tf_op jit(solution)/shard_map/all_to_all | solution.py:20
  159.8 0.0 copy-start.5
  159.9 0.0 copy-start.7
  159.9 0.8 fusion
  160.7 0.0 all-gather.6.cloned.1.call-done
  160.7 0.0 copy-done.2
  160.7 1.4 copy-done.1
  162.1 1.2 shared_feed.1
  163.4 15.5 %all_gather.17 = bf16[512,384]{1,0:T(8,128)(2,1)S(1)} all-gather(bf16[32,384]{1,0:T(8,128)(2,1)S(1)} %shared_feed.1), channel_id=1, replica_groups=mesh['zh'=4,'zl'=2,'x'=4,'tp'=16] {'tp'}, dimensions={0}, use_global_device_ids=true | all-gather | bytes 417792 | tf_op jit(solution)/shard_map/all_gather | solution.py:362
  178.9 0.0 copy-done.5
  178.9 1.0 convolution_add_fusion.1
  179.9 0.0 all-to-all-done.5
  179.9 0.5 fusion.24
  180.4 0.4 copy-done.6
  180.8 1.1 fusion.9
  (27 shorter events, 0.3 us)
Async XLA Ops:
  6.5 79.3 %copy-start = (bf16[1024,128]{1,0:T(8,128)(2,1)S(1)}, bf16[1024,128]{1,0:T(8,128)(2,1)}, u32[]{:S(2)}) copy-start(bf16[1024,128]{1,0:T(8,128)(2,1)} %param.22) | copy-start | bytes 786436
  6.5 2.2 %copy-start.10 = (bf16[384,64]{0,1:T(8,128)(2,1)S(1)}, bf16[384,64]{0,1:T(8,128)(2,1)}, u32[]{:S(2)}) copy-start(bf16[384,64]{0,1:T(8,128)(2,1)} %param.17) | copy-start | bytes 147460
  6.5 2.2 %copy-start.9 = (bf16[384,64]{0,1:T(8,128)(2,1)S(1)}, bf16[384,64]{0,1:T(8,128)(2,1)}, u32[]{:S(2)}) copy-start(bf16[384,64]{0,1:T(8,128)(2,1)} %param.18) | copy-start | bytes 147460
  6.5 124.5 %all-gather.8.cloned.1.call-start = ((), (), s32[]{:S(2)}) async-start(), calls=%async_computation.7 | async-start | bytes 13369344 | tf_op jit(solution)/shard_map/all_gather | solution.py:306
  8.7 7.8 %copy-start.11 = (bf16[384,64]{0,1:T(8,128)(2,1)S(1)}, bf16[384,64]{0,1:T(8,128)(2,1)}, u32[]{:S(2)}) copy-start(bf16[384,64]{0,1:T(8,128)(2,1)} %param.16) | copy-start | bytes 147460
  8.7 24.9 %copy-start.12 = (s32[384,2]{0,1:T(2,128)S(1)}, s32[384,2]{0,1:T(2,128)}, u32[]{:S(2)}) copy-start(s32[384,2]{0,1:T(2,128)} %param.24) | copy-start | bytes 9220
  8.8 25.9 %copy-start.13 = (f32[1024]{0:T(1024)S(1)}, f32[1024]{0:T(1024)}, u32[]{:S(2)}) copy-start(f32[1024]{0:T(1024)} %param.21) | copy-start | bytes 12292
  9.8 27.2 %all-to-all-start = ((bf16[8,128,384]{2,1,0:T(8,128)(2,1)}), bf16[8,128,384]{2,1,0:T(8,128)(2,1)S(1)}, u32[]{:S(2)}, u32[]{:S(2)}) async-start(bf16[8,128,384]{2,1,0:T(8,128)(2,1)} %broadcast_in_dim.53), calls=%async_computation | async-start | bytes 1572864 | tf_op jit(solution)/shard_map/all_to_all | solution.py:20
  16.5 18.5 %collective-permute-start = (bf16[64,384]{1,0:T(8,128)(2,1)S(1)}, bf16[64,384]{1,0:T(8,128)(2,1)S(1)}, u32[]{:S(2)}, u32[]{:S(2)}) collective-permute-start(bf16[64,384]{1,0:T(8,128)(2,1)S(1)} %get-tuple-element.20), channel_id=1, source_target_pairs={{0,128},{128,256},{256,384},{384,0},{1,129},{129,257},{257,385},{3... | collective-permute-start | bytes 147464 | tf_op jit(solution)/shard_map/ppermute | solution.py:298
  22.3 14.6 %collective-permute-start.1 = (bf16[64,384]{1,0:T(8,128)(2,1)S(1)}, bf16[64,384]{1,0:T(8,128)(2,1)S(1)}, u32[]{:S(2)}, u32[]{:S(2)}) collective-permute-start(bf16[64,384]{1,0:T(8,128)(2,1)S(1)} %get-tuple-element.20), channel_id=1, source_target_pairs={{0,256},{128,384},{256,0},{384,128},{1,257},{129,385},{257,1},{385... | collective-permute-start | bytes 147464 | tf_op jit(solution)/shard_map/ppermute | solution.py:298
  30.3 6.7 %collective-permute-start.2 = (bf16[64,384]{1,0:T(8,128)(2,1)S(1)}, bf16[64,384]{1,0:T(8,128)(2,1)S(1)}, u32[]{:S(2)}, u32[]{:S(2)}) collective-permute-start(bf16[64,384]{1,0:T(8,128)(2,1)S(1)} %get-tuple-element.20), channel_id=1, source_target_pairs={{0,384},{128,0},{256,128},{384,256},{1,385},{129,1},{257,129},{385... | collective-permute-start | bytes 147464 | tf_op jit(solution)/shard_map/ppermute | solution.py:298
  45.5 12.0 %all-to-all-start.1 = ((bf16[4,80,384]{2,1,0:T(8,128)(2,1)}), bf16[4,80,384]{2,1,0:T(8,128)(2,1)S(1)}, u32[]{:S(2)}, u32[]{:S(2)}) async-start(bf16[4,80,384]{2,1,0:T(8,128)(2,1)} %partial_attention.1), calls=%async_computation.1 | async-start | bytes 491520 | tf_op jit(solution)/shard_map/all_to_all | solution.py:20
  48.9 111.8 %all-gather.6.cloned.1.call-start = ((), (), s32[]{:S(2)}) async-start(), calls=%async_computation.6 | async-start | bytes 1671168 | tf_op jit(solution)/shard_map/all_gather | solution.py:324
  57.6 28.2 %copy-start.8 = (bf16[384,128]{1,0:T(8,128)(2,1)S(1)}, bf16[384,128]{1,0:T(8,128)(2,1)}, u32[]{:S(2)}) copy-start(bf16[384,128]{1,0:T(8,128)(2,1)} %param.20) | copy-start | bytes 294916
  88.3 42.8 %copy-start.4 = (f32[2048]{0:T(1024)S(1)}, f32[2048]{0:T(1024)}, u32[]{:S(2)}) copy-start(f32[2048]{0:T(1024)} %param.23) | copy-start | bytes 24580
  109.3 21.8 %all-to-all-start.3 = ((bf16[16,96,128]{2,1,0:T(8,128)(2,1)}), bf16[16,96,128]{2,1,0:T(8,128)(2,1)S(1)}, u32[]{:S(2)}, u32[]{:S(2)}) async-start(bf16[16,96,128]{2,1,0:T(8,128)(2,1)} %bitcast.20), calls=%async_computation.3 | async-start | bytes 786432 | tf_op jit(solution)/shard_map/all_to_all | solution.py:20
  131.1 9.5 %copy-start.14 = (f32[384,2]{0,1:T(2,128)S(1)}, f32[384,2]{0,1:T(2,128)}, u32[]{:S(2)}) copy-start(f32[384,2]{0,1:T(2,128)} %param.25) | copy-start | bytes 9220
  135.6 19.4 %all-to-all-start.4 = ((bf16[16,96,128]{2,1,0:T(8,128)(2,1)}), bf16[16,96,128]{2,1,0:T(8,128)(2,1)S(1)}, u32[]{:S(2)}, u32[]{:S(2)}) async-start(bf16[16,96,128]{2,1,0:T(8,128)(2,1)} %routed_feed.1), calls=%async_computation.4 | async-start | bytes 786432 | tf_op jit(solution)/shard_map/all_to_all | solution.py:20
  155.8 4.9 %copy-start.2 = (bf16[2048,32]{0,1:T(8,128)(2,1)S(1)}, bf16[2048,32]{0,1:T(8,128)(2,1)}, u32[]{:S(2)}) copy-start(bf16[2048,32]{0,1:T(8,128)(2,1)} %param.26) | copy-start | bytes 393220
  155.8 4.9 %copy-start.3 = (bf16[2048,32]{0,1:T(8,128)(2,1)S(1)}, bf16[2048,32]{0,1:T(8,128)(2,1)}, u32[]{:S(2)}) copy-start(bf16[2048,32]{0,1:T(8,128)(2,1)} %param.27) | copy-start | bytes 393220
  155.8 24.1 %all-to-all-start.5 = ((bf16[32,48,128]{2,1,0:T(8,128)(2,1)}), bf16[32,48,128]{2,1,0:T(8,128)(2,1)S(1)}, u32[]{:S(2)}, u32[]{:S(2)}) async-start(bf16[32,48,128]{2,1,0:T(8,128)(2,1)} %bitcast.27), calls=%async_computation.5 | async-start | bytes 786432 | tf_op jit(solution)/shard_map/all_to_all | solution.py:20
  159.8 19.1 %copy-start.5 = (bf16[384,128]{1,0:T(8,128)(2,1)S(1)}, bf16[384,128]{1,0:T(8,128)(2,1)}, u32[]{:S(2)}) copy-start(bf16[384,128]{1,0:T(8,128)(2,1)} %fusion.8) | copy-start | bytes 294916
  159.9 19.0 %copy-start.7 = (bf16[512,128]{1,0:T(8,128)(2,1)S(1)}, bf16[512,128]{1,0:T(8,128)(2,1)}, u32[]{:S(2)}) copy-start(bf16[512,128]{1,0:T(8,128)(2,1)} %param.28) | copy-start | bytes 393220
  160.7 1.4 copy-start.1
  179.9 0.9 copy-start.6
Sparse Core Ops, SparseCore 0:
  9.5 87.9 all-gather.7
  99.6 42.9 all-gather.5

commit v8 on v7

--- a/solution.py
+++ b/solution.py
@@ -18,10 +18,6 @@
 
 def exchange(value, axis):
     return lax.all_to_all(value, axis, split_axis=0, concat_axis=0, tiled=True)
-
-
-def copy_to_each(value, axis):
-    return exchange(jnp.broadcast_to(value, (lax.axis_size(axis), *value.shape)), axis)
 
 
 def three_parts(value):
@@ -255,9 +251,48 @@
         out_shape=jax.ShapeDtypeStruct((gate.shape[0], rows.shape[1]), BF16),
         in_specs=[pl.BlockSpec(memory_space=pltpu.VMEM) for _ in range(4)],
         out_specs=pl.BlockSpec(memory_space=pltpu.VMEM),
-        compiler_params=pltpu.CompilerParams(vmem_limit_bytes=24 * 1024 * 1024),
+        compiler_params=pltpu.CompilerParams(vmem_limit_bytes=60 * 1024 * 1024),
         name="shared_feed",
     )(rows, gain, gate, upward)
+
+
+def copies_kernel(key_t, value_t, out):
+    both = jnp.concatenate([key_t[...], value_t[...]], axis=0)
+    for n in range(out.shape[0]):
+        out[n] = both
+
+
+def key_value_copies(key_t, value_t, count):
+    head, width = key_t.shape
+    return pl.pallas_call(
+        copies_kernel,
+        out_shape=jax.ShapeDtypeStruct((count, 2 * head, width), BF16),
+        in_specs=[pl.BlockSpec(memory_space=pltpu.VMEM) for _ in range(2)],
+        out_specs=pl.BlockSpec(memory_space=pltpu.VMEM),
+        name="key_value_copies",
+    )(key_t, value_t)
+
+
+def final_kernel(share_hidden, sh_down, weight_high, weight_low, answers, updated, out):
+    shared = lax.dot_general(
+        share_hidden[...], sh_down[...], (((0,), (0,)), ((), ())), preferred_element_type=F32
+    )
+    rows = answers[...]
+    routed = jnp.dot(weight_high[...], rows, preferred_element_type=F32) + jnp.dot(
+        weight_low[...], rows, preferred_element_type=F32
+    )
+    out[...] = (updated[...].astype(F32) + shared + routed).astype(BF16)
+
+
+def final_sum(*operands):
+    return pl.pallas_call(
+        final_kernel,
+        out_shape=jax.ShapeDtypeStruct(operands[-1].shape, BF16),
+        in_specs=[pl.BlockSpec(memory_space=pltpu.VMEM) for _ in operands],
+        out_specs=pl.BlockSpec(memory_space=pltpu.VMEM),
+        compiler_params=pltpu.CompilerParams(vmem_limit_bytes=24 * 1024 * 1024),
+        name="final_sum",
+    )(*operands)
 
 
 def per_device(
@@ -290,8 +325,7 @@
     owners = shards // local_experts
 
     scale = head ** (-0.5)
-    key_value = jnp.concatenate([keys.T, values.T], axis=0)
-    key_value = copy_to_each(key_value, near)
+    key_value = exchange(key_value_copies(keys.T, values.T, group), near)
     query = (queries.T.astype(F32) * scale).astype(BF16)
     teams = lax.axis_size("zh")
     moved = [
@@ -360,13 +394,7 @@
     answers = exchange(returned, whole).reshape(slots, LANES)
     share_hidden = shared_feed(all_rows, gain, sh_gate.T, sh_up.T)
     share_hidden = lax.all_gather(share_hidden, "tp", axis=0, tiled=True)
-    shared = lax.dot_general(
-        share_hidden, sh_down, (((0,), (0,)), ((), ())), preferred_element_type=F32
-    )
-    routed = jnp.dot(weight_high, answers, preferred_element_type=F32) + jnp.dot(
-        weight_low, answers, preferred_element_type=F32
-    )
-    return (updated.astype(F32) + shared + routed).astype(BF16)
+    return final_sum(share_hidden, sh_down, weight_high, weight_low, answers, updated)
 
 
 def solution(mesh):

time: 190 us -> 190 us (level)
  Pallas kernels: 16.4 us -> 21.8 us
  matrix products: 5.23 us -> 2.65 us
  local copies, waits for them, and re-layouts: 5.37 us -> 3.33 us
    pallas_call x0 -> x2, Pallas kernels: none -> 3.35 us  [the longest x1 1.81 us: key_value_copies(): pl.pallas_call(copies_kernel, out_shape=jax.ShapeDtypeStruct((count, 2 *...]
    dot_general x3 -> x0, matrix products: 2.58 us -> none  [the longest x1 1.12 us: per_device(): jnp.dot(weight_low, answers, preferred_element_type=F32)]
    pallas_call x1, Pallas kernels: 1.23 us -> 3.3 us  [shared_feed(): pl.pallas_call(shared_kernel, out_shape=jax.ShapeDtypeStruct((gate.shape[...]
  transfers between devices with their start and end apart: 10 -> 10, of which waited for: 5 -> 5; matrix products, arithmetic and copies ran while one was open for 5% -> 4% of each run, Pallas kernels for 8% -> 10%
where the time goes in v8:
time: 190 us; the launch traced here: 189 us
  blocking collectives  63.5 us (33%)
  waiting for transfers between devices  41.1 us (22%)
  starting transfers between devices  40.9 us (22%)
  Pallas kernels  21.8 us (11%)
  between operations  13.6 us (7%)
  local copies, waits for them, and re-layouts  3.33 us (2%)
  matrix products  2.65 us (1%)
  other arithmetic  2.27 us (1%)
    all_to_all x5, waiting for transfers between devices, exchange(): return lax.all_to_all(value, axis, split_axis=0, concat_axis=0, tiled=True)  38.9 us
    all_gather x1, blocking collectives, per_device(): lax.all_gather(head_out[None], 'tp', axis=0, tiled=True).astype(F32)  27.5 us
    all_to_all x5, starting transfers between devices, exchange(): return lax.all_to_all(value, axis, split_axis=0, concat_axis=0, tiled=True)  23.7 us
    all_to_all x1, blocking collectives, exchange(): return lax.all_to_all(value, axis, split_axis=0, concat_axis=0, tiled=True)  20.2 us
    ppermute x3, starting transfers between devices, per_device(): lax.ppermute(query, 'zh', [(i, (i + n) % teams) for i in range(teams)])  17.1 us
    all_gather x1, blocking collectives, per_device(): share_hidden = lax.all_gather(share_hidden, 'tp', axis=0, tiled=True)  15.8 us
    pallas_call x1, Pallas kernels, partial_attention(): pl.pallas_call(attention_kernel, out_shape=jax.ShapeDtypeStruct((teams, h...  8.46 us
    pallas_call x1, Pallas kernels, feed_forward(): pl.pallas_call(lambda *refs: feed_kernel(*refs, experts=experts), out_sha...  4.55 us
  transfers between devices with their start and end apart: 10, of which 5 were waited for; matrix products, arithmetic and copies ran while one was open for 4% of the time, Pallas kernels for 10%

profile of v8, /device:TPU:1, one launch (start us, length us, event | category | flops | bytes accessed | tf_op | source)
XLA Modules:
  0.0 189.2 jit_solution(16549716138723703922)
XLA Ops:
  6.5 0.0 copy-start
  6.5 0.0 all-gather.8.cloned.1.call-start
  6.5 0.0 copy-start.5
  6.5 0.0 copy-start.6
  6.5 2.1 %pack_shards.1 = bf16[3072,128]{1,0:T(8,128)(2,1)} custom-call(bf16[2,32,2048]{2,1,0:T(8,128)(2,1)} %bitcast.58, bf16[2,32,2048]{2,1,0:T(8,128)(2,1)} %bitcast.59, bf16[1024,128]{1,0:T(8,128)(2,1)} %bitcast.60), custom_call_target="tpu_custom_call" | custom-call | tf_op jit(solution)/shard_map/pack_shards/pallas_call | solution.py:159
  8.7 0.0 copy-start.7
  8.7 0.0 all-gather.8.cloned.1.call-update
  8.7 1.8 key_value_copies.1
  10.5 6.6 %all-to-all-start = ((bf16[8,128,384]{2,1,0:T(8,128)(2,1)}), bf16[8,128,384]{2,1,0:T(8,128)(2,1)S(1)}, u32[]{:S(2)}, u32[]{:S(2)}) async-start(bf16[8,128,384]{2,1,0:T(8,128)(2,1)} %key_value_copies.1), calls=%async_computation | async-start | bytes 1572864 | tf_op jit(solution)/shard_map/all_to_all | solution.py:20
  17.2 0.0 copy-done.5
  17.2 5.8 %collective-permute-start = (bf16[64,384]{1,0:T(8,128)(2,1)S(1)}, bf16[64,384]{1,0:T(8,128)(2,1)S(1)}, u32[]{:S(2)}, u32[]{:S(2)}) collective-permute-start(bf16[64,384]{1,0:T(8,128)(2,1)S(1)} %get-tuple-element.20), channel_id=1, source_target_pairs={{0,128},{128,256},{256,384},{384,0},{1,129},{129,257},{257,385},{3... | collective-permute-start | bytes 147464 | tf_op jit(solution)/shard_map/ppermute | solution.py:332
  23.0 7.9 %collective-permute-start.1 = (bf16[64,384]{1,0:T(8,128)(2,1)S(1)}, bf16[64,384]{1,0:T(8,128)(2,1)S(1)}, u32[]{:S(2)}, u32[]{:S(2)}) collective-permute-start(bf16[64,384]{1,0:T(8,128)(2,1)S(1)} %get-tuple-element.20), channel_id=1, source_target_pairs={{0,256},{128,384},{256,0},{384,128},{1,257},{129,385},{257,1},{385... | collective-permute-start | bytes 147464 | tf_op jit(solution)/shard_map/ppermute | solution.py:332
  31.0 3.4 %collective-permute-start.2 = (bf16[64,384]{1,0:T(8,128)(2,1)S(1)}, bf16[64,384]{1,0:T(8,128)(2,1)S(1)}, u32[]{:S(2)}, u32[]{:S(2)}) collective-permute-start(bf16[64,384]{1,0:T(8,128)(2,1)S(1)} %get-tuple-element.20), channel_id=1, source_target_pairs={{0,384},{128,0},{256,128},{384,256},{1,385},{129,1},{257,129},{385... | collective-permute-start | bytes 147464 | tf_op jit(solution)/shard_map/ppermute | solution.py:332
  34.4 0.0 copy-done.6
  34.4 0.2 select_reduce_fusion.1
  34.6 0.7 constant_dynamic-slice_fusion.cum
  35.4 0.1 pad_add_fusion.place
  35.4 0.0 copy-done.7
  35.4 0.1 mul.75
  35.5 0.2 collective-permute-done
  35.7 2.0 %collective-permute-done.1 = bf16[64,384]{1,0:T(8,128)(2,1)S(1)} collective-permute-done((bf16[64,384]{1,0:T(8,128)(2,1)S(1)}, bf16[64,384]{1,0:T(8,128)(2,1)S(1)}, u32[]{:S(2)}, u32[]{:S(2)}) %collective-permute-start.1) | collective-permute-done | bytes 49184 | tf_op jit(solution)/shard_map/ppermute | solution.py:332
  37.7 0.0 collective-permute-done.2
  37.7 0.0 all-to-all-done.kv
  37.7 8.5 %partial_attention.1 = bf16[4,80,384]{2,1,0:T(8,128)(2,1)} custom-call(s32[2]{0:T(128)S(1)} %pad_add_fusion.place, bf16[8,128,384]{2,1,0:T(8,128)(2,1)S(1)} %all-to-all-done.kv, bf16[4,64,384]{2,1,0:T(8,128)(2,1)S(1)} %pad_maximum_fusion.query, f32[1,3072]{1,0:T(1,128)S(1)} %constant_dynamic-slice_fusion.cum), custom_call_target="tpu_custom_call" | custom-call | tf_op jit(solution)/shard_map/partial_attention/pallas_call | solution.py:117
  46.2 3.4 %all-to-all-start.1 = ((bf16[4,80,384]{2,1,0:T(8,128)(2,1)}), bf16[4,80,384]{2,1,0:T(8,128)(2,1)S(1)}, u32[]{:S(2)}, u32[]{:S(2)}) async-start(bf16[4,80,384]{2,1,0:T(8,128)(2,1)} %partial_attention.1), calls=%async_computation.1 | async-start | bytes 491520 | tf_op jit(solution)/shard_map/all_to_all | solution.py:20
  49.6 0.0 all-gather.6.cloned.1.call-start
  49.6 0.7 fusion.6
  50.3 0.0 copy-start.4
  50.3 7.8 %all-to-all-done.1 = bf16[4,80,384]{2,1,0:T(8,128)(2,1)S(1)} async-done(((bf16[4,80,384]{2,1,0:T(8,128)(2,1)}), bf16[4,80,384]{2,1,0:T(8,128)(2,1)S(1)}, u32[]{:S(2)}, u32[]{:S(2)}) %all-to-all-start.1) | async-done | bytes 245792 | tf_op jit(solution)/shard_map/all_to_all | solution.py:20
  58.3 27.5 %all-gather = bf16[1024,384]{1,0:T(8,128)(2,1)S(1)} all-gather(bf16[64,384]{1,0:T(8,128)(2,1)S(1)} %fusion.9), channel_id=2, replica_groups=mesh['zh'=4,'zl'=2,'x'=4,'tp'=16] {'tp'}, dimensions={0}, use_global_device_ids=true | all-gather | bytes 835584 | tf_op jit(solution)/shard_map/all_gather | solution.py:351
  85.9 0.2 fusion.3
  86.1 0.2 fusion.5
  86.4 0.0 copy-done
  86.4 0.0 copy-done.4
  86.4 1.1 fusion.7.updated
  87.4 0.0 copy-start.3
  87.4 0.0 all-gather.6.cloned.1.call-update
  87.5 1.4 convolution_convert_fusion
  88.8 20.2 %all_to_all.30 = bf16[32,48,128]{2,1,0:T(8,128)(2,1)S(1)} all-to-all(bf16[32,48,128]{2,1,0:T(8,128)(2,1)S(1)} %bitcast.57), channel_id=1, replica_groups=mesh['zh'=4,'zl'=2,'x'=4,'tp'=16] {'zh','zl','x'}, dimensions={0} | all-to-all | bytes 786432 | tf_op jit(solution)/shard_map/all_to_all | solution.py:20
  109.0 0.8 copy.20
  109.8 6.3 %all-to-all-start.3 = ((bf16[16,96,128]{2,1,0:T(8,128)(2,1)}), bf16[16,96,128]{2,1,0:T(8,128)(2,1)S(1)}, u32[]{:S(2)}, u32[]{:S(2)}) async-start(bf16[16,96,128]{2,1,0:T(8,128)(2,1)} %bitcast.20), calls=%async_computation.3 | async-start | bytes 786432 | tf_op jit(solution)/shard_map/all_to_all | solution.py:20
  116.1 16.7 %all-to-all-done.3.refs_1_ = bf16[16,96,128]{2,1,0:T(8,128)(2,1)S(1)} async-done(((bf16[16,96,128]{2,1,0:T(8,128)(2,1)}), bf16[16,96,128]{2,1,0:T(8,128)(2,1)S(1)}, u32[]{:S(2)}, u32[]{:S(2)}) %all-to-all-start.3) | async-done | bytes 393248 | tf_op jit(solution)/shard_map/all_to_all | solution.py:20
  132.7 0.0 all-gather.8.cloned.1.call-done
  132.7 0.0 copy-done.3
  132.7 4.6 %routed_feed.1 = bf16[16,96,128]{2,1,0:T(8,128)(2,1)} custom-call(s32[1]{0:T(128)} %bitcast.16.refs_0_, bf16[16,96,128]{2,1,0:T(8,128)(2,1)S(1)} %all-to-all-done.3.refs_1_, f32[16,1,128]{2,1,0:T(1,128)S(1)} %bitcast.51, bf16[16,3072,128]{2,1,0:T(8,128)(2,1)} %bitcast.52), custom_call_target="tpu_custom_call" | custom-call | tf_op jit(solution)/shard_map/routed_feed/pallas_call | solution.py:214
  137.3 0.0 copy-start.8
  137.3 3.5 %all-to-all-start.4 = ((bf16[16,96,128]{2,1,0:T(8,128)(2,1)}), bf16[16,96,128]{2,1,0:T(8,128)(2,1)S(1)}, u32[]{:S(2)}, u32[]{:S(2)}) async-start(bf16[16,96,128]{2,1,0:T(8,128)(2,1)} %routed_feed.1), calls=%async_computation.4 | async-start | bytes 786432 | tf_op jit(solution)/shard_map/all_to_all | solution.py:20
  140.8 14.5 %all-to-all-done.4 = bf16[16,96,128]{2,1,0:T(8,128)(2,1)S(1)} async-done(((bf16[16,96,128]{2,1,0:T(8,128)(2,1)}), bf16[16,96,128]{2,1,0:T(8,128)(2,1)S(1)}, u32[]{:S(2)}, u32[]{:S(2)}) %all-to-all-start.4) | async-done | bytes 393248 | tf_op jit(solution)/shard_map/all_to_all | solution.py:20
  155.3 0.8 copy.21
  156.1 3.9 %all-to-all-start.5 = ((bf16[32,48,128]{2,1,0:T(8,128)(2,1)}), bf16[32,48,128]{2,1,0:T(8,128)(2,1)S(1)}, u32[]{:S(2)}, u32[]{:S(2)}) async-start(bf16[32,48,128]{2,1,0:T(8,128)(2,1)} %bitcast.27), calls=%async_computation.5 | async-start | bytes 786432 | tf_op jit(solution)/shard_map/all_to_all | solution.py:20
  160.0 0.0 copy-done.8
  160.0 0.0 copy-start.1
  160.0 0.8 fusion
  160.8 0.0 all-gather.6.cloned.1.call-done
  160.8 3.3 %shared_feed.1 = bf16[32,384]{1,0:T(8,128)(2,1)} custom-call(bf16[16,384,128]{2,1,0:T(8,128)(2,1)} %bitcast.54, f32[16,1,128]{2,1,0:T(1,128)} %bitcast.50, bf16[32,2048]{1,0:T(8,128)(2,1)} %bitcast.61, bf16[32,2048]{1,0:T(8,128)(2,1)} %bitcast.62), custom_call_target="tpu_custom_call" | custom-call | tf_op jit(solution)/shard_map/shared_feed/pallas_call | solution.py:249
  164.1 15.8 %all_gather.17.share_hidden = bf16[512,384]{1,0:T(8,128)(2,1)S(1)} all-gather(bf16[32,384]{1,0:T(8,128)(2,1)} %shared_feed.1), channel_id=1, replica_groups=mesh['zh'=4,'zl'=2,'x'=4,'tp'=16] {'tp'}, dimensions={0}, use_global_device_ids=true | all-gather | bytes 417792 | tf_op jit(solution)/shard_map/all_gather | solution.py:396
  179.9 0.0 all-to-all-done.5
  179.9 0.0 copy-done.1
  179.9 0.0 copy-start.2
  179.9 0.9 copy-done.2
  180.8 1.5 final_sum.1
  (15 shorter events, 0.3 us)
Async XLA Ops:
  6.5 79.8 %copy-start = (bf16[1024,128]{1,0:T(8,128)(2,1)S(1)}, bf16[1024,128]{1,0:T(8,128)(2,1)}, u32[]{:S(2)}) copy-start(bf16[1024,128]{1,0:T(8,128)(2,1)} %param.22) | copy-start | bytes 786436
  6.5 126.2 %all-gather.8.cloned.1.call-start = ((), (), s32[]{:S(2)}) async-start(), calls=%async_computation.7 | async-start | bytes 13369344 | tf_op jit(solution)/shard_map/all_gather | solution.py:340
  6.5 10.6 %copy-start.5 = (bf16[384,64]{0,1:T(8,128)(2,1)S(1)}, bf16[384,64]{0,1:T(8,128)(2,1)}, u32[]{:S(2)}) copy-start(bf16[384,64]{0,1:T(8,128)(2,1)} %param.16) | copy-start | bytes 147460
  6.5 27.8 %copy-start.6 = (s32[384,2]{0,1:T(2,128)S(1)}, s32[384,2]{0,1:T(2,128)}, u32[]{:S(2)}) copy-start(s32[384,2]{0,1:T(2,128)} %param.24) | copy-start | bytes 9220
  8.7 26.8 %copy-start.7 = (f32[1024]{0:T(1024)S(1)}, f32[1024]{0:T(1024)}, u32[]{:S(2)}) copy-start(f32[1024]{0:T(1024)} %param.21) | copy-start | bytes 12292
  10.5 27.2 %all-to-all-start = ((bf16[8,128,384]{2,1,0:T(8,128)(2,1)}), bf16[8,128,384]{2,1,0:T(8,128)(2,1)S(1)}, u32[]{:S(2)}, u32[]{:S(2)}) async-start(bf16[8,128,384]{2,1,0:T(8,128)(2,1)} %key_value_copies.1), calls=%async_computation | async-start | bytes 1572864 | tf_op jit(solution)/shard_map/all_to_all | solution.py:20
  17.2 18.5 %collective-permute-start = (bf16[64,384]{1,0:T(8,128)(2,1)S(1)}, bf16[64,384]{1,0:T(8,128)(2,1)S(1)}, u32[]{:S(2)}, u32[]{:S(2)}) collective-permute-start(bf16[64,384]{1,0:T(8,128)(2,1)S(1)} %get-tuple-element.20), channel_id=1, source_target_pairs={{0,128},{128,256},{256,384},{384,0},{1,129},{129,257},{257,385},{3... | collective-permute-start | bytes 147464 | tf_op jit(solution)/shard_map/ppermute | solution.py:332
  23.0 14.6 %collective-permute-start.1 = (bf16[64,384]{1,0:T(8,128)(2,1)S(1)}, bf16[64,384]{1,0:T(8,128)(2,1)S(1)}, u32[]{:S(2)}, u32[]{:S(2)}) collective-permute-start(bf16[64,384]{1,0:T(8,128)(2,1)S(1)} %get-tuple-element.20), channel_id=1, source_target_pairs={{0,256},{128,384},{256,0},{384,128},{1,257},{129,385},{257,1},{385... | collective-permute-start | bytes 147464 | tf_op jit(solution)/shard_map/ppermute | solution.py:332
  31.0 6.7 %collective-permute-start.2 = (bf16[64,384]{1,0:T(8,128)(2,1)S(1)}, bf16[64,384]{1,0:T(8,128)(2,1)S(1)}, u32[]{:S(2)}, u32[]{:S(2)}) collective-permute-start(bf16[64,384]{1,0:T(8,128)(2,1)S(1)} %get-tuple-element.20), channel_id=1, source_target_pairs={{0,384},{128,0},{256,128},{384,256},{1,385},{129,1},{257,129},{385... | collective-permute-start | bytes 147464 | tf_op jit(solution)/shard_map/ppermute | solution.py:332
  46.2 12.0 %all-to-all-start.1 = ((bf16[4,80,384]{2,1,0:T(8,128)(2,1)}), bf16[4,80,384]{2,1,0:T(8,128)(2,1)S(1)}, u32[]{:S(2)}, u32[]{:S(2)}) async-start(bf16[4,80,384]{2,1,0:T(8,128)(2,1)} %partial_attention.1), calls=%async_computation.1 | async-start | bytes 491520 | tf_op jit(solution)/shard_map/all_to_all | solution.py:20
  49.6 111.2 %all-gather.6.cloned.1.call-start = ((), (), s32[]{:S(2)}) async-start(), calls=%async_computation.6 | async-start | bytes 1671168 | tf_op jit(solution)/shard_map/all_gather | solution.py:358
  50.3 36.0 %copy-start.4 = (bf16[384,128]{1,0:T(8,128)(2,1)S(1)}, bf16[384,128]{1,0:T(8,128)(2,1)}, u32[]{:S(2)}) copy-start(bf16[384,128]{1,0:T(8,128)(2,1)} %param.20) | copy-start | bytes 294916
  87.4 45.3 %copy-start.3 = (f32[2048]{0:T(1024)S(1)}, f32[2048]{0:T(1024)}, u32[]{:S(2)}) copy-start(f32[2048]{0:T(1024)} %param.23) | copy-start | bytes 24580
  109.8 23.0 %all-to-all-start.3 = ((bf16[16,96,128]{2,1,0:T(8,128)(2,1)}), bf16[16,96,128]{2,1,0:T(8,128)(2,1)S(1)}, u32[]{:S(2)}, u32[]{:S(2)}) async-start(bf16[16,96,128]{2,1,0:T(8,128)(2,1)} %bitcast.20), calls=%async_computation.3 | async-start | bytes 786432 | tf_op jit(solution)/shard_map/all_to_all | solution.py:20
  137.3 22.7 %copy-start.8 = (f32[384,2]{0,1:T(2,128)S(1)}, f32[384,2]{0,1:T(2,128)}, u32[]{:S(2)}) copy-start(f32[384,2]{0,1:T(2,128)} %param.25) | copy-start | bytes 9220
  137.3 18.0 %all-to-all-start.4 = ((bf16[16,96,128]{2,1,0:T(8,128)(2,1)}), bf16[16,96,128]{2,1,0:T(8,128)(2,1)S(1)}, u32[]{:S(2)}, u32[]{:S(2)}) async-start(bf16[16,96,128]{2,1,0:T(8,128)(2,1)} %routed_feed.1), calls=%async_computation.4 | async-start | bytes 786432 | tf_op jit(solution)/shard_map/all_to_all | solution.py:20
  156.1 23.8 %all-to-all-start.5 = ((bf16[32,48,128]{2,1,0:T(8,128)(2,1)}), bf16[32,48,128]{2,1,0:T(8,128)(2,1)S(1)}, u32[]{:S(2)}, u32[]{:S(2)}) async-start(bf16[32,48,128]{2,1,0:T(8,128)(2,1)} %bitcast.27), calls=%async_computation.5 | async-start | bytes 786432 | tf_op jit(solution)/shard_map/all_to_all | solution.py:20
  160.0 19.9 %copy-start.1 = (bf16[384,128]{1,0:T(8,128)(2,1)S(1)}, bf16[384,128]{1,0:T(8,128)(2,1)}, u32[]{:S(2)}) copy-start(bf16[384,128]{1,0:T(8,128)(2,1)} %fusion.7.updated) | copy-start | bytes 294916
  179.9 0.9 copy-start.2
Sparse Core Ops, SparseCore 0:
  9.5 87.9 all-gather.7
  99.6 43.0 all-gather.5
